TPU v7x, 256 devices: a 4x2x16 block of a 4x16x16 slice. The times are simulated.
256 devices in a mesh: grp: 2 (over y), sp: 16 (over z), tp: 8 (over x, core).
Axes of the slice: x: 4, y: 2, z: 16, core: 2. Of those that a mesh axis runs over, the one named last changes fastest.
The devices are a block of a 4x16x16 slice.
Arguments:
- tokens: bfloat16 [32768, 2048], P(('grp', 'sp')), parts along dimension 0, may hold values from -6 to 6
- doc_ids: int32 [32768], P(('grp', 'sp')), parts along dimension 0, may hold values from 0 to 3, never falling along the last dimension, each value on 1 to 8192 neighbouring positions
- gains: bfloat16 [2, 2048], replicated, may hold values from 0.099609375 to 1.8984375
- w_query: bfloat16 [2, 2048, 1024], P(None, None, 'tp'), may hold values from -0.125 to 0.125
- w_key: bfloat16 [2, 2048, 1024], P(None, None, 'tp'), may hold values from -0.125 to 0.125
- w_value: bfloat16 [2, 2048, 1024], P(None, None, 'tp'), may hold values from -0.125 to 0.125
- rel_table: float32 [2, 16, 257], P(None, 'tp'), may hold values from -6 to 270
- out_first: bfloat16 [1024, 2048], replicated, may hold values from -0.5 to 0.5
- out_last: bfloat16 [1024, 2048], P(None, 'tp'), may hold values from -0.5 to 0.5
Outputs:
- mixed: bfloat16 [32768, 2048], P(('grp', 'sp'), 'tp'), parts along dimension 0
There are 2 independent parts, one for each index of `grp`. A program takes and returns all parts, laid end to end along the dimension named above; an argument that names none is the same for every part. Nothing has to cross between parts.
Inputs may be any that keep to these rules, and one draw needn't show every extreme that they name: `doc_ids`: document numbers never fall along the sequence.
All inputs are finite; a program needn't handle non-finite values.
Results may differ from a plain program's by a relative error of at most 0.014.
Values may be sent and summed in bfloat16 or wider, within the bound.
No kernel may reach another device: no remote copies, remote signals or barrier semaphores. Data moves between devices by JAX's collectives and lax.ppermute only.
A program may use at most 128 MiB of HBM per device.

v0:
```python
import functools

import jax
import jax.numpy as jnp
from jax import lax
from jax.experimental import pallas as pl
from jax.experimental.pallas import tpu as pltpu
from jax.sharding import PartitionSpec as P

SEG = 64
PREV_SEGS = 8
MAX_REL = 128
LAYERS = 2
REACH = PREV_SEGS * SEG
QUERY_ROWS = 2 * SEG
BAND = REACH + QUERY_ROWS
NEG = -1e30
EPS = 1e-06
DOC_ROWS = 16

F32 = jnp.float32
BF16 = jnp.bfloat16


def cost(flops, bytes_accessed, transcendentals=0):
    return pl.CostEstimate(
        flops=flops, bytes_accessed=bytes_accessed, transcendentals=transcendentals
    )


def project_heads(rows, gain, wq, wk, wv, q_scale):
    rows32 = rows.astype(F32)
    inv = lax.rsqrt(jnp.mean(rows32 * rows32, axis=-1, keepdims=True) + EPS)
    scaled = rows * gain
    queries = jnp.dot(scaled, wq, preferred_element_type=F32) * (inv * q_scale)
    wkv = jnp.concatenate([wk, wv], axis=1)
    kv = jnp.dot(scaled, wkv, preferred_element_type=F32) * inv
    return queries.astype(BF16), kv.astype(BF16)


def store_kv(kv_ref, kv, docs_ref, step, block_rows):
    kv_ref[pl.ds(pl.multiple_of(step * block_rows, block_rows), block_rows), :] = kv
    if docs_ref is not None:

        @pl.when(step == 0)
        def _():
            width = kv_ref.shape[1]
            halves = [
                docs_ref[:, part * width : (part + 1) * width]
                for part in range(docs_ref.shape[1] // width)
            ]
            pad = jnp.zeros((DOC_ROWS - len(halves), width), F32)
            kv_ref[-DOC_ROWS:, :] = jnp.concatenate(halves + [pad], axis=0).astype(BF16)


def heads_kernel(q_scale, block_rows, *refs):
    x_ref, gain_ref, wq_ref, wk_ref, wv_ref, *rest = refs
    docs_ref = rest[0] if len(rest) == 3 else None
    q_ref, kv_ref = rest[-2:]
    queries, kv = project_heads(
        x_ref[...], gain_ref[...], wq_ref[...], wk_ref[...], wv_ref[...], q_scale
    )
    q_ref[...] = queries
    store_kv(kv_ref, kv, docs_ref, pl.program_id(0), block_rows)


def weight_specs(depth, width, layer):
    return [
        pl.BlockSpec((None, 1, depth), lambda i, *_: (layer, 0, 0)),
        *[pl.BlockSpec((None, depth, width), lambda i, *_: (layer, 0, 0)) for _ in range(3)],
    ]


def heads(tokens, gains, wq, wk, wv, docs, layer, half, half_rows, q_scale, block_rows=256):
    depth, width = wq.shape[1:]
    steps = half_rows // block_rows
    in_specs = [
        pl.BlockSpec((block_rows, depth), lambda i: (i + half * steps, 0)),
        *weight_specs(depth, width, layer),
    ]
    args = [tokens, gains, wq, wk, wv]
    extra = 0
    if half == 1:
        in_specs.append(pl.BlockSpec((1, half_rows), lambda i: (0, half)))
        args.append(docs)
        extra = DOC_ROWS
    return pl.pallas_call(
        functools.partial(heads_kernel, q_scale, block_rows),
        grid=(steps,),
        in_specs=in_specs,
        out_specs=[
            pl.BlockSpec((block_rows, width), lambda i: (i, 0)),
            pl.BlockSpec((half_rows + extra, 2 * width), lambda i: (0, 0)),
        ],
        out_shape=[
            jax.ShapeDtypeStruct((half_rows, width), BF16),
            jax.ShapeDtypeStruct((half_rows + extra, 2 * width), BF16),
        ],
        cost_estimate=cost(6 * half_rows * depth * width, 2 * depth * (half_rows + 3 * width)),
        name="heads",
    )(*args)


def bias_kernel(line_ref, out_ref):
    width = line_ref.shape[1]
    row = lax.broadcasted_iota(jnp.int32, (QUERY_ROWS, BAND), 0)
    col = lax.broadcasted_iota(jnp.int32, (QUERY_ROWS, BAND), 1)
    upper = row >= SEG
    seen = jnp.logical_and(
        jnp.logical_or(jnp.logical_not(upper), col >= SEG),
        jnp.logical_or(upper, col < BAND - SEG),
    )
    for item in range(line_ref.shape[0]):
        lines = jnp.broadcast_to(line_ref[item : item + 1, :], (QUERY_ROWS, width))
        rolled = pltpu.roll(lines, 0, 1, stride=1, stride_axis=0)
        out_ref[item] = jnp.where(seen, rolled[:, :BAND], NEG)


def bias_blocks(rel_table):
    layers, head_count, table_width = rel_table.shape
    flipped = jnp.flip(rel_table[:, :, 1:], axis=2)
    far = jnp.broadcast_to(rel_table[:, :, -1:], (layers, head_count, REACH - MAX_REL))
    tail = jnp.broadcast_to(rel_table[:, :, -1:], (layers, head_count, QUERY_ROWS))
    line = jnp.concatenate([far, flipped, tail], axis=2).reshape(layers * head_count, -1)
    return pl.pallas_call(
        bias_kernel,
        out_shape=jax.ShapeDtypeStruct((layers * head_count, QUERY_ROWS, BAND), F32),
        cost_estimate=cost(layers * head_count * QUERY_ROWS * BAND * 4, 0),
        name="bias",
    )(line)


def attention_kernel(head_width, from_far, *refs):
    if from_far:
        q_ref, lo_ref, hi_ref, docs_ref, bias_ref, out_ref = refs
        docs_rows = lo_ref[-DOC_ROWS:, :].astype(F32)
        width = docs_rows.shape[1]
        parts = q_ref.shape[0] // width
        docs_lo = jnp.concatenate([docs_rows[i : i + 1] for i in range(parts)], axis=1)
        docs_hi = docs_ref[...]
    else:
        q_ref, lo_ref, hi_ref, docs_ref, bias_ref, out_ref = refs
        docs_lo = docs_ref[:, : q_ref.shape[0]]
        docs_hi = docs_ref[:, q_ref.shape[0] :]
    half_rows, width = q_ref.shape
    head_count = width // head_width
    lane = lax.broadcasted_iota(jnp.int32, (QUERY_ROWS, width), 1) // head_width
    square = (QUERY_ROWS, QUERY_ROWS)
    diagonal = lax.broadcasted_iota(jnp.int32, square, 0) == lax.broadcasted_iota(
        jnp.int32, square, 1
    )
    ones = jnp.ones((BAND, width), BF16)
    bias = [bias_ref[head] for head in range(head_count)]
    for block in range(half_rows // QUERY_ROWS):
        start = block * QUERY_ROWS
        stop = start + QUERY_ROWS
        kv = jnp.concatenate([lo_ref[start:half_rows, :], hi_ref[:stop, :]], axis=0)
        docs_keys = jnp.concatenate([docs_lo[:, start:], docs_hi[:, :stop]], axis=1)
        docs_queries = jnp.sum(
            jnp.where(diagonal, docs_hi[:, start:stop], 0.0), axis=1, keepdims=True
        )
        same = docs_keys == docs_queries
        queries = q_ref[start:stop, :]
        zero = jnp.zeros_like(queries)
        stacked = jnp.concatenate(
            [jnp.where(lane == head, queries, zero) for head in range(head_count)], axis=0
        )
        scores = lax.dot_general(
            stacked, kv[:, :width], (((1,), (1,)), ((), ())), preferred_element_type=F32
        )
        weights = []
        for head in range(head_count):
            part = scores[head * QUERY_ROWS : (head + 1) * QUERY_ROWS] + bias[head]
            part = jnp.where(same, part, NEG)
            top = jnp.max(part, axis=1, keepdims=True)
            weights.append(jnp.exp(part - top).astype(BF16))
        weights = jnp.concatenate(weights, axis=0)
        summed = jnp.dot(
            weights,
            jnp.concatenate([kv[:, width:], ones], axis=1),
            preferred_element_type=F32,
        )
        result = summed[:, :width] / summed[:, width:]
        mine = result[:QUERY_ROWS]
        for head in range(1, head_count):
            mine = jnp.where(lane == head, result[head * QUERY_ROWS : (head + 1) * QUERY_ROWS], mine)
        out_ref[start:stop, :] = mine.astype(BF16)


def attention(queries, lo, hi, docs, biases, layer, head_width, from_far):
    half_rows, width = queries.shape
    head_count = width // head_width
    return pl.pallas_call(
        functools.partial(attention_kernel, head_width, from_far),
        grid=(1,),
        in_specs=[
            pl.BlockSpec(queries.shape, lambda i: (0, 0)),
            pl.BlockSpec(lo.shape, lambda i: (0, 0)),
            pl.BlockSpec(hi.shape, lambda i: (0, 0)),
            pl.BlockSpec((1, half_rows if from_far else 2 * half_rows), lambda i: (0, 0)),
            pl.BlockSpec((head_count, QUERY_ROWS, BAND), lambda i: (layer, 0, 0)),
        ],
        out_specs=pl.BlockSpec(queries.shape, lambda i: (0, 0)),
        out_shape=jax.ShapeDtypeStruct(queries.shape, BF16),
        cost_estimate=cost(
            8 * half_rows * BAND * width, 4 * head_count * QUERY_ROWS * BAND, half_rows * BAND * 2
        ),
        name="attend",
    )(queries, lo, hi, docs, biases)


def gather(block):
    chips = lax.axis_size("tp") // 2
    pairs = [(x, core) for x in range(chips) for core in range(2)]

    def moved(array, by, other=False):
        return lax.ppermute(
            array,
            "tp",
            [
                (2 * x + core, 2 * ((x + by) % chips) + (1 - core if other else core))
                for x, core in pairs
            ],
        )

    received = [moved(block, by) for by in range(1, chips)]
    partner = moved(block, 0, True)
    partners = moved(jnp.stack(received), 0, True)
    return [block, partner, *received, partners]


def slots_of(me, chips):
    x, core = me // 2, me % 2
    others = [(x + chips - by) % chips for by in range(1, chips)]
    return [
        2 * x + core,
        2 * x + 1 - core,
        *[2 * other + core for other in others],
        *[2 * other + 1 - core for other in others],
    ]


def place(me_ref, block_refs, slots_ref):
    chips = slots_ref.shape[0] // 2
    arrays = [ref[...] for ref in block_refs[:-1]]
    arrays += [block_refs[-1][i] for i in range(chips - 1)]
    for slot, array in zip(slots_of(me_ref[0], chips), arrays):
        slots_ref[slot] = array
    return jnp.concatenate([slots_ref[i] for i in range(2 * chips)], axis=1)


def gathered_specs(blocks, block_rows):
    width = blocks[0].shape[1]
    specs = [pl.BlockSpec((block_rows, width), lambda i, *_: (i, 0)) for _ in blocks[:-1]]
    count = blocks[-1].shape[0]
    specs.append(pl.BlockSpec((count, block_rows, width), lambda i, *_: (0, i, 0)))
    return specs


def next_kernel(q_scale, block_rows, gathered_count, *refs):
    me_ref, *refs = refs
    block_refs, refs = refs[:gathered_count], refs[gathered_count:]
    x_ref, w_ref, gain_ref, wq_ref, wk_ref, wv_ref, *rest = refs
    docs_ref = rest[0] if len(rest) == 6 else None
    q_ref, kv_ref, own_ref, slots_ref, cols_ref = rest[-5:]
    attended = place(me_ref, block_refs, slots_ref)
    update = jnp.dot(attended, w_ref[...], preferred_element_type=F32)
    hidden = (x_ref[...].astype(F32) + update).astype(BF16)
    col_width = own_ref.shape[1]
    for part in range(cols_ref.shape[0]):
        cols_ref[part] = hidden[:, part * col_width : (part + 1) * col_width]
    own_ref[...] = cols_ref[me_ref[0]]
    queries, kv = project_heads(
        hidden, gain_ref[...], wq_ref[...], wk_ref[...], wv_ref[...], q_scale
    )
    q_ref[...] = queries
    store_kv(kv_ref, kv, docs_ref, pl.program_id(0), block_rows)


def next_heads(
    me, blocks, tokens, w_out, gains, wq, wk, wv, docs, layer, half, q_scale, block_rows=256
):
    half_rows, block_width = blocks[0].shape
    depth, width = wq.shape[1:]
    inner = w_out.shape[0]
    members = inner // block_width
    col_width = depth // members
    steps = half_rows // block_rows
    in_specs = [
        *gathered_specs(blocks, block_rows),
        pl.BlockSpec((block_rows, depth), lambda i, *_: (i + half * steps, 0)),
        pl.BlockSpec(w_out.shape, lambda i, *_: (0, 0)),
        *weight_specs(depth, width, layer),
    ]
    args = [*blocks, tokens, w_out, gains, wq, wk, wv]
    extra = 0
    if half == 1:
        in_specs.append(pl.BlockSpec((1, half_rows), lambda i, *_: (0, half)))
        args.append(docs)
        extra = DOC_ROWS
    return pl.pallas_call(
        functools.partial(next_kernel, q_scale, block_rows, len(blocks)),
        grid_spec=pltpu.PrefetchScalarGridSpec(
            num_scalar_prefetch=1,
            grid=(steps,),
            in_specs=in_specs,
            out_specs=[
                pl.BlockSpec((block_rows, width), lambda i, *_: (i, 0)),
                pl.BlockSpec((half_rows + extra, 2 * width), lambda i, *_: (0, 0)),
                pl.BlockSpec((block_rows, col_width), lambda i, *_: (i, 0)),
            ],
            scratch_shapes=[
                pltpu.VMEM((members, block_rows, block_width), BF16),
                pltpu.VMEM((members, block_rows, col_width), BF16),
            ],
        ),
        out_shape=[
            jax.ShapeDtypeStruct((half_rows, width), BF16),
            jax.ShapeDtypeStruct((half_rows + extra, 2 * width), BF16),
            jax.ShapeDtypeStruct((half_rows, col_width), BF16),
        ],
        cost_estimate=cost(
            2 * half_rows * depth * (inner + 3 * width),
            2 * depth * (half_rows + 3 * width + inner),
        ),
        name="next_heads",
    )(me, *args)


def last_kernel(gathered_count, *refs):
    me_ref, *refs = refs
    block_refs, refs = refs[:gathered_count], refs[gathered_count:]
    own_ref, w_ref = refs[:2]
    out_ref, slots_ref = refs[-2:]
    attended = place(me_ref, block_refs, slots_ref)
    update = jnp.dot(attended, w_ref[...], preferred_element_type=F32)
    out_ref[...] = (own_ref[...].astype(F32) + update).astype(BF16)


def last_update(me, blocks, own, w_out, earlier, half, block_rows=256):
    half_rows, block_width = blocks[0].shape
    inner, col_width = w_out.shape
    steps = half_rows // block_rows
    in_specs = [
        *gathered_specs(blocks, block_rows),
        pl.BlockSpec((block_rows, col_width), lambda i, *_: (i, 0)),
        pl.BlockSpec(w_out.shape, lambda i, *_: (0, 0)),
    ]
    args = [me, *blocks, own, w_out]
    aliases = {}
    if earlier is not None:
        in_specs.append(pl.BlockSpec(memory_space=pl.ANY))
        aliases = {len(args): 0}
        args.append(earlier)
    return pl.pallas_call(
        functools.partial(last_kernel, len(blocks)),
        grid_spec=pltpu.PrefetchScalarGridSpec(
            num_scalar_prefetch=1,
            grid=(steps,),
            in_specs=in_specs,
            out_specs=pl.BlockSpec((block_rows, col_width), lambda i, *_: (i + half * steps, 0)),
            scratch_shapes=[pltpu.VMEM((inner // block_width, block_rows, block_width), BF16)],
        ),
        out_shape=jax.ShapeDtypeStruct((2 * half_rows, col_width), BF16),
        input_output_aliases=aliases,
        cost_estimate=cost(
            2 * half_rows * inner * col_width, 2 * inner * (half_rows + col_width)
        ),
        name="last",
    )(*args)


def shards(tokens, doc_ids, gains, w_query, w_key, w_value, rel_table, out_first, out_last):
    row_count = tokens.shape[0]
    half_rows = row_count // 2
    head_count = rel_table.shape[1]
    width = w_query.shape[2]
    head_width = width // head_count
    q_scale = head_width ** (-0.5)
    members = lax.axis_size("sp")
    onward = [(i, i + 1) for i in range(members - 1)]
    me = lax.axis_index("tp").astype(jnp.int32).reshape(1)
    docs = (doc_ids + 1).astype(F32).reshape(1, row_count)
    gains = gains[:, None, :]
    weights = (gains, w_query, w_key, w_value)

    q_late, kv_late = heads(tokens, *weights, docs, 0, 1, half_rows, q_scale)
    far = lax.ppermute(kv_late, "sp", onward)
    q_early, kv_early = heads(tokens, *weights, docs, 0, 0, half_rows, q_scale)
    biases = bias_blocks(rel_table)
    result = None
    for layer in range(LAYERS):
        late = attention(q_late, kv_early, kv_late, docs, biases, layer, head_width, False)
        late = gather(late)
        early = attention(q_early, far, kv_early, docs, biases, layer, head_width, True)
        early = gather(early)
        if layer == 0:
            q_late, kv_late, own_late = next_heads(
                me, late, tokens, out_first, *weights, docs, 1, 1, q_scale
            )
            far = lax.ppermute(kv_late, "sp", onward)
            q_early, kv_early, own_early = next_heads(
                me, early, tokens, out_first, *weights, docs, 1, 0, q_scale
            )
        else:
            result = last_update(me, late, own_late, out_last, None, 1)
            result = last_update(me, early, own_early, out_last, result, 0)
    return result


def solution(mesh):
    placed = (
        P(("grp", "sp"), None),
        P(("grp", "sp")),
        P(),
        P(None, None, "tp"),
        P(None, None, "tp"),
        P(None, None, "tp"),
        P(None, "tp", None),
        P(),
        P(None, "tp"),
    )
    return jax.shard_map(
        shards, mesh=mesh, in_specs=placed, out_specs=P(("grp", "sp"), "tp"), check_vma=False
    )
```

profile of v0, /device:TPU:33, one launch (start us, length us, event | category | flops | bytes accessed | tf_op | source)
XLA Modules:
  0.0 113.1 jit_solution(9203120336212512903)
XLA Ops:
  0.0 1.3 %copy.11.refs_1_.refs_9_ = bf16[2,1,2048]{2,1,0:T(2,128)(2,1)} copy(bf16[2,1,2048]{2,0,1:T(2,128)(2,1)} %bitcast.33) | data formatting | bytes 16384 | tf_op jit(solution)/shard_map/broadcast_in_dim | solution.py:384
  1.3 1.3 %add_convert_fusion = f32[1024]{0:T(1024)} fusion(s32[1024]{0:T(1024)} %param.10), kind=kLoop, calls=%fused_computation.5 | loop fusion | flops 2048 | bytes 8192 | tf_op jit(solution)/shard_map/convert_element_type | solution.py:383
  2.6 3.9 %heads.3 = (bf16[512,128]{1,0:T(8,128)(2,1)}, bf16[528,256]{1,0:T(8,128)(2,1)}) custom-call(bf16[1024,2048]{1,0:T(8,128)(2,1)} %refs_7_.3, bf16[2,1,2048]{2,1,0:T(2,128)(2,1)} %copy.11.refs_1_.refs_9_, bf16[2,2048,128]{2,1,0:T(8,128)(2,1)} %refs_10_.3, bf16[2,2048,128]{2,1,0:T(8,128)(2,1)} %refs_11_.3, bf16[2,2048,128]{2,1,0:T(8,128)(2,1)} %refs_12_.3, ...), custom_call_target="tpu_custom_call" | custom-call | flops 805306368 | bytes 3670016 | tf_op jit(solution)/shard_map/heads/pallas_call | solution.py:87
  6.5 5.4 %collective-permute-start = (bf16[528,256]{1,0:T(8,128)(2,1)}, bf16[528,256]{1,0:T(8,128)(2,1)S(1)}, u32[]{:S(2)}, u32[]{:S(2)}) collective-permute-start(bf16[528,256]{1,0:T(8,128)(2,1)} %get-tuple-element.16.refs_2_), channel_id=1, source_target_pairs={{0,8},{8,16},{16,24},{24,32},{32,40},{40,48},{48,56},{56,64},{64,7... | collective-permute-start | bytes 811016 | tf_op jit(solution)/shard_map/ppermute | solution.py:388
  11.9 3.9 %heads.2 = (bf16[512,128]{1,0:T(8,128)(2,1)}, bf16[512,256]{1,0:T(8,128)(2,1)}) custom-call(bf16[1024,2048]{1,0:T(8,128)(2,1)} %refs_7_.3, bf16[2,1,2048]{2,1,0:T(2,128)(2,1)} %copy.11.refs_1_.refs_9_, bf16[2,2048,128]{2,1,0:T(8,128)(2,1)} %refs_10_.3, bf16[2,2048,128]{2,1,0:T(8,128)(2,1)} %refs_11_.3, bf16[2,2048,128]{2,1,0:T(8,128)(2,1)} %refs_12_.3), custom_call_target="tpu_custom_call" | custom-call | flops 805306368 | bytes 3670016 | tf_op jit(solution)/shard_map/heads/pallas_call | solution.py:87
  16.9 2.3 %bias.1.refs_4_ = f32[4,128,640]{2,1,0:T(8,128)} custom-call(f32[4,768]{1,0:T(4,128)} %reshape.11.line_ref), custom_call_target="tpu_custom_call" | custom-call | flops 1310720 | tf_op jit(solution)/shard_map/bias/pallas_call | solution.py:125
  19.2 3.4 %attend.5.refs_1_ = bf16[512,128]{1,0:T(8,128)(2,1)} custom-call(bf16[512,128]{1,0:T(8,128)(2,1)} %get-tuple-element.19.refs_0_, bf16[512,256]{1,0:T(8,128)(2,1)} %get-tuple-element.17.refs_2_.refs_1_, bf16[528,256]{1,0:T(8,128)(2,1)} %get-tuple-element.16.refs_2_, f32[1,1024]{1,0:T(1,128)} %bitcast.28, f32[4,128,640]{2,1,0:T(8,128)} %bias.1.refs_4_), custom_call_target="tpu_custom_call" | custom-call | flops 335544320 | bytes 655360 | tf_op jit(solution)/shard_map/attend/pallas_call | solution.py:193
  22.6 1.3 %collective-permute-start.7 = (bf16[512,128]{1,0:T(8,128)(2,1)}, bf16[512,128]{1,0:T(8,128)(2,1)S(1)}, u32[]{:S(2)}, u32[]{:S(2)}) collective-permute-start(bf16[512,128]{1,0:T(8,128)(2,1)} %attend.5.refs_1_), channel_id=1, source_target_pairs={{0,2},{1,3},{2,4},{3,5},{4,6},{5,7},{6,0},{7,1},{8,10},{9,11},{10,... | collective-permute-start | bytes 393224 | tf_op jit(solution)/shard_map/ppermute | solution.py:217
  24.0 2.7 %collective-permute-start.8 = (bf16[512,128]{1,0:T(8,128)(2,1)}, bf16[512,128]{1,0:T(8,128)(2,1)S(1)}, u32[]{:S(2)}, u32[]{:S(2)}) collective-permute-start(bf16[512,128]{1,0:T(8,128)(2,1)} %attend.5.refs_1_), channel_id=1, source_target_pairs={{0,4},{1,5},{2,6},{3,7},{4,0},{5,1},{6,2},{7,3},{8,12},{9,13},{10,... | collective-permute-start | bytes 393224 | tf_op jit(solution)/shard_map/ppermute | solution.py:217
  26.7 1.0 collective-permute-start.9
  28.1 4.0 %collective-permute-done.8.refs_4_ = bf16[512,128]{1,0:T(8,128)(2,1)S(1)} collective-permute-done((bf16[512,128]{1,0:T(8,128)(2,1)}, bf16[512,128]{1,0:T(8,128)(2,1)S(1)}, u32[]{:S(2)}, u32[]{:S(2)}) %collective-permute-start.8) | collective-permute-done | bytes 131104 | tf_op jit(solution)/shard_map/ppermute | solution.py:217
  32.1 15.8 %collective-permute-start.10 = (bf16[3,512,128]{2,1,0:T(8,128)(2,1)S(1)}, bf16[3,512,128]{2,1,0:T(8,128)(2,1)S(1)}, u32[]{:S(2)}, u32[]{:S(2)}) collective-permute-start(bf16[3,512,128]{2,1,0:T(8,128)(2,1)S(1)} %pad_maximum_fusion.1), channel_id=1, source_target_pairs={{0,1},{1,0},{2,3},{3,2},{4,5},{5,4},{6,7},{7,6},{8,9},{9,8},{10,11... | collective-permute-start | bytes 1179656 | tf_op jit(solution)/shard_map/ppermute | solution.py:217
  48.7 3.4 %attend.4.refs_1_ = bf16[512,128]{1,0:T(8,128)(2,1)} custom-call(bf16[512,128]{1,0:T(8,128)(2,1)} %get-tuple-element.15.refs_0_, bf16[528,256]{1,0:T(8,128)(2,1)} %copy-done.16, bf16[512,256]{1,0:T(8,128)(2,1)} %get-tuple-element.17.refs_2_.refs_1_, f32[1,1024]{1,0:T(1,128)} %bitcast.29, f32[4,128,640]{2,1,0:T(8,128)} %bias.1.refs_4_), custom_call_target="tpu_custom_call" | custom-call | flops 335544320 | bytes 655360 | tf_op jit(solution)/shard_map/attend/pallas_call | solution.py:193
  52.4 2.9 %collective-permute-start.3 = (bf16[512,128]{1,0:T(8,128)(2,1)}, bf16[512,128]{1,0:T(8,128)(2,1)S(1)}, u32[]{:S(2)}, u32[]{:S(2)}) collective-permute-start(bf16[512,128]{1,0:T(8,128)(2,1)} %attend.4.refs_1_), channel_id=1, source_target_pairs={{0,4},{1,5},{2,6},{3,7},{4,0},{5,1},{6,2},{7,3},{8,12},{9,13},{10,... | collective-permute-start | bytes 393224 | tf_op jit(solution)/shard_map/ppermute | solution.py:217
  55.9 2.6 %collective-permute-done.2.refs_3_ = bf16[512,128]{1,0:T(8,128)(2,1)S(1)} collective-permute-done((bf16[512,128]{1,0:T(8,128)(2,1)}, bf16[512,128]{1,0:T(8,128)(2,1)S(1)}, u32[]{:S(2)}, u32[]{:S(2)}) %collective-permute-start.2) | collective-permute-done | bytes 131104 | tf_op jit(solution)/shard_map/ppermute | solution.py:217
  58.5 3.4 %collective-permute-done.3.refs_4_ = bf16[512,128]{1,0:T(8,128)(2,1)S(1)} collective-permute-done((bf16[512,128]{1,0:T(8,128)(2,1)}, bf16[512,128]{1,0:T(8,128)(2,1)S(1)}, u32[]{:S(2)}, u32[]{:S(2)}) %collective-permute-start.3) | collective-permute-done | bytes 131104 | tf_op jit(solution)/shard_map/ppermute | solution.py:217
  62.0 1.0 collective-permute-start.5
  64.1 7.9 %next_heads.3 = (bf16[512,128]{1,0:T(8,128)(2,1)}, bf16[528,256]{1,0:T(8,128)(2,1)}, bf16[512,256]{1,0:T(8,128)(2,1)}) custom-call(s32[1]{0:T(128)} %bitcast.refs_0_, bf16[512,128]{1,0:T(8,128)(2,1)} %attend.5.refs_1_, bf16[512,128]{1,0:T(8,128)(2,1)} %copy-done.18, bf16[512,128]{1,0:T(8,128)(2,1)} %copy-done, bf16[512,128]{1,0:T(8,128)(2,1)} %copy-done.1, ...), custom_call_target="tpu_custom_call" | custom-call | flops 2952790016 | bytes 7864320 | tf_op jit(solution)/shard_map/next_heads/pallas_call | solution.py:301
  72.1 1.3 %collective-permute-start.11 = (bf16[528,256]{1,0:T(8,128)(2,1)}, bf16[528,256]{1,0:T(8,128)(2,1)S(1)}, u32[]{:S(2)}, u32[]{:S(2)}) collective-permute-start(bf16[528,256]{1,0:T(8,128)(2,1)} %get-tuple-element.20.refs_2_), channel_id=1, source_target_pairs={{0,8},{8,16},{16,24},{24,32},{32,40},{40,48},{48,56},{56,64},{64,7... | collective-permute-start | bytes 811016 | tf_op jit(solution)/shard_map/ppermute | solution.py:401
  74.8 7.7 %next_heads.2 = (bf16[512,128]{1,0:T(8,128)(2,1)}, bf16[512,256]{1,0:T(8,128)(2,1)}, bf16[512,256]{1,0:T(8,128)(2,1)}) custom-call(s32[1]{0:T(128)} %bitcast.refs_0_, bf16[512,128]{1,0:T(8,128)(2,1)} %attend.4.refs_1_, bf16[512,128]{1,0:T(8,128)(2,1)} %copy-done.19, bf16[512,128]{1,0:T(8,128)(2,1)} %copy-done.3, bf16[512,128]{1,0:T(8,128)(2,1)} %copy-done.4, ...), custom_call_target="tpu_custom_call" | custom-call | flops 2952790016 | bytes 7864320 | tf_op jit(solution)/shard_map/next_heads/pallas_call | solution.py:301
  82.4 3.4 %attend.7.refs_1_ = bf16[512,128]{1,0:T(8,128)(2,1)} custom-call(bf16[512,128]{1,0:T(8,128)(2,1)} %get-tuple-element.23.refs_0_, bf16[512,256]{1,0:T(8,128)(2,1)} %get-tuple-element.21.refs_2_.refs_1_, bf16[528,256]{1,0:T(8,128)(2,1)} %get-tuple-element.20.refs_2_, f32[1,1024]{1,0:T(1,128)} %bitcast.31, f32[4,128,640]{2,1,0:T(8,128)} %bias.1.refs_4_), custom_call_target="tpu_custom_call" | custom-call | flops 335544320 | bytes 655360 | tf_op jit(solution)/shard_map/attend/pallas_call | solution.py:193
  85.9 3.5 %collective-permute-start.19 = (bf16[512,128]{1,0:T(8,128)(2,1)}, bf16[512,128]{1,0:T(8,128)(2,1)S(1)}, u32[]{:S(2)}, u32[]{:S(2)}) collective-permute-start(bf16[512,128]{1,0:T(8,128)(2,1)} %attend.7.refs_1_), channel_id=1, source_target_pairs={{0,4},{1,5},{2,6},{3,7},{4,0},{5,1},{6,2},{7,3},{8,12},{9,13},{10,... | collective-permute-start | bytes 393224 | tf_op jit(solution)/shard_map/ppermute | solution.py:217
  90.2 3.5 %attend.6.refs_1_ = bf16[512,128]{1,0:T(8,128)(2,1)} custom-call(bf16[512,128]{1,0:T(8,128)(2,1)} %get-tuple-element.18.refs_0_, bf16[528,256]{1,0:T(8,128)(2,1)} %copy-done.17, bf16[512,256]{1,0:T(8,128)(2,1)} %get-tuple-element.21.refs_2_.refs_1_, f32[1,1024]{1,0:T(1,128)} %bitcast.32, f32[4,128,640]{2,1,0:T(8,128)} %bias.1.refs_4_), custom_call_target="tpu_custom_call" | custom-call | flops 335544320 | bytes 655360 | tf_op jit(solution)/shard_map/attend/pallas_call | solution.py:193
  93.6 1.5 %collective-permute-start.13 = (bf16[512,128]{1,0:T(8,128)(2,1)}, bf16[512,128]{1,0:T(8,128)(2,1)S(1)}, u32[]{:S(2)}, u32[]{:S(2)}) collective-permute-start(bf16[512,128]{1,0:T(8,128)(2,1)} %attend.6.refs_1_), channel_id=1, source_target_pairs={{0,2},{1,3},{2,4},{3,5},{4,6},{5,7},{6,0},{7,1},{8,10},{9,11},{10,... | collective-permute-start | bytes 393224 | tf_op jit(solution)/shard_map/ppermute | solution.py:217
  95.1 2.4 %collective-permute-start.15 = (bf16[512,128]{1,0:T(8,128)(2,1)}, bf16[512,128]{1,0:T(8,128)(2,1)S(1)}, u32[]{:S(2)}, u32[]{:S(2)}) collective-permute-start(bf16[512,128]{1,0:T(8,128)(2,1)} %attend.6.refs_1_), channel_id=1, source_target_pairs={{0,6},{1,7},{2,0},{3,1},{4,2},{5,3},{6,4},{7,5},{8,14},{9,15},{10,... | collective-permute-start | bytes 393224 | tf_op jit(solution)/shard_map/ppermute | solution.py:217
  97.6 1.7 %collective-permute-start.21 = (bf16[3,512,128]{2,1,0:T(8,128)(2,1)S(1)}, bf16[3,512,128]{2,1,0:T(8,128)(2,1)S(1)}, u32[]{:S(2)}, u32[]{:S(2)}) collective-permute-start(bf16[3,512,128]{2,1,0:T(8,128)(2,1)S(1)} %pad_maximum_fusion.3), channel_id=1, source_target_pairs={{0,1},{1,0},{2,3},{3,2},{4,5},{5,4},{6,7},{7,6},{8,9},{9,8},{10,11... | collective-permute-start | bytes 1179656 | tf_op jit(solution)/shard_map/ppermute | solution.py:217
  99.3 1.4 %collective-permute-done.14.refs_4_ = bf16[512,128]{1,0:T(8,128)(2,1)S(1)} collective-permute-done((bf16[512,128]{1,0:T(8,128)(2,1)}, bf16[512,128]{1,0:T(8,128)(2,1)S(1)}, u32[]{:S(2)}, u32[]{:S(2)}) %collective-permute-start.14) | collective-permute-done | bytes 131104 | tf_op jit(solution)/shard_map/ppermute | solution.py:217
  100.7 1.7 %collective-permute-done.15.refs_5_ = bf16[512,128]{1,0:T(8,128)(2,1)S(1)} collective-permute-done((bf16[512,128]{1,0:T(8,128)(2,1)}, bf16[512,128]{1,0:T(8,128)(2,1)S(1)}, u32[]{:S(2)}, u32[]{:S(2)}) %collective-permute-start.15) | collective-permute-done | bytes 131104 | tf_op jit(solution)/shard_map/ppermute | solution.py:217
  102.5 2.0 %collective-permute-start.16 = (bf16[3,512,128]{2,1,0:T(8,128)(2,1)S(1)}, bf16[3,512,128]{2,1,0:T(8,128)(2,1)S(1)}, u32[]{:S(2)}, u32[]{:S(2)}) collective-permute-start(bf16[3,512,128]{2,1,0:T(8,128)(2,1)S(1)} %pad_maximum_fusion.2), channel_id=1, source_target_pairs={{0,1},{1,0},{2,3},{3,2},{4,5},{5,4},{6,7},{7,6},{8,9},{9,8},{10,11... | collective-permute-start | bytes 1179656 | tf_op jit(solution)/shard_map/ppermute | solution.py:217
  105.0 1.0 collective-permute-done.17.refs_2_
  106.9 2.7 %last.2.refs_9_ = bf16[1024,256]{1,0:T(8,128)(2,1)} custom-call(s32[1]{0:T(128)} %bitcast.refs_0_, bf16[512,128]{1,0:T(8,128)(2,1)} %attend.7.refs_1_, bf16[512,128]{1,0:T(8,128)(2,1)} %copy-done.21, bf16[512,128]{1,0:T(8,128)(2,1)} %copy-done.6, bf16[512,128]{1,0:T(8,128)(2,1)} %copy-done.7, bf16[512,128]{1,0:T(8,128)(2,1)} %copy-done.9, ...), custom_call_target="tpu_custom_call" | custom-call | flops 268435456 | bytes 1572864 | tf_op jit(solution)/shard_map/last/pallas_call | solution.py:355
  110.4 2.7 %last.3 = bf16[1024,256]{1,0:T(8,128)(2,1)} custom-call(s32[1]{0:T(128)} %bitcast.refs_0_, bf16[512,128]{1,0:T(8,128)(2,1)} %attend.6.refs_1_, bf16[512,128]{1,0:T(8,128)(2,1)} %copy-done.20, bf16[512,128]{1,0:T(8,128)(2,1)} %copy-done.8, bf16[512,128]{1,0:T(8,128)(2,1)} %copy-done.10, bf16[512,128]{1,0:T(8,128)(2,1)} %copy-done.11, ...), custom_call_target="tpu_custom_call", output_to_operand_aliasing={{}: (9, {})} | custom-call | flops 268435456 | bytes 1572864 | tf_op jit(solution)/shard_map/last/pallas_call | solution.py:355
  (82 shorter events, 8.7 us)
Async XLA Ops:
  6.5 9.3 %copy-start.22 = (f32[2,2,257]{2,1,0:T(2,128)S(1)}, f32[2,2,257]{2,1,0:T(2,128)}, u32[]{:S(2)}) copy-start(f32[2,2,257]{2,1,0:T(2,128)} %param.15) | copy-start | bytes 12340
  6.5 41.5 %collective-permute-start = (bf16[528,256]{1,0:T(8,128)(2,1)}, bf16[528,256]{1,0:T(8,128)(2,1)S(1)}, u32[]{:S(2)}, u32[]{:S(2)}) collective-permute-start(bf16[528,256]{1,0:T(8,128)(2,1)} %get-tuple-element.16.refs_2_), channel_id=1, source_target_pairs={{0,8},{8,16},{16,24},{24,32},{32,40},{40,48},{48,56},{56,64},{64,7... | collective-permute-start | bytes 811016 | tf_op jit(solution)/shard_map/ppermute | solution.py:388
  22.6 5.4 %collective-permute-start.7 = (bf16[512,128]{1,0:T(8,128)(2,1)}, bf16[512,128]{1,0:T(8,128)(2,1)S(1)}, u32[]{:S(2)}, u32[]{:S(2)}) collective-permute-start(bf16[512,128]{1,0:T(8,128)(2,1)} %attend.5.refs_1_), channel_id=1, source_target_pairs={{0,2},{1,3},{2,4},{3,5},{4,6},{5,7},{6,0},{7,1},{8,10},{9,11},{10,... | collective-permute-start | bytes 393224 | tf_op jit(solution)/shard_map/ppermute | solution.py:217
  24.0 8.1 %collective-permute-start.8 = (bf16[512,128]{1,0:T(8,128)(2,1)}, bf16[512,128]{1,0:T(8,128)(2,1)S(1)}, u32[]{:S(2)}, u32[]{:S(2)}) collective-permute-start(bf16[512,128]{1,0:T(8,128)(2,1)} %attend.5.refs_1_), channel_id=1, source_target_pairs={{0,4},{1,5},{2,6},{3,7},{4,0},{5,1},{6,2},{7,3},{8,12},{9,13},{10,... | collective-permute-start | bytes 393224 | tf_op jit(solution)/shard_map/ppermute | solution.py:217
  26.7 5.4 %collective-permute-start.9 = (bf16[512,128]{1,0:T(8,128)(2,1)}, bf16[512,128]{1,0:T(8,128)(2,1)S(1)}, u32[]{:S(2)}, u32[]{:S(2)}) collective-permute-start(bf16[512,128]{1,0:T(8,128)(2,1)} %attend.5.refs_1_), channel_id=1, source_target_pairs={{0,6},{1,7},{2,0},{3,1},{4,2},{5,3},{6,4},{7,5},{8,14},{9,15},{10,... | collective-permute-start | bytes 393224 | tf_op jit(solution)/shard_map/ppermute | solution.py:217
  28.1 35.3 %copy-start = (bf16[512,128]{1,0:T(8,128)(2,1)}, bf16[512,128]{1,0:T(8,128)(2,1)S(1)}, u32[]{:S(2)}) copy-start(bf16[512,128]{1,0:T(8,128)(2,1)S(1)} %collective-permute-done.7.refs_3_) | copy-start | bytes 393220
  32.1 31.3 %copy-start.1 = (bf16[512,128]{1,0:T(8,128)(2,1)}, bf16[512,128]{1,0:T(8,128)(2,1)S(1)}, u32[]{:S(2)}) copy-start(bf16[512,128]{1,0:T(8,128)(2,1)S(1)} %collective-permute-done.8.refs_4_) | copy-start | bytes 393220
  32.1 31.3 %copy-start.2 = (bf16[512,128]{1,0:T(8,128)(2,1)}, bf16[512,128]{1,0:T(8,128)(2,1)S(1)}, u32[]{:S(2)}) copy-start(bf16[512,128]{1,0:T(8,128)(2,1)S(1)} %collective-permute-done.9.refs_5_) | copy-start | bytes 393220
  32.1 31.2 %collective-permute-start.10 = (bf16[3,512,128]{2,1,0:T(8,128)(2,1)S(1)}, bf16[3,512,128]{2,1,0:T(8,128)(2,1)S(1)}, u32[]{:S(2)}, u32[]{:S(2)}) collective-permute-start(bf16[3,512,128]{2,1,0:T(8,128)(2,1)S(1)} %pad_maximum_fusion.1), channel_id=1, source_target_pairs={{0,1},{1,0},{2,3},{3,2},{4,5},{5,4},{6,7},{7,6},{8,9},{9,8},{10,11... | collective-permute-start | bytes 1179656 | tf_op jit(solution)/shard_map/ppermute | solution.py:217
  52.1 6.4 %collective-permute-start.2 = (bf16[512,128]{1,0:T(8,128)(2,1)}, bf16[512,128]{1,0:T(8,128)(2,1)S(1)}, u32[]{:S(2)}, u32[]{:S(2)}) collective-permute-start(bf16[512,128]{1,0:T(8,128)(2,1)} %attend.4.refs_1_), channel_id=1, source_target_pairs={{0,2},{1,3},{2,4},{3,5},{4,6},{5,7},{6,0},{7,1},{8,10},{9,11},{10,... | collective-permute-start | bytes 393224 | tf_op jit(solution)/shard_map/ppermute | solution.py:217
  52.4 9.5 %collective-permute-start.3 = (bf16[512,128]{1,0:T(8,128)(2,1)}, bf16[512,128]{1,0:T(8,128)(2,1)S(1)}, u32[]{:S(2)}, u32[]{:S(2)}) collective-permute-start(bf16[512,128]{1,0:T(8,128)(2,1)} %attend.4.refs_1_), channel_id=1, source_target_pairs={{0,4},{1,5},{2,6},{3,7},{4,0},{5,1},{6,2},{7,3},{8,12},{9,13},{10,... | collective-permute-start | bytes 393224 | tf_op jit(solution)/shard_map/ppermute | solution.py:217
  55.3 6.6 %collective-permute-start.4 = (bf16[512,128]{1,0:T(8,128)(2,1)}, bf16[512,128]{1,0:T(8,128)(2,1)S(1)}, u32[]{:S(2)}, u32[]{:S(2)}) collective-permute-start(bf16[512,128]{1,0:T(8,128)(2,1)} %attend.4.refs_1_), channel_id=1, source_target_pairs={{0,6},{1,7},{2,0},{3,1},{4,2},{5,3},{6,4},{7,5},{8,14},{9,15},{10,... | collective-permute-start | bytes 393224 | tf_op jit(solution)/shard_map/ppermute | solution.py:217
  55.3 8.0 %collective-permute-start.6 = (bf16[512,128]{1,0:T(8,128)(2,1)}, bf16[512,128]{1,0:T(8,128)(2,1)S(1)}, u32[]{:S(2)}, u32[]{:S(2)}) collective-permute-start(bf16[512,128]{1,0:T(8,128)(2,1)} %attend.5.refs_1_), channel_id=1, source_target_pairs={{0,1},{1,0},{2,3},{3,2},{4,5},{5,4},{6,7},{7,6},{8,9},{9,8},{10,11... | collective-permute-start | bytes 393224 | tf_op jit(solution)/shard_map/ppermute | solution.py:217
  58.5 13.5 %copy-start.3 = (bf16[512,128]{1,0:T(8,128)(2,1)}, bf16[512,128]{1,0:T(8,128)(2,1)S(1)}, u32[]{:S(2)}) copy-start(bf16[512,128]{1,0:T(8,128)(2,1)S(1)} %collective-permute-done.2.refs_3_) | copy-start | bytes 393220
  61.9 10.1 %copy-start.4 = (bf16[512,128]{1,0:T(8,128)(2,1)}, bf16[512,128]{1,0:T(8,128)(2,1)S(1)}, u32[]{:S(2)}) copy-start(bf16[512,128]{1,0:T(8,128)(2,1)S(1)} %collective-permute-done.3.refs_4_) | copy-start | bytes 393220
  61.9 10.1 %copy-start.5 = (bf16[512,128]{1,0:T(8,128)(2,1)}, bf16[512,128]{1,0:T(8,128)(2,1)S(1)}, u32[]{:S(2)}) copy-start(bf16[512,128]{1,0:T(8,128)(2,1)S(1)} %collective-permute-done.4.refs_5_) | copy-start | bytes 393220
  62.0 11.4 %collective-permute-start.5 = (bf16[3,512,128]{2,1,0:T(8,128)(2,1)S(1)}, bf16[3,512,128]{2,1,0:T(8,128)(2,1)S(1)}, u32[]{:S(2)}, u32[]{:S(2)}) collective-permute-start(bf16[3,512,128]{2,1,0:T(8,128)(2,1)S(1)} %pad_maximum_fusion), channel_id=1, source_target_pairs={{0,1},{1,0},{2,3},{3,2},{4,5},{5,4},{6,7},{7,6},{8,9},{9,8},{10,11... | collective-permute-start | bytes 1179656 | tf_op jit(solution)/shard_map/ppermute | solution.py:217
  63.0 10.4 %collective-permute-start.1 = (bf16[512,128]{1,0:T(8,128)(2,1)}, bf16[512,128]{1,0:T(8,128)(2,1)S(1)}, u32[]{:S(2)}, u32[]{:S(2)}) collective-permute-start(bf16[512,128]{1,0:T(8,128)(2,1)} %attend.4.refs_1_), channel_id=1, source_target_pairs={{0,1},{1,0},{2,3},{3,2},{4,5},{5,4},{6,7},{7,6},{8,9},{9,8},{10,11... | collective-permute-start | bytes 393224 | tf_op jit(solution)/shard_map/ppermute | solution.py:217
  72.1 17.4 %collective-permute-start.11 = (bf16[528,256]{1,0:T(8,128)(2,1)}, bf16[528,256]{1,0:T(8,128)(2,1)S(1)}, u32[]{:S(2)}, u32[]{:S(2)}) collective-permute-start(bf16[528,256]{1,0:T(8,128)(2,1)} %get-tuple-element.20.refs_2_), channel_id=1, source_target_pairs={{0,8},{8,16},{16,24},{24,32},{32,40},{40,48},{48,56},{56,64},{64,7... | collective-permute-start | bytes 811016 | tf_op jit(solution)/shard_map/ppermute | solution.py:401
  85.9 9.2 %collective-permute-start.18 = (bf16[512,128]{1,0:T(8,128)(2,1)}, bf16[512,128]{1,0:T(8,128)(2,1)S(1)}, u32[]{:S(2)}, u32[]{:S(2)}) collective-permute-start(bf16[512,128]{1,0:T(8,128)(2,1)} %attend.7.refs_1_), channel_id=1, source_target_pairs={{0,2},{1,3},{2,4},{3,5},{4,6},{5,7},{6,0},{7,1},{8,10},{9,11},{10,... | collective-permute-start | bytes 393224 | tf_op jit(solution)/shard_map/ppermute | solution.py:217
  85.9 11.6 %collective-permute-start.19 = (bf16[512,128]{1,0:T(8,128)(2,1)}, bf16[512,128]{1,0:T(8,128)(2,1)S(1)}, u32[]{:S(2)}, u32[]{:S(2)}) collective-permute-start(bf16[512,128]{1,0:T(8,128)(2,1)} %attend.7.refs_1_), channel_id=1, source_target_pairs={{0,4},{1,5},{2,6},{3,7},{4,0},{5,1},{6,2},{7,3},{8,12},{9,13},{10,... | collective-permute-start | bytes 393224 | tf_op jit(solution)/shard_map/ppermute | solution.py:217
  89.4 8.0 %collective-permute-start.20 = (bf16[512,128]{1,0:T(8,128)(2,1)}, bf16[512,128]{1,0:T(8,128)(2,1)S(1)}, u32[]{:S(2)}, u32[]{:S(2)}) collective-permute-start(bf16[512,128]{1,0:T(8,128)(2,1)} %attend.7.refs_1_), channel_id=1, source_target_pairs={{0,6},{1,7},{2,0},{3,1},{4,2},{5,3},{6,4},{7,5},{8,14},{9,15},{10,... | collective-permute-start | bytes 393224 | tf_op jit(solution)/shard_map/ppermute | solution.py:217
  93.6 5.7 %collective-permute-start.13 = (bf16[512,128]{1,0:T(8,128)(2,1)}, bf16[512,128]{1,0:T(8,128)(2,1)S(1)}, u32[]{:S(2)}, u32[]{:S(2)}) collective-permute-start(bf16[512,128]{1,0:T(8,128)(2,1)} %attend.6.refs_1_), channel_id=1, source_target_pairs={{0,2},{1,3},{2,4},{3,5},{4,6},{5,7},{6,0},{7,1},{8,10},{9,11},{10,... | collective-permute-start | bytes 393224 | tf_op jit(solution)/shard_map/ppermute | solution.py:217
  95.1 5.6 %collective-permute-start.14 = (bf16[512,128]{1,0:T(8,128)(2,1)}, bf16[512,128]{1,0:T(8,128)(2,1)S(1)}, u32[]{:S(2)}, u32[]{:S(2)}) collective-permute-start(bf16[512,128]{1,0:T(8,128)(2,1)} %attend.6.refs_1_), channel_id=1, source_target_pairs={{0,4},{1,5},{2,6},{3,7},{4,0},{5,1},{6,2},{7,3},{8,12},{9,13},{10,... | collective-permute-start | bytes 393224 | tf_op jit(solution)/shard_map/ppermute | solution.py:217
  95.1 11.0 %copy-start.6 = (bf16[512,128]{1,0:T(8,128)(2,1)}, bf16[512,128]{1,0:T(8,128)(2,1)S(1)}, u32[]{:S(2)}) copy-start(bf16[512,128]{1,0:T(8,128)(2,1)S(1)} %collective-permute-done.18.refs_3_) | copy-start | bytes 393220
  95.1 7.4 %collective-permute-start.15 = (bf16[512,128]{1,0:T(8,128)(2,1)}, bf16[512,128]{1,0:T(8,128)(2,1)S(1)}, u32[]{:S(2)}, u32[]{:S(2)}) collective-permute-start(bf16[512,128]{1,0:T(8,128)(2,1)} %attend.6.refs_1_), channel_id=1, source_target_pairs={{0,6},{1,7},{2,0},{3,1},{4,2},{5,3},{6,4},{7,5},{8,14},{9,15},{10,... | collective-permute-start | bytes 393224 | tf_op jit(solution)/shard_map/ppermute | solution.py:217
  97.6 8.5 %collective-permute-start.21 = (bf16[3,512,128]{2,1,0:T(8,128)(2,1)S(1)}, bf16[3,512,128]{2,1,0:T(8,128)(2,1)S(1)}, u32[]{:S(2)}, u32[]{:S(2)}) collective-permute-start(bf16[3,512,128]{2,1,0:T(8,128)(2,1)S(1)} %pad_maximum_fusion.3), channel_id=1, source_target_pairs={{0,1},{1,0},{2,3},{3,2},{4,5},{5,4},{6,7},{7,6},{8,9},{9,8},{10,11... | collective-permute-start | bytes 1179656 | tf_op jit(solution)/shard_map/ppermute | solution.py:217
  99.3 10.3 %copy-start.8 = (bf16[512,128]{1,0:T(8,128)(2,1)}, bf16[512,128]{1,0:T(8,128)(2,1)S(1)}, u32[]{:S(2)}) copy-start(bf16[512,128]{1,0:T(8,128)(2,1)S(1)} %collective-permute-done.13.refs_3_) | copy-start | bytes 393220
  100.7 8.9 %copy-start.10 = (bf16[512,128]{1,0:T(8,128)(2,1)}, bf16[512,128]{1,0:T(8,128)(2,1)S(1)}, u32[]{:S(2)}) copy-start(bf16[512,128]{1,0:T(8,128)(2,1)S(1)} %collective-permute-done.14.refs_4_) | copy-start | bytes 393220
  102.5 7.1 %collective-permute-start.16 = (bf16[3,512,128]{2,1,0:T(8,128)(2,1)S(1)}, bf16[3,512,128]{2,1,0:T(8,128)(2,1)S(1)}, u32[]{:S(2)}, u32[]{:S(2)}) collective-permute-start(bf16[3,512,128]{2,1,0:T(8,128)(2,1)S(1)} %pad_maximum_fusion.2), channel_id=1, source_target_pairs={{0,1},{1,0},{2,3},{3,2},{4,5},{5,4},{6,7},{7,6},{8,9},{9,8},{10,11... | collective-permute-start | bytes 1179656 | tf_op jit(solution)/shard_map/ppermute | solution.py:217
  104.5 1.6 %collective-permute-start.17 = (bf16[512,128]{1,0:T(8,128)(2,1)}, bf16[512,128]{1,0:T(8,128)(2,1)S(1)}, u32[]{:S(2)}, u32[]{:S(2)}) collective-permute-start(bf16[512,128]{1,0:T(8,128)(2,1)} %attend.7.refs_1_), channel_id=1, source_target_pairs={{0,1},{1,0},{2,3},{3,2},{4,5},{5,4},{6,7},{7,6},{8,9},{9,8},{10,11... | collective-permute-start | bytes 393224 | tf_op jit(solution)/shard_map/ppermute | solution.py:217
  104.7 4.9 %collective-permute-start.12 = (bf16[512,128]{1,0:T(8,128)(2,1)}, bf16[512,128]{1,0:T(8,128)(2,1)S(1)}, u32[]{:S(2)}, u32[]{:S(2)}) collective-permute-start(bf16[512,128]{1,0:T(8,128)(2,1)} %attend.6.refs_1_), channel_id=1, source_target_pairs={{0,1},{1,0},{2,3},{3,2},{4,5},{5,4},{6,7},{7,6},{8,9},{9,8},{10,11... | collective-permute-start | bytes 393224 | tf_op jit(solution)/shard_map/ppermute | solution.py:217
  (13 other events, 31.5 us)
where the time goes:
time: 114 us; the launch traced here: 113 us
  Pallas kernels  44.8 us (39%)
  starting transfers between devices  44.5 us (39%)
  waiting for transfers between devices  14.6 us (13%)
  local copies, waits for them, and re-layouts  7.48 us (7%)
  other arithmetic  1.47 us (1%)
    ppermute x20, starting transfers between devices, moved(): lax.ppermute(array, 'tp', [(2 * x + core, 2 * ((x + by) % chips) + (1 - c...  37.7 us
    pallas_call x2, Pallas kernels, next_heads(): pl.pallas_call(functools.partial(next_kernel, q_scale, block_rows, len(bl...  15.5 us
    ppermute x20, waiting for transfers between devices, moved(): lax.ppermute(array, 'tp', [(2 * x + core, 2 * ((x + by) % chips) + (1 - c...  14.6 us
    pallas_call x4, Pallas kernels, attention(): pl.pallas_call(functools.partial(attention_kernel, head_width, from_far),...  13.8 us
    pallas_call x2, Pallas kernels, heads(): pl.pallas_call(functools.partial(heads_kernel, q_scale, block_rows), grid...  7.78 us
    ppermute x2, starting transfers between devices, shards(): far = lax.ppermute(kv_late, 'sp', onward)  6.72 us
    pallas_call x2, Pallas kernels, last_update(): pl.pallas_call(functools.partial(last_kernel, len(blocks)), grid_spec=plt...  5.42 us
    unnamed x46, local copies, waits for them, and re-layouts  5.08 us
  transfers between devices with their start and end apart: 22, of which 8 were waited for; matrix products, arithmetic and copies ran while one was open for 1% of the time, Pallas kernels for 34%

commit v1 on v0

v1 whole, which is shorter than its diff:
```python
import functools

import jax
import jax.numpy as jnp
from jax import lax
from jax.experimental import pallas as pl
from jax.experimental.pallas import tpu as pltpu
from jax.sharding import PartitionSpec as P

SEG = 64
PREV_SEGS = 8
MAX_REL = 128
LAYERS = 2
REACH = PREV_SEGS * SEG
QUERY_ROWS = 2 * SEG
BAND = REACH + QUERY_ROWS
NEG = -1e30
EPS = 1e-06
LOG2E = 1.4426950408889634
DOC_ROWS = 16
VMEM_LIMIT = 24 * 2**20
FIRST_VMEM_LIMIT = 51 * 2**20

F32 = jnp.float32
BF16 = jnp.bfloat16


def cost(flops, bytes_accessed, transcendentals=0):
    return pl.CostEstimate(
        flops=flops, bytes_accessed=bytes_accessed, transcendentals=transcendentals
    )


def project_heads(rows, gain, wq, wk, wv, q_scale):
    rows32 = rows.astype(F32)
    inv = lax.rsqrt(jnp.mean(rows32 * rows32, axis=-1, keepdims=True) + EPS)
    scaled = rows * gain
    queries = jnp.dot(scaled, wq, preferred_element_type=F32) * (inv * q_scale)
    wkv = jnp.concatenate([wk, wv], axis=1)
    kv = jnp.dot(scaled, wkv, preferred_element_type=F32) * inv
    return queries.astype(BF16), kv.astype(BF16)


def doc_rows(docs, width):
    parts = [docs[:, i : i + width] for i in range(0, docs.shape[1], width)]
    pad = jnp.zeros((DOC_ROWS - len(parts), width), F32)
    return jnp.concatenate(parts + [pad], axis=0).astype(BF16)


def heads_kernel(q_scale, block_rows, *refs):
    x_hbm, gain_hbm, *w_hbm, docs_hbm, table_hbm = refs[:7]
    q_ref, early_ref, late_ref, docs_ref, near_ref, gain_ref, *next_refs = refs[7:16]
    x_ref, *w_refs, ids_ref, table_ref, x_sem, w_sem, next_sem, side_sem = refs[16:]
    row_count = x_ref.shape[0]
    half_rows = row_count // 2
    order = [*range(half_rows, row_count, block_rows), *range(0, half_rows, block_rows)]
    side_copies = [
        pltpu.make_async_copy(source, target, side_sem.at[i])
        for i, (source, target) in enumerate(
            [(docs_hbm, ids_ref), (table_hbm, table_ref), (gain_hbm, gain_ref)]
        )
    ]
    w_copies = [
        pltpu.make_async_copy(w.at[0], w_ref, w_sem.at[i])
        for i, (w, w_ref) in enumerate(zip(w_hbm, w_refs))
    ]
    next_copies = [
        pltpu.make_async_copy(w.at[1], next_ref, next_sem.at[i])
        for i, (w, next_ref) in enumerate(zip(w_hbm, next_refs))
    ]
    x_copies = [
        pltpu.make_async_copy(
            x_hbm.at[pl.ds(row, block_rows)], x_ref.at[pl.ds(row, block_rows)], x_sem.at[i]
        )
        for i, row in enumerate(order)
    ]
    for copy in (*side_copies, x_copies[0], *w_copies, *x_copies[1:], *next_copies):
        copy.start()
    for copy in side_copies:
        copy.wait()
    near_bias(table_ref, near_ref)
    docs = (ids_ref[...] + 1).astype(F32)[None, :]
    docs_ref[...] = docs
    width = late_ref.shape[1]
    late_ref[half_rows:, :] = doc_rows(docs[:, half_rows:], width)
    for copy in w_copies:
        copy.wait()
    for copy, row in zip(x_copies, order):
        copy.wait()
        queries, kv = project_heads(
            x_ref[pl.ds(row, block_rows), :],
            gain_ref[0:1, :],
            *[w_ref[...] for w_ref in w_refs],
            q_scale,
        )
        q_ref[pl.ds(row, block_rows), :] = queries
        if row < half_rows:
            early_ref[pl.ds(row, block_rows), :] = kv
        else:
            late_ref[pl.ds(row - half_rows, block_rows), :] = kv
    for copy in next_copies:
        copy.wait()


def whole(count):
    return [pl.BlockSpec(memory_space=pltpu.VMEM)] * count


def heads(tokens, gains, wq, wk, wv, doc_ids, rel_table, q_scale, block_rows=256):
    row_count = tokens.shape[0]
    half_rows = row_count // 2
    depth, width = wq.shape[1:]
    items = rel_table.shape[0] * rel_table.shape[1]
    hbm = pl.BlockSpec(memory_space=pl.ANY)
    return pl.pallas_call(
        functools.partial(heads_kernel, q_scale, block_rows),
        in_specs=[hbm] * 7,
        out_specs=whole(9),
        out_shape=[
            jax.ShapeDtypeStruct((row_count, width), BF16),
            jax.ShapeDtypeStruct((half_rows, 2 * width), BF16),
            jax.ShapeDtypeStruct((half_rows + DOC_ROWS, 2 * width), BF16),
            jax.ShapeDtypeStruct((1, row_count), F32),
            jax.ShapeDtypeStruct((items, QUERY_ROWS, 2 * MAX_REL), F32),
            jax.ShapeDtypeStruct(gains.shape, BF16),
            *[jax.ShapeDtypeStruct((depth, width), BF16) for _ in range(3)],
        ],
        scratch_shapes=[
            pltpu.VMEM((row_count, depth), BF16),
            *[pltpu.VMEM((depth, width), BF16) for _ in range(3)],
            pltpu.VMEM(doc_ids.shape, doc_ids.dtype),
            pltpu.VMEM(rel_table.shape, F32),
            pltpu.SemaphoreType.DMA((row_count // block_rows,)),
            *[pltpu.SemaphoreType.DMA((3,)) for _ in range(3)],
        ],
        cost_estimate=cost(6 * row_count * depth * width, 2 * depth * (row_count + 3 * width)),
        compiler_params=pltpu.CompilerParams(vmem_limit_bytes=FIRST_VMEM_LIMIT),
        name="heads",
    )(tokens, gains, wq, wk, wv, doc_ids, rel_table)


def near_bias(table_ref, out_ref):
    layers, head_count, table_width = table_ref.shape
    near = 2 * MAX_REL
    width = near + QUERY_ROWS
    index = lax.broadcasted_iota(jnp.int32, (table_width, width), 0)
    place_of = lax.broadcasted_iota(jnp.int32, (table_width, width), 1)
    wanted = jnp.where(place_of < near, near - place_of, near)
    picked = (index == wanted).astype(F32)
    row = lax.broadcasted_iota(jnp.int32, (QUERY_ROWS, near), 0)
    col = lax.broadcasted_iota(jnp.int32, (QUERY_ROWS, near), 1)
    seen = jnp.logical_or(row >= SEG, col < near - SEG)
    for layer in range(layers):
        table = table_ref[layer]
        lines = jnp.dot(
            table, picked, precision=lax.Precision.HIGHEST, preferred_element_type=F32
        )
        lines = (lines - lines[:, near : near + 1]) * LOG2E
        for head in range(head_count):
            spread = jnp.broadcast_to(lines[head : head + 1, :], (QUERY_ROWS, width))
            rolled = pltpu.roll(spread, 0, 1, stride=1, stride_axis=0)
            out_ref[layer * head_count + head] = jnp.where(seen, rolled[:, :near], NEG)


def attention_kernel(head_width, layer, from_far, *refs):
    q_ref, lo_ref, hi_ref, docs_ref, bias_ref, out_ref = (*refs[:5], refs[-1])
    half_rows, width = out_ref.shape
    first_query = 0 if from_far else q_ref.shape[0] - half_rows
    if from_far:
        docs_rows = lo_ref[-DOC_ROWS:, :].astype(F32)
        parts = half_rows // docs_rows.shape[1]
        docs_lo = jnp.concatenate([docs_rows[i : i + 1] for i in range(parts)], axis=1)
        docs_hi = docs_ref[:, :half_rows]
    else:
        docs_lo = docs_ref[:, :half_rows]
        docs_hi = docs_ref[:, half_rows:]
    head_count = width // head_width
    lane = lax.broadcasted_iota(jnp.int32, (QUERY_ROWS, width), 1) // head_width
    square = (QUERY_ROWS, QUERY_ROWS)
    diagonal = lax.broadcasted_iota(jnp.int32, square, 0) == lax.broadcasted_iota(
        jnp.int32, square, 1
    )
    seen = jnp.logical_or(
        lax.broadcasted_iota(jnp.int32, square, 0) < SEG,
        lax.broadcasted_iota(jnp.int32, square, 1) >= SEG,
    )
    ones = jnp.ones((BAND, width), BF16)
    chunks = BAND // QUERY_ROWS
    plain = chunks - bias_ref.shape[2] // QUERY_ROWS
    first_head = layer * head_count
    for block in range(half_rows // QUERY_ROWS):
        start = block * QUERY_ROWS
        stop = start + QUERY_ROWS
        kv = jnp.concatenate([lo_ref[start:half_rows, :], hi_ref[:stop, :]], axis=0)
        docs_keys = jnp.concatenate([docs_lo[:, start:], docs_hi[:, :stop]], axis=1)
        docs_queries = jnp.sum(
            jnp.where(diagonal, docs_hi[:, start:stop], 0.0), axis=1, keepdims=True
        )
        same = []
        for c in range(chunks):
            keys = docs_keys[:, c * QUERY_ROWS : (c + 1) * QUERY_ROWS]
            if c == 0:
                keys = jnp.where(seen, keys, -1.0)
            same.append(keys == docs_queries)
        queries = q_ref[first_query + start : first_query + stop, :]
        zero = jnp.zeros_like(queries)
        stacked = jnp.concatenate(
            [jnp.where(lane == head, queries, zero) for head in range(head_count)], axis=0
        )
        scores = lax.dot_general(
            stacked, kv[:, :width], (((1,), (1,)), ((), ())), preferred_element_type=F32
        )
        weights = []
        for head in range(head_count):
            parts = []
            for c in range(chunks):
                part = scores[
                    head * QUERY_ROWS : (head + 1) * QUERY_ROWS,
                    c * QUERY_ROWS : (c + 1) * QUERY_ROWS,
                ]
                if c >= plain:
                    near = (c - plain) * QUERY_ROWS
                    part = part + bias_ref[first_head + head, :, near : near + QUERY_ROWS]
                parts.append(jnp.where(same[c], part, NEG))
            top = jnp.max(functools.reduce(jnp.maximum, parts), axis=1, keepdims=True)
            weights.append(
                jnp.concatenate([jnp.exp2(part - top).astype(BF16) for part in parts], axis=1)
            )
        weights = jnp.concatenate(weights, axis=0)
        summed = jnp.dot(
            weights,
            jnp.concatenate([kv[:, width:], ones], axis=1),
            preferred_element_type=F32,
        )
        result = summed[:, :width] / summed[:, width:]
        mine = result[:QUERY_ROWS]
        for head in range(1, head_count):
            mine = jnp.where(lane == head, result[head * QUERY_ROWS : (head + 1) * QUERY_ROWS], mine)
        out_ref[start:stop, :] = mine.astype(BF16)


def attention(queries, lo, hi, docs, biases, layer, head_width, from_far, ahead=()):
    half_rows = docs.shape[1] // 2
    width = queries.shape[1]
    return pl.pallas_call(
        functools.partial(attention_kernel, head_width, layer, from_far),
        in_specs=whole(5 + len(ahead)),
        out_specs=pl.BlockSpec(memory_space=pltpu.VMEM),
        out_shape=jax.ShapeDtypeStruct((half_rows, width), BF16),
        cost_estimate=cost(8 * half_rows * BAND * width, 8 * half_rows * width, half_rows * BAND * 2),
        compiler_params=pltpu.CompilerParams(vmem_limit_bytes=VMEM_LIMIT),
        name="attend",
    )(queries, lo, hi, docs, biases, *ahead)


def gather(block):
    chips = lax.axis_size("tp") // 2
    pairs = [(x, core) for x in range(chips) for core in range(2)]

    def moved(array, by, other=False):
        return lax.ppermute(
            array,
            "tp",
            [
                (2 * x + core, 2 * ((x + by) % chips) + (1 - core if other else core))
                for x, core in pairs
            ],
        )

    return moved, [block, *[moved(block, by) for by in range(1, chips)]]


def stack_kernel(*refs):
    out_ref = refs[-1]
    for i in range(out_ref.shape[0]):
        out_ref[i] = refs[i][...]


def from_partner(moved, blocks, after):
    stacked = pl.pallas_call(
        stack_kernel,
        in_specs=[*whole(len(blocks)), pl.BlockSpec(memory_space=pl.ANY)],
        out_specs=pl.BlockSpec(memory_space=pltpu.VMEM),
        out_shape=jax.ShapeDtypeStruct((len(blocks), *blocks[0].shape), BF16),
        compiler_params=pltpu.CompilerParams(vmem_limit_bytes=VMEM_LIMIT),
        name="stack",
    )(*blocks, after)
    return [*blocks, moved(stacked, 0, True)]


def slots_of(me, chips):
    x, core = me // 2, me % 2
    others = [(x + chips - by) % chips for by in range(1, chips)]
    return [
        2 * x + core,
        *[2 * other + core for other in others],
        2 * x + 1 - core,
        *[2 * other + 1 - core for other in others],
    ]


def place(me, block_refs, slots_ref):
    chips = slots_ref.shape[0] // 2
    arrays = [ref[...] for ref in block_refs[:-1]]
    arrays += [block_refs[-1][i] for i in range(chips)]
    for slot, array in zip(slots_of(me, chips), arrays):
        slots_ref[slot] = array


def rows_of(slots_ref, start, count):
    parts = [slots_ref[i, start : start + count, :] for i in range(slots_ref.shape[0])]
    return jnp.concatenate(parts, axis=1)


def next_kernel(q_scale, block_rows, gathered_count, half, *refs):
    me = lax.axis_index("tp")
    block_refs, refs = refs[:gathered_count], refs[gathered_count:]
    x_ref, w_ref, gain_ref, wq_ref, wk_ref, wv_ref, docs_ref, *rest = refs
    q_ref, kv_ref, own_ref, slots_ref, cols_ref = rest
    place(me, block_refs, slots_ref)
    half_rows, col_width = own_ref.shape
    first_row = half * half_rows
    if half == 1:
        kv_ref[half_rows:, :] = doc_rows(docs_ref[:, half_rows:], kv_ref.shape[1])
    for start in range(0, half_rows, block_rows):
        block = slice(start, start + block_rows)
        attended = rows_of(slots_ref, start, block_rows)
        update = jnp.dot(attended, w_ref[...], preferred_element_type=F32)
        rows = x_ref[first_row + start : first_row + start + block_rows, :]
        hidden = (rows.astype(F32) + update).astype(BF16)
        for part in range(cols_ref.shape[0]):
            cols_ref[part, block, :] = hidden[:, part * col_width : (part + 1) * col_width]
        queries, kv = project_heads(
            hidden, gain_ref[1:2, :], wq_ref[...], wk_ref[...], wv_ref[...], q_scale
        )
        q_ref[block, :] = queries
        kv_ref[block, :] = kv
    own_ref[...] = cols_ref[me]


def next_heads(blocks, tokens, w_out, gains, wq, wk, wv, docs, half, q_scale, block_rows=256):
    half_rows, block_width = blocks[0].shape
    depth, width = wq.shape
    inner = w_out.shape[0]
    members = inner // block_width
    col_width = depth // members
    args = [*blocks, tokens, w_out, gains, wq, wk, wv, docs]
    return pl.pallas_call(
        functools.partial(next_kernel, q_scale, block_rows, len(blocks), half),
        in_specs=whole(len(args)),
        out_specs=whole(3),
        out_shape=[
            jax.ShapeDtypeStruct((half_rows, width), BF16),
            jax.ShapeDtypeStruct((half_rows + half * DOC_ROWS, 2 * width), BF16),
            jax.ShapeDtypeStruct((half_rows, col_width), BF16),
        ],
        scratch_shapes=[
            pltpu.VMEM((members, half_rows, block_width), BF16),
            pltpu.VMEM((members, half_rows, col_width), BF16),
        ],
        cost_estimate=cost(
            2 * half_rows * depth * (inner + 3 * width),
            2 * depth * (half_rows + 3 * width + inner),
        ),
        compiler_params=pltpu.CompilerParams(vmem_limit_bytes=VMEM_LIMIT),
        name="next_heads",
    )(*args)


def last_kernel(gathered_count, *refs):
    block_refs, refs = refs[:gathered_count], refs[gathered_count:]
    own_ref, w_ref, out_ref, slots_ref = refs[0], refs[1], refs[-2], refs[-1]
    place(lax.axis_index("tp"), block_refs, slots_ref)
    half_rows = own_ref.shape[0]
    attended = rows_of(slots_ref, 0, half_rows)
    update = jnp.dot(attended, w_ref[...], preferred_element_type=F32)
    out_ref[:half_rows, :] = (own_ref[...].astype(F32) + update).astype(BF16)
    if len(refs) == 5:
        out_ref[half_rows:, :] = refs[2][...]


def last_update(blocks, own, w_out, below=()):
    half_rows, block_width = blocks[0].shape
    inner, col_width = w_out.shape
    args = [*blocks, own, w_out, *below]
    rows = half_rows + sum(array.shape[0] for array in below)
    return pl.pallas_call(
        functools.partial(last_kernel, len(blocks)),
        in_specs=whole(len(args)),
        out_specs=pl.BlockSpec(memory_space=pltpu.VMEM),
        scratch_shapes=[pltpu.VMEM((inner // block_width, half_rows, block_width), BF16)],
        out_shape=jax.ShapeDtypeStruct((rows, col_width), BF16),
        cost_estimate=cost(
            2 * half_rows * inner * col_width, 2 * inner * (half_rows + col_width)
        ),
        compiler_params=pltpu.CompilerParams(vmem_limit_bytes=VMEM_LIMIT),
        name="last",
    )(*args)


def shards(tokens, doc_ids, gains, w_query, w_key, w_value, rel_table, out_first, out_last):
    row_count = tokens.shape[0]
    half_rows = row_count // 2
    head_count = rel_table.shape[1]
    width = w_query.shape[2]
    head_width = width // head_count
    q_scale = head_width ** (-0.5) * LOG2E
    members = lax.axis_size("sp")
    onward = [(i, i + 1) for i in range(members - 1)]

    queries, kv_early, kv_late, docs, biases, *weights = heads(
        tokens, gains, w_query, w_key, w_value, doc_ids, rel_table, q_scale
    )
    q_late = q_early = queries
    far = lax.ppermute(kv_late, "sp", onward)
    result = None
    for layer in range(LAYERS):
        late = attention(q_late, kv_early, kv_late, docs, biases, layer, head_width, False)
        moved, late = gather(late)
        ahead = (tokens, out_first) if layer == 0 else (out_last,)
        early = attention(q_early, far, kv_early, docs, biases, layer, head_width, True, ahead)
        late = from_partner(moved, late, early)
        moved, early = gather(early)
        if layer == 0:
            q_late, kv_late, own_late = next_heads(
                late, tokens, out_first, *weights, docs, 1, q_scale
            )
            far = lax.ppermute(kv_late, "sp", onward)
            early = from_partner(moved, early, kv_late)
            q_early, kv_early, own_early = next_heads(
                early, tokens, out_first, *weights, docs, 0, q_scale
            )
        else:
            below = last_update(late, own_late, out_last)
            early = from_partner(moved, early, below)
            result = last_update(early, own_early, out_last, (below,))
    return result


def solution(mesh):
    placed = (
        P(("grp", "sp"), None),
        P(("grp", "sp")),
        P(),
        P(None, None, "tp"),
        P(None, None, "tp"),
        P(None, None, "tp"),
        P(None, "tp", None),
        P(),
        P(None, "tp"),
    )
    return jax.shard_map(
        shards, mesh=mesh, in_specs=placed, out_specs=P(("grp", "sp"), "tp"), check_vma=False
    )
```

time: 114 us -> 83.3 us (0.73)
  Pallas kernels: 44.8 us -> 20.9 us
  local copies, waits for them, and re-layouts: 7.48 us -> 3.18 us
  starting transfers between devices: 44.5 us -> 41.6 us
  waiting for transfers between devices: 14.6 us -> 17.2 us
  other arithmetic: 1.47 us -> 0 us
    pallas_call x9 -> x11, Pallas kernels: 29.3 us -> 13.6 us  [the longest x4 6.06 us: attention(): pl.pallas_call(functools.partial(attention_kernel, head_width, layer, fro...]
    pallas_call x2, Pallas kernels: 15.5 us -> 7.3 us  [next_heads(): pl.pallas_call(functools.partial(next_kernel, q_scale, block_rows, len(bl...]
    ppermute x20 -> x16, starting transfers between devices: 37.7 us -> 35.1 us  [moved(): lax.ppermute(array, 'tp', [(2 * x + core, 2 * ((x + by) % chips) + (1 - c...]
    ppermute x20 -> x16, waiting for transfers between devices: 14.6 us -> 17.2 us  [moved(): lax.ppermute(array, 'tp', [(2 * x + core, 2 * ((x + by) % chips) + (1 - c...]
    unnamed x46 -> x12, local copies, waits for them, and re-layouts: 5.08 us -> 3.18 us
    broadcast_in_dim x3 -> x0, local copies, waits for them, and re-layouts: 1.44 us -> none  [the longest x1 1.3 us: shards(): gains = gains[:, None, :]]
    convert_element_type x1 -> x0, other arithmetic: 1.27 us -> none  [shards(): docs = (doc_ids + 1).astype(F32).reshape(1, row_count)]
  transfers between devices with their start and end apart: 22 -> 18, of which waited for: 8 -> 8; matrix products, arithmetic and copies ran while one was open for 1% -> 0% of each run, Pallas kernels for 34% -> 17%
where the time goes in v1:
time: 83.3 us; the launch traced here: 83.1 us
  starting transfers between devices  41.6 us (50%)
  Pallas kernels  20.9 us (25%)
  waiting for transfers between devices  17.2 us (21%)
  local copies, waits for them, and re-layouts  3.18 us (4%)
    ppermute x16, starting transfers between devices, moved(): lax.ppermute(array, 'tp', [(2 * x + core, 2 * ((x + by) % chips) + (1 - c...  35.1 us
    ppermute x16, waiting for transfers between devices, moved(): lax.ppermute(array, 'tp', [(2 * x + core, 2 * ((x + by) % chips) + (1 - c...  17.2 us
    pallas_call x2, Pallas kernels, next_heads(): pl.pallas_call(functools.partial(next_kernel, q_scale, block_rows, len(bl...  7.3 us
    ppermute x2, starting transfers between devices, shards(): far = lax.ppermute(kv_late, 'sp', onward)  6.58 us
    pallas_call x4, Pallas kernels, attention(): pl.pallas_call(functools.partial(attention_kernel, head_width, layer, fro...  6.06 us
    pallas_call x1, Pallas kernels, heads(): pl.pallas_call(functools.partial(heads_kernel, q_scale, block_rows), in_s...  5.6 us
    unnamed x12, local copies, waits for them, and re-layouts  3.18 us
    pallas_call x2, Pallas kernels, last_update(): pl.pallas_call(functools.partial(last_kernel, len(blocks)), in_specs=whol...  1.79 us
  transfers between devices with their start and end apart: 18, of which 8 were waited for; matrix products, arithmetic and copies ran while one was open for 0% of the time, Pallas kernels for 17%

profile of v1, /device:TPU:33, one launch (start us, length us, event | category | flops | bytes accessed | tf_op | source)
XLA Modules:
  0.0 83.1 jit_solution(5026302117381729737)
XLA Ops:
  0.0 0.8 %copy-done.3 = bf16[2,2048]{1,0:T(2,128)(2,1)S(1)} copy-done((bf16[2,2048]{1,0:T(2,128)(2,1)S(1)}, bf16[2,2048]{1,0:T(2,128)(2,1)}, u32[]{:S(2)}) %copy-start.3) | copy-done | bytes 8216
  0.9 1.1 %copy-done.4 = f32[2,2,257]{2,1,0:T(2,128)S(1)} copy-done((f32[2,2,257]{2,1,0:T(2,128)S(1)}, f32[2,2,257]{2,1,0:T(2,128)}, u32[]{:S(2)}) %copy-start.4) | copy-done | bytes 4136
  2.0 1.2 %copy-done.5 = s32[1024]{0:T(1024)S(1)} copy-done((s32[1024]{0:T(1024)S(1)}, s32[1024]{0:T(1024)}, u32[]{:S(2)}) %copy-start.5) | copy-done | bytes 4120
  3.2 5.6 %heads.1 = (bf16[1024,128]{1,0:T(8,128)(2,1)S(1)}, bf16[512,256]{1,0:T(8,128)(2,1)S(1)}, bf16[528,256]{1,0:T(8,128)(2,1)S(1)}, f32[1,1024]{1,0:T(1,128)S(1)}, f3...) custom-call(bf16[1024,2048]{1,0:T(8,128)(2,1)} %refs_5_.8, ...), custom_call_target="tpu_custom_call" | custom-call | flops 1610612736 | bytes 5767168 | tf_op jit(solution)/shard_map/heads/pallas_call | solution.py:115
  8.8 5.3 %collective-permute-start = (bf16[528,256]{1,0:T(8,128)(2,1)S(1)}, bf16[528,256]{1,0:T(8,128)(2,1)S(1)}, u32[]{:S(2)}, u32[]{:S(2)}) collective-permute-start(bf16[528,256]{1,0:T(8,128)(2,1)S(1)} %get-tuple-element.21.refs_2_), channel_id=1, source_target_pairs={{0,8},{8,16},{16,24},{24,32},{32,40},{40,48},{48,56},{56,64},{64,7... | collective-permute-start | bytes 811016 | tf_op jit(solution)/shard_map/ppermute | solution.py:415
  14.1 1.5 %attend.5.refs_0_ = bf16[512,128]{1,0:T(8,128)(2,1)S(1)} custom-call(bf16[1024,128]{1,0:T(8,128)(2,1)S(1)} %get-tuple-element.20.refs_0_, bf16[512,256]{1,0:T(8,128)(2,1)S(1)} %get-tuple-element.22.refs_2_.refs_1_, bf16[528,256]{1,0:T(8,128)(2,1)S(1)} %get-tuple-element.21.refs_2_, f32[1,1024]{1,0:T(1,128)S(1)} %get-tuple-element.23.refs_3_.refs_11_, ...), custom_call_target="tpu_custom_call" | custom-call | flops 335544320 | bytes 524288 | tf_op jit(solution)/shard_map/attend/pallas_call | solution.py:245
  15.6 1.5 %collective-permute-start.4 = (bf16[512,128]{1,0:T(8,128)(2,1)S(1)}, bf16[512,128]{1,0:T(8,128)(2,1)S(1)}, u32[]{:S(2)}, u32[]{:S(2)}) collective-permute-start(bf16[512,128]{1,0:T(8,128)(2,1)S(1)} %attend.5.refs_0_), channel_id=1, source_target_pairs={{0,2},{1,3},{2,4},{3,5},{4,6},{5,7},{6,0},{7,1},{8,10},{9,11},{10,... | collective-permute-start | bytes 393224 | tf_op jit(solution)/shard_map/ppermute | solution.py:261
  17.0 2.7 %collective-permute-start.5 = (bf16[512,128]{1,0:T(8,128)(2,1)S(1)}, bf16[512,128]{1,0:T(8,128)(2,1)S(1)}, u32[]{:S(2)}, u32[]{:S(2)}) collective-permute-start(bf16[512,128]{1,0:T(8,128)(2,1)S(1)} %attend.5.refs_0_), channel_id=1, source_target_pairs={{0,4},{1,5},{2,6},{3,7},{4,0},{5,1},{6,2},{7,3},{8,12},{9,13},{10,... | collective-permute-start | bytes 393224 | tf_op jit(solution)/shard_map/ppermute | solution.py:261
  19.8 1.0 %collective-permute-start.6 = (bf16[512,128]{1,0:T(8,128)(2,1)S(1)}, bf16[512,128]{1,0:T(8,128)(2,1)S(1)}, u32[]{:S(2)}, u32[]{:S(2)}) collective-permute-start(bf16[512,128]{1,0:T(8,128)(2,1)S(1)} %attend.5.refs_0_), channel_id=1, source_target_pairs={{0,6},{1,7},{2,0},{3,1},{4,2},{5,3},{6,4},{7,5},{8,14},{9,15},{10,... | collective-permute-start | bytes 393224 | tf_op jit(solution)/shard_map/ppermute | solution.py:261
  20.8 1.5 %attend.4.refs_4_.refs_0_ = bf16[512,128]{1,0:T(8,128)(2,1)S(1)} custom-call(bf16[1024,128]{1,0:T(8,128)(2,1)S(1)} %get-tuple-element.20.refs_0_, bf16[528,256]{1,0:T(8,128)(2,1)S(1)} %collective-permute-done.refs_1_, bf16[512,256]{1,0:T(8,128)(2,1)S(1)} %get-tuple-element.22.refs_2_.refs_1_, f32[1,1024]{1,0:T(1,128)S(1)} %get-tuple-element.23.refs_3_.refs_11_, ...), custom_call_target="tpu_custom_call" | custom-call | flops 335544320 | bytes 524288 | tf_op jit(solution)/shard_map/attend/pallas_call | solution.py:245
  22.3 2.6 %collective-permute-done.5.refs_2_ = bf16[512,128]{1,0:T(8,128)(2,1)S(1)} collective-permute-done((bf16[512,128]{1,0:T(8,128)(2,1)S(1)}, bf16[512,128]{1,0:T(8,128)(2,1)S(1)}, u32[]{:S(2)}, u32[]{:S(2)}) %collective-permute-start.5) | collective-permute-done | bytes 131104 | tf_op jit(solution)/shard_map/ppermute | solution.py:261
  25.0 15.8 %collective-permute-start.7 = (bf16[4,512,128]{2,1,0:T(8,128)(2,1)S(1)}, bf16[4,512,128]{2,1,0:T(8,128)(2,1)S(1)}, u32[]{:S(2)}, u32[]{:S(2)}) collective-permute-start(bf16[4,512,128]{2,1,0:T(8,128)(2,1)S(1)} %stack.4), channel_id=1, source_target_pairs={{0,1},{1,0},{2,3},{3,2},{4,5},{5,4},{6,7},{7,6},{8,9},{9,8},{10,11... | collective-permute-start | bytes 1572872 | tf_op jit(solution)/shard_map/ppermute | solution.py:261
  40.8 0.3 collective-permute-start.1
  41.1 2.9 %collective-permute-start.2 = (bf16[512,128]{1,0:T(8,128)(2,1)S(1)}, bf16[512,128]{1,0:T(8,128)(2,1)S(1)}, u32[]{:S(2)}, u32[]{:S(2)}) collective-permute-start(bf16[512,128]{1,0:T(8,128)(2,1)S(1)} %attend.4.refs_4_.refs_0_), channel_id=1, source_target_pairs={{0,4},{1,5},{2,6},{3,7},{4,0},{5,1},{6,2},{7,3},{8,12},{9,13},{10,... | collective-permute-start | bytes 393224 | tf_op jit(solution)/shard_map/ppermute | solution.py:261
  44.1 3.7 %next_heads.2 = (bf16[512,128]{1,0:T(8,128)(2,1)S(1)}, bf16[528,256]{1,0:T(8,128)(2,1)S(1)}, bf16[512,256]{1,0:T(8,128)(2,1)S(1)}) custom-call(bf16[512,128]{1,0:T(8,128)(2,1)S(1)} %attend.5.refs_0_, bf16[512,128]{1,0:T(8,128)(2,1)S(1)} %collective-permute-done.4.refs_1_, bf16[512,128]{1,0:T(8,128)(2,1)S(1)} %collective-permute-done.5.refs_2_, ...), custom_call_target="tpu_custom_call" | custom-call | flops 2952790016 | bytes 7864320 | tf_op jit(solution)/shard_map/next_heads/pallas_call | solution.py:348
  47.7 2.6 %collective-permute-done.2.refs_2_ = bf16[512,128]{1,0:T(8,128)(2,1)S(1)} collective-permute-done((bf16[512,128]{1,0:T(8,128)(2,1)S(1)}, bf16[512,128]{1,0:T(8,128)(2,1)S(1)}, u32[]{:S(2)}, u32[]{:S(2)}) %collective-permute-start.2) | collective-permute-done | bytes 131104 | tf_op jit(solution)/shard_map/ppermute | solution.py:261
  50.4 1.1 %collective-permute-start.8 = (bf16[4,512,128]{2,1,0:T(8,128)(2,1)S(1)}, bf16[4,512,128]{2,1,0:T(8,128)(2,1)S(1)}, u32[]{:S(2)}, u32[]{:S(2)}) collective-permute-start(bf16[4,512,128]{2,1,0:T(8,128)(2,1)S(1)} %stack.5), channel_id=1, source_target_pairs={{0,1},{1,0},{2,3},{3,2},{4,5},{5,4},{6,7},{7,6},{8,9},{9,8},{10,11... | collective-permute-start | bytes 1572872 | tf_op jit(solution)/shard_map/ppermute | solution.py:261
  51.5 1.3 %collective-permute-start.9 = (bf16[528,256]{1,0:T(8,128)(2,1)S(1)}, bf16[528,256]{1,0:T(8,128)(2,1)S(1)}, u32[]{:S(2)}, u32[]{:S(2)}) collective-permute-start(bf16[528,256]{1,0:T(8,128)(2,1)S(1)} %get-tuple-element.29.refs_4_.refs_2_), channel_id=1, source_target_pairs={{0,8},{8,16},{16,24},{24,32},{32,40},{40,48},{48,56},{56,64},{64,7... | collective-permute-start | bytes 811016 | tf_op jit(solution)/shard_map/ppermute | solution.py:428
  53.0 3.6 %next_heads.3 = (bf16[512,128]{1,0:T(8,128)(2,1)S(1)}, bf16[512,256]{1,0:T(8,128)(2,1)S(1)}, bf16[512,256]{1,0:T(8,128)(2,1)S(1)}) custom-call(bf16[512,128]{1,0:T(8,128)(2,1)S(1)} %attend.4.refs_4_.refs_0_, bf16[512,128]{1,0:T(8,128)(2,1)S(1)} %collective-permute-done.1.refs_1_, bf16[512,128]{1,0:T(8,128)(2,1)S(1)} %collective-permute-done.2.refs_2_, ...), custom_call_target="tpu_custom_call" | custom-call | flops 2952790016 | bytes 7864320 | tf_op jit(solution)/shard_map/next_heads/pallas_call | solution.py:348
  56.7 1.5 %attend.7.refs_0_ = bf16[512,128]{1,0:T(8,128)(2,1)S(1)} custom-call(bf16[512,128]{1,0:T(8,128)(2,1)S(1)} %get-tuple-element.32.refs_0_, bf16[512,256]{1,0:T(8,128)(2,1)S(1)} %get-tuple-element.31.refs_2_.refs_1_, bf16[528,256]{1,0:T(8,128)(2,1)S(1)} %get-tuple-element.29.refs_4_.refs_2_, f32[1,1024]{1,0:T(1,128)S(1)} %get-tuple-element.23.refs_3_.refs_11_, ...), custom_call_target="tpu_custom_call" | custom-call | flops 335544320 | bytes 524288 | tf_op jit(solution)/shard_map/attend/pallas_call | solution.py:245
  58.4 3.5 %collective-permute-start.14 = (bf16[512,128]{1,0:T(8,128)(2,1)S(1)}, bf16[512,128]{1,0:T(8,128)(2,1)S(1)}, u32[]{:S(2)}, u32[]{:S(2)}) collective-permute-start(bf16[512,128]{1,0:T(8,128)(2,1)S(1)} %attend.7.refs_0_), channel_id=1, source_target_pairs={{0,4},{1,5},{2,6},{3,7},{4,0},{5,1},{6,2},{7,3},{8,12},{9,13},{10,... | collective-permute-start | bytes 393224 | tf_op jit(solution)/shard_map/ppermute | solution.py:261
  61.9 1.5 %attend.6.refs_4_.refs_0_ = bf16[512,128]{1,0:T(8,128)(2,1)S(1)} custom-call(bf16[512,128]{1,0:T(8,128)(2,1)S(1)} %get-tuple-element.30.refs_0_, bf16[528,256]{1,0:T(8,128)(2,1)S(1)} %collective-permute-done.9.refs_1_, bf16[512,256]{1,0:T(8,128)(2,1)S(1)} %get-tuple-element.31.refs_2_.refs_1_, f32[1,1024]{1,0:T(1,128)S(1)} %get-tuple-element.23.refs_3_.refs_11_, ...), custom_call_target="tpu_custom_call" | custom-call | flops 335544320 | bytes 524288 | tf_op jit(solution)/shard_map/attend/pallas_call | solution.py:245
  63.4 0.8 collective-permute-done.13.refs_1_
  64.2 3.7 %collective-permute-done.14.refs_2_ = bf16[512,128]{1,0:T(8,128)(2,1)S(1)} collective-permute-done((bf16[512,128]{1,0:T(8,128)(2,1)S(1)}, bf16[512,128]{1,0:T(8,128)(2,1)S(1)}, u32[]{:S(2)}, u32[]{:S(2)}) %collective-permute-start.14) | collective-permute-done | bytes 131104 | tf_op jit(solution)/shard_map/ppermute | solution.py:261
  68.0 1.6 %collective-permute-start.16 = (bf16[4,512,128]{2,1,0:T(8,128)(2,1)S(1)}, bf16[4,512,128]{2,1,0:T(8,128)(2,1)S(1)}, u32[]{:S(2)}, u32[]{:S(2)}) collective-permute-start(bf16[4,512,128]{2,1,0:T(8,128)(2,1)S(1)} %stack.6), channel_id=1, source_target_pairs={{0,1},{1,0},{2,3},{3,2},{4,5},{5,4},{6,7},{7,6},{8,9},{9,8},{10,11... | collective-permute-start | bytes 1572872 | tf_op jit(solution)/shard_map/ppermute | solution.py:261
  69.5 3.3 %collective-permute-start.11 = (bf16[512,128]{1,0:T(8,128)(2,1)S(1)}, bf16[512,128]{1,0:T(8,128)(2,1)S(1)}, u32[]{:S(2)}, u32[]{:S(2)}) collective-permute-start(bf16[512,128]{1,0:T(8,128)(2,1)S(1)} %attend.6.refs_4_.refs_0_), channel_id=1, source_target_pairs={{0,4},{1,5},{2,6},{3,7},{4,0},{5,1},{6,2},{7,3},{8,12},{9,13},{10,... | collective-permute-start | bytes 393224 | tf_op jit(solution)/shard_map/ppermute | solution.py:261
  72.8 0.5 last.2.refs_4_.refs_7_
  73.3 2.4 %collective-permute-done.10.refs_1_ = bf16[512,128]{1,0:T(8,128)(2,1)S(1)} collective-permute-done((bf16[512,128]{1,0:T(8,128)(2,1)S(1)}, bf16[512,128]{1,0:T(8,128)(2,1)S(1)}, u32[]{:S(2)}, u32[]{:S(2)}) %collective-permute-start.10) | collective-permute-done | bytes 131104 | tf_op jit(solution)/shard_map/ppermute | solution.py:261
  75.7 3.4 %collective-permute-done.11.refs_2_ = bf16[512,128]{1,0:T(8,128)(2,1)S(1)} collective-permute-done((bf16[512,128]{1,0:T(8,128)(2,1)S(1)}, bf16[512,128]{1,0:T(8,128)(2,1)S(1)}, u32[]{:S(2)}, u32[]{:S(2)}) %collective-permute-start.11) | collective-permute-done | bytes 131104 | tf_op jit(solution)/shard_map/ppermute | solution.py:261
  79.1 1.1 %collective-permute-start.17 = (bf16[4,512,128]{2,1,0:T(8,128)(2,1)S(1)}, bf16[4,512,128]{2,1,0:T(8,128)(2,1)S(1)}, u32[]{:S(2)}, u32[]{:S(2)}) collective-permute-start(bf16[4,512,128]{2,1,0:T(8,128)(2,1)S(1)} %stack.7), channel_id=1, source_target_pairs={{0,1},{1,0},{2,3},{3,2},{4,5},{5,4},{6,7},{7,6},{8,9},{9,8},{10,11... | collective-permute-start | bytes 1572872 | tf_op jit(solution)/shard_map/ppermute | solution.py:261
  80.2 1.5 %collective-permute-done.17.refs_4_ = bf16[4,512,128]{2,1,0:T(8,128)(2,1)S(1)} collective-permute-done((bf16[4,512,128]{2,1,0:T(8,128)(2,1)S(1)}, bf16[4,512,128]{2,1,0:T(8,128)(2,1)S(1)}, u32[]{:S(2)}, u32[]{:S(2)}) %collective-permute-start.17) | collective-permute-done | bytes 524320 | tf_op jit(solution)/shard_map/ppermute | solution.py:261
  81.8 1.3 %last.3 = bf16[1024,256]{1,0:T(8,128)(2,1)} custom-call(bf16[512,128]{1,0:T(8,128)(2,1)S(1)} %attend.6.refs_4_.refs_0_, bf16[512,128]{1,0:T(8,128)(2,1)S(1)} %collective-permute-done.10.refs_1_, bf16[512,128]{1,0:T(8,128)(2,1)S(1)} %collective-permute-done.11.refs_2_, bf16[512,128]{1,0:T(8,128)(2,1)S(1)} %collective-permute-done.12.refs_3_, ...), custom_call_target="tpu_custom_call" | custom-call | flops 268435456 | bytes 1572864 | tf_op jit(solution)/shard_map/last/pallas_call | solution.py:387
  (29 shorter events, 0.5 us)
Async XLA Ops:
  0.0 20.8 %copy-start = (bf16[1024,2048]{1,0:T(8,128)(2,1)S(1)}, bf16[1024,2048]{1,0:T(8,128)(2,1)}, u32[]{:S(2)}) copy-start(bf16[1024,2048]{1,0:T(8,128)(2,1)} %refs_5_.8) | copy-start | bytes 12582916
  0.0 20.8 %copy-start.1 = (bf16[1024,2048]{1,0:T(8,128)(2,1)S(1)}, bf16[1024,2048]{1,0:T(8,128)(2,1)}, u32[]{:S(2)}) copy-start(bf16[1024,2048]{1,0:T(8,128)(2,1)} %refs_6_.9) | copy-start | bytes 12582916
  0.0 0.8 %copy-start.3 = (bf16[2,2048]{1,0:T(2,128)(2,1)S(1)}, bf16[2,2048]{1,0:T(2,128)(2,1)}, u32[]{:S(2)}) copy-start(bf16[2,2048]{1,0:T(2,128)(2,1)} %refs_1_.1) | copy-start | bytes 24580
  0.9 1.1 %copy-start.4 = (f32[2,2,257]{2,1,0:T(2,128)S(1)}, f32[2,2,257]{2,1,0:T(2,128)}, u32[]{:S(2)}) copy-start(f32[2,2,257]{2,1,0:T(2,128)} %refs_6_.6) | copy-start | bytes 12340
  2.0 1.2 %copy-start.5 = (s32[1024]{0:T(1024)S(1)}, s32[1024]{0:T(1024)}, u32[]{:S(2)}) copy-start(s32[1024]{0:T(1024)} %refs_5_.5) | copy-start | bytes 12292
  8.8 12.0 %collective-permute-start = (bf16[528,256]{1,0:T(8,128)(2,1)S(1)}, bf16[528,256]{1,0:T(8,128)(2,1)S(1)}, u32[]{:S(2)}, u32[]{:S(2)}) collective-permute-start(bf16[528,256]{1,0:T(8,128)(2,1)S(1)} %get-tuple-element.21.refs_2_), channel_id=1, source_target_pairs={{0,8},{8,16},{16,24},{24,32},{32,40},{40,48},{48,56},{56,64},{64,7... | collective-permute-start | bytes 811016 | tf_op jit(solution)/shard_map/ppermute | solution.py:415
  15.6 6.7 %collective-permute-start.4 = (bf16[512,128]{1,0:T(8,128)(2,1)S(1)}, bf16[512,128]{1,0:T(8,128)(2,1)S(1)}, u32[]{:S(2)}, u32[]{:S(2)}) collective-permute-start(bf16[512,128]{1,0:T(8,128)(2,1)S(1)} %attend.5.refs_0_), channel_id=1, source_target_pairs={{0,2},{1,3},{2,4},{3,5},{4,6},{5,7},{6,0},{7,1},{8,10},{9,11},{10,... | collective-permute-start | bytes 393224 | tf_op jit(solution)/shard_map/ppermute | solution.py:261
  17.0 7.9 %collective-permute-start.5 = (bf16[512,128]{1,0:T(8,128)(2,1)S(1)}, bf16[512,128]{1,0:T(8,128)(2,1)S(1)}, u32[]{:S(2)}, u32[]{:S(2)}) collective-permute-start(bf16[512,128]{1,0:T(8,128)(2,1)S(1)} %attend.5.refs_0_), channel_id=1, source_target_pairs={{0,4},{1,5},{2,6},{3,7},{4,0},{5,1},{6,2},{7,3},{8,12},{9,13},{10,... | collective-permute-start | bytes 393224 | tf_op jit(solution)/shard_map/ppermute | solution.py:261
  19.8 5.2 %collective-permute-start.6 = (bf16[512,128]{1,0:T(8,128)(2,1)S(1)}, bf16[512,128]{1,0:T(8,128)(2,1)S(1)}, u32[]{:S(2)}, u32[]{:S(2)}) collective-permute-start(bf16[512,128]{1,0:T(8,128)(2,1)S(1)} %attend.5.refs_0_), channel_id=1, source_target_pairs={{0,6},{1,7},{2,0},{3,1},{4,2},{5,3},{6,4},{7,5},{8,14},{9,15},{10,... | collective-permute-start | bytes 393224 | tf_op jit(solution)/shard_map/ppermute | solution.py:261
  25.0 19.1 %collective-permute-start.7 = (bf16[4,512,128]{2,1,0:T(8,128)(2,1)S(1)}, bf16[4,512,128]{2,1,0:T(8,128)(2,1)S(1)}, u32[]{:S(2)}, u32[]{:S(2)}) collective-permute-start(bf16[4,512,128]{2,1,0:T(8,128)(2,1)S(1)} %stack.4), channel_id=1, source_target_pairs={{0,1},{1,0},{2,3},{3,2},{4,5},{5,4},{6,7},{7,6},{8,9},{9,8},{10,11... | collective-permute-start | bytes 1572872 | tf_op jit(solution)/shard_map/ppermute | solution.py:261
  40.8 6.9 %collective-permute-start.1 = (bf16[512,128]{1,0:T(8,128)(2,1)S(1)}, bf16[512,128]{1,0:T(8,128)(2,1)S(1)}, u32[]{:S(2)}, u32[]{:S(2)}) collective-permute-start(bf16[512,128]{1,0:T(8,128)(2,1)S(1)} %attend.4.refs_4_.refs_0_), channel_id=1, source_target_pairs={{0,2},{1,3},{2,4},{3,5},{4,6},{5,7},{6,0},{7,1},{8,10},{9,11},{10,... | collective-permute-start | bytes 393224 | tf_op jit(solution)/shard_map/ppermute | solution.py:261
  41.1 9.2 %collective-permute-start.2 = (bf16[512,128]{1,0:T(8,128)(2,1)S(1)}, bf16[512,128]{1,0:T(8,128)(2,1)S(1)}, u32[]{:S(2)}, u32[]{:S(2)}) collective-permute-start(bf16[512,128]{1,0:T(8,128)(2,1)S(1)} %attend.4.refs_4_.refs_0_), channel_id=1, source_target_pairs={{0,4},{1,5},{2,6},{3,7},{4,0},{5,1},{6,2},{7,3},{8,12},{9,13},{10,... | collective-permute-start | bytes 393224 | tf_op jit(solution)/shard_map/ppermute | solution.py:261
  44.0 6.3 %collective-permute-start.3 = (bf16[512,128]{1,0:T(8,128)(2,1)S(1)}, bf16[512,128]{1,0:T(8,128)(2,1)S(1)}, u32[]{:S(2)}, u32[]{:S(2)}) collective-permute-start(bf16[512,128]{1,0:T(8,128)(2,1)S(1)} %attend.4.refs_4_.refs_0_), channel_id=1, source_target_pairs={{0,6},{1,7},{2,0},{3,1},{4,2},{5,3},{6,4},{7,5},{8,14},{9,15},{10,... | collective-permute-start | bytes 393224 | tf_op jit(solution)/shard_map/ppermute | solution.py:261
  50.3 11.6 %copy-start.2 = (bf16[1024,256]{1,0:T(8,128)(2,1)S(1)}, bf16[1024,256]{1,0:T(8,128)(2,1)}, u32[]{:S(2)}) copy-start(bf16[1024,256]{1,0:T(8,128)(2,1)} %refs_6_.11) | copy-start | bytes 1572868
  50.4 2.7 %collective-permute-start.8 = (bf16[4,512,128]{2,1,0:T(8,128)(2,1)S(1)}, bf16[4,512,128]{2,1,0:T(8,128)(2,1)S(1)}, u32[]{:S(2)}, u32[]{:S(2)}) collective-permute-start(bf16[4,512,128]{2,1,0:T(8,128)(2,1)S(1)} %stack.5), channel_id=1, source_target_pairs={{0,1},{1,0},{2,3},{3,2},{4,5},{5,4},{6,7},{7,6},{8,9},{9,8},{10,11... | collective-permute-start | bytes 1572872 | tf_op jit(solution)/shard_map/ppermute | solution.py:261
  51.5 10.4 %collective-permute-start.9 = (bf16[528,256]{1,0:T(8,128)(2,1)S(1)}, bf16[528,256]{1,0:T(8,128)(2,1)S(1)}, u32[]{:S(2)}, u32[]{:S(2)}) collective-permute-start(bf16[528,256]{1,0:T(8,128)(2,1)S(1)} %get-tuple-element.29.refs_4_.refs_2_), channel_id=1, source_target_pairs={{0,8},{8,16},{16,24},{24,32},{32,40},{40,48},{48,56},{56,64},{64,7... | collective-permute-start | bytes 811016 | tf_op jit(solution)/shard_map/ppermute | solution.py:428
  58.2 6.0 %collective-permute-start.13 = (bf16[512,128]{1,0:T(8,128)(2,1)S(1)}, bf16[512,128]{1,0:T(8,128)(2,1)S(1)}, u32[]{:S(2)}, u32[]{:S(2)}) collective-permute-start(bf16[512,128]{1,0:T(8,128)(2,1)S(1)} %attend.7.refs_0_), channel_id=1, source_target_pairs={{0,2},{1,3},{2,4},{3,5},{4,6},{5,7},{6,0},{7,1},{8,10},{9,11},{10,... | collective-permute-start | bytes 393224 | tf_op jit(solution)/shard_map/ppermute | solution.py:261
  58.4 9.6 %collective-permute-start.14 = (bf16[512,128]{1,0:T(8,128)(2,1)S(1)}, bf16[512,128]{1,0:T(8,128)(2,1)S(1)}, u32[]{:S(2)}, u32[]{:S(2)}) collective-permute-start(bf16[512,128]{1,0:T(8,128)(2,1)S(1)} %attend.7.refs_0_), channel_id=1, source_target_pairs={{0,4},{1,5},{2,6},{3,7},{4,0},{5,1},{6,2},{7,3},{8,12},{9,13},{10,... | collective-permute-start | bytes 393224 | tf_op jit(solution)/shard_map/ppermute | solution.py:261
  61.9 6.0 %collective-permute-start.15 = (bf16[512,128]{1,0:T(8,128)(2,1)S(1)}, bf16[512,128]{1,0:T(8,128)(2,1)S(1)}, u32[]{:S(2)}, u32[]{:S(2)}) collective-permute-start(bf16[512,128]{1,0:T(8,128)(2,1)S(1)} %attend.7.refs_0_), channel_id=1, source_target_pairs={{0,6},{1,7},{2,0},{3,1},{4,2},{5,3},{6,4},{7,5},{8,14},{9,15},{10,... | collective-permute-start | bytes 393224 | tf_op jit(solution)/shard_map/ppermute | solution.py:261
  68.0 4.8 %collective-permute-start.16 = (bf16[4,512,128]{2,1,0:T(8,128)(2,1)S(1)}, bf16[4,512,128]{2,1,0:T(8,128)(2,1)S(1)}, u32[]{:S(2)}, u32[]{:S(2)}) collective-permute-start(bf16[4,512,128]{2,1,0:T(8,128)(2,1)S(1)} %stack.6), channel_id=1, source_target_pairs={{0,1},{1,0},{2,3},{3,2},{4,5},{5,4},{6,7},{7,6},{8,9},{9,8},{10,11... | collective-permute-start | bytes 1572872 | tf_op jit(solution)/shard_map/ppermute | solution.py:261
  69.5 6.1 %collective-permute-start.10 = (bf16[512,128]{1,0:T(8,128)(2,1)S(1)}, bf16[512,128]{1,0:T(8,128)(2,1)S(1)}, u32[]{:S(2)}, u32[]{:S(2)}) collective-permute-start(bf16[512,128]{1,0:T(8,128)(2,1)S(1)} %attend.6.refs_4_.refs_0_), channel_id=1, source_target_pairs={{0,2},{1,3},{2,4},{3,5},{4,6},{5,7},{6,0},{7,1},{8,10},{9,11},{10,... | collective-permute-start | bytes 393224 | tf_op jit(solution)/shard_map/ppermute | solution.py:261
  69.5 9.5 %collective-permute-start.11 = (bf16[512,128]{1,0:T(8,128)(2,1)S(1)}, bf16[512,128]{1,0:T(8,128)(2,1)S(1)}, u32[]{:S(2)}, u32[]{:S(2)}) collective-permute-start(bf16[512,128]{1,0:T(8,128)(2,1)S(1)} %attend.6.refs_4_.refs_0_), channel_id=1, source_target_pairs={{0,4},{1,5},{2,6},{3,7},{4,0},{5,1},{6,2},{7,3},{8,12},{9,13},{10,... | collective-permute-start | bytes 393224 | tf_op jit(solution)/shard_map/ppermute | solution.py:261
  72.8 6.3 %collective-permute-start.12 = (bf16[512,128]{1,0:T(8,128)(2,1)S(1)}, bf16[512,128]{1,0:T(8,128)(2,1)S(1)}, u32[]{:S(2)}, u32[]{:S(2)}) collective-permute-start(bf16[512,128]{1,0:T(8,128)(2,1)S(1)} %attend.6.refs_4_.refs_0_), channel_id=1, source_target_pairs={{0,6},{1,7},{2,0},{3,1},{4,2},{5,3},{6,4},{7,5},{8,14},{9,15},{10,... | collective-permute-start | bytes 393224 | tf_op jit(solution)/shard_map/ppermute | solution.py:261
  79.1 2.7 %collective-permute-start.17 = (bf16[4,512,128]{2,1,0:T(8,128)(2,1)S(1)}, bf16[4,512,128]{2,1,0:T(8,128)(2,1)S(1)}, u32[]{:S(2)}, u32[]{:S(2)}) collective-permute-start(bf16[4,512,128]{2,1,0:T(8,128)(2,1)S(1)} %stack.7), channel_id=1, source_target_pairs={{0,1},{1,0},{2,3},{3,2},{4,5},{5,4},{6,7},{7,6},{8,9},{9,8},{10,11... | collective-permute-start | bytes 1572872 | tf_op jit(solution)/shard_map/ppermute | solution.py:261

commit v2 on v1

--- a/solution.py
+++ b/solution.py
@@ -6,6 +6,7 @@
 from jax.experimental import pallas as pl
 from jax.experimental.pallas import tpu as pltpu
 from jax.sharding import PartitionSpec as P
+
 
 SEG = 64
 PREV_SEGS = 8
@@ -21,6 +22,7 @@
 VMEM_LIMIT = 24 * 2**20
 FIRST_VMEM_LIMIT = 51 * 2**20
 
+
 F32 = jnp.float32
 BF16 = jnp.bfloat16
 
@@ -74,7 +76,7 @@
         )
         for i, row in enumerate(order)
     ]
-    for copy in (*side_copies, x_copies[0], *w_copies, *x_copies[1:], *next_copies):
+    for copy in (*side_copies, x_copies[0], *w_copies, x_copies[1]):
         copy.start()
     for copy in side_copies:
         copy.wait()
@@ -85,8 +87,11 @@
     late_ref[half_rows:, :] = doc_rows(docs[:, half_rows:], width)
     for copy in w_copies:
         copy.wait()
-    for copy, row in zip(x_copies, order):
+    later = [[copy] for copy in x_copies[2:]] + [next_copies, []]
+    for copy, row, starting in zip(x_copies, order, later):
         copy.wait()
+        for other in starting:
+            other.start()
         queries, kv = project_heads(
             x_ref[pl.ds(row, block_rows), :],
             gain_ref[0:1, :],
@@ -267,7 +272,10 @@
             ],
         )
 
-    return moved, [block, *[moved(block, by) for by in range(1, chips)]]
+    blocks = [block]
+    for by in range(1, chips):
+        blocks.append(moved(block, by))
+    return moved, blocks
 
 
 def stack_kernel(*refs):
@@ -277,14 +285,15 @@
 
 
 def from_partner(moved, blocks, after):
-    stacked = pl.pallas_call(
+    stack = pl.pallas_call(
         stack_kernel,
         in_specs=[*whole(len(blocks)), pl.BlockSpec(memory_space=pl.ANY)],
         out_specs=pl.BlockSpec(memory_space=pltpu.VMEM),
         out_shape=jax.ShapeDtypeStruct((len(blocks), *blocks[0].shape), BF16),
         compiler_params=pltpu.CompilerParams(vmem_limit_bytes=VMEM_LIMIT),
         name="stack",
-    )(*blocks, after)
+    )
+    stacked = stack(*blocks, after)
     return [*blocks, moved(stacked, 0, True)]
 
 
@@ -399,8 +408,6 @@
 
 
 def shards(tokens, doc_ids, gains, w_query, w_key, w_value, rel_table, out_first, out_last):
-    row_count = tokens.shape[0]
-    half_rows = row_count // 2
     head_count = rel_table.shape[1]
     width = w_query.shape[2]
     head_width = width // head_count
@@ -418,7 +425,9 @@
         late = attention(q_late, kv_early, kv_late, docs, biases, layer, head_width, False)
         moved, late = gather(late)
         ahead = (tokens, out_first) if layer == 0 else (out_last,)
-        early = attention(q_early, far, kv_early, docs, biases, layer, head_width, True, ahead)
+        early = attention(
+            q_early, far, kv_early, docs, biases, layer, head_width, True, ahead
+        )
         late = from_partner(moved, late, early)
         moved, early = gather(early)
         if layer == 0:

time: 83.3 us -> 82.4 us (0.989)
  Pallas kernels: 20.9 us -> 19.9 us
    pallas_call x1, Pallas kernels: 5.6 us -> 4.65 us  [heads(): pl.pallas_call(functools.partial(heads_kernel, q_scale, block_rows), in_s...]
where the time goes in v2:
time: 82.4 us; the launch traced here: 82.1 us
  starting transfers between devices  41.6 us (50%)
  Pallas kernels  19.9 us (24%)
  waiting for transfers between devices  17.2 us (21%)
  local copies, waits for them, and re-layouts  3.18 us (4%)
    ppermute x16, starting transfers between devices, moved(): lax.ppermute(array, 'tp', [(2 * x + core, 2 * ((x + by) % chips) + (1 - c...  35.1 us
    ppermute x16, waiting for transfers between devices, moved(): lax.ppermute(array, 'tp', [(2 * x + core, 2 * ((x + by) % chips) + (1 - c...  17.2 us
    pallas_call x2, Pallas kernels, next_heads(): pl.pallas_call(functools.partial(next_kernel, q_scale, block_rows, len(bl...  7.3 us
    ppermute x2, starting transfers between devices, shards(): far = lax.ppermute(kv_late, 'sp', onward)  6.58 us
    pallas_call x4, Pallas kernels, attention(): pl.pallas_call(functools.partial(attention_kernel, head_width, layer, fro...  6.06 us
    pallas_call x1, Pallas kernels, heads(): pl.pallas_call(functools.partial(heads_kernel, q_scale, block_rows), in_s...  4.65 us
    unnamed x12, local copies, waits for them, and re-layouts  3.18 us
    pallas_call x2, Pallas kernels, last_update(): pl.pallas_call(functools.partial(last_kernel, len(blocks)), in_specs=whol...  1.79 us
  transfers between devices with their start and end apart: 18, of which 8 were waited for; matrix products, arithmetic and copies ran while one was open for 0% of the time, Pallas kernels for 17%

profile of v2, /device:TPU:33, one launch (start us, length us, event | category | flops | bytes accessed | tf_op | source)
XLA Modules:
  0.0 82.1 jit_solution(15252697149139352809)
XLA Ops:
  0.0 0.8 %copy-done.3 = bf16[2,2048]{1,0:T(2,128)(2,1)S(1)} copy-done((bf16[2,2048]{1,0:T(2,128)(2,1)S(1)}, bf16[2,2048]{1,0:T(2,128)(2,1)}, u32[]{:S(2)}) %copy-start.3) | copy-done | bytes 8216
  0.9 1.1 %copy-done.4 = f32[2,2,257]{2,1,0:T(2,128)S(1)} copy-done((f32[2,2,257]{2,1,0:T(2,128)S(1)}, f32[2,2,257]{2,1,0:T(2,128)}, u32[]{:S(2)}) %copy-start.4) | copy-done | bytes 4136
  2.0 1.2 %copy-done.5 = s32[1024]{0:T(1024)S(1)} copy-done((s32[1024]{0:T(1024)S(1)}, s32[1024]{0:T(1024)}, u32[]{:S(2)}) %copy-start.5) | copy-done | bytes 4120
  3.2 4.7 %heads.1 = (bf16[1024,128]{1,0:T(8,128)(2,1)S(1)}, bf16[512,256]{1,0:T(8,128)(2,1)S(1)}, bf16[528,256]{1,0:T(8,128)(2,1)S(1)}, f32[1,1024]{1,0:T(1,128)S(1)}, f3...) custom-call(bf16[1024,2048]{1,0:T(8,128)(2,1)} %refs_5_.8, ...), custom_call_target="tpu_custom_call" | custom-call | flops 1610612736 | bytes 5767168 | tf_op jit(solution)/shard_map/heads/pallas_call | solution.py:120
  7.8 5.3 %collective-permute-start = (bf16[528,256]{1,0:T(8,128)(2,1)S(1)}, bf16[528,256]{1,0:T(8,128)(2,1)S(1)}, u32[]{:S(2)}, u32[]{:S(2)}) collective-permute-start(bf16[528,256]{1,0:T(8,128)(2,1)S(1)} %get-tuple-element.21.refs_2_), channel_id=1, source_target_pairs={{0,8},{8,16},{16,24},{24,32},{32,40},{40,48},{48,56},{56,64},{64,7... | collective-permute-start | bytes 811016 | tf_op jit(solution)/shard_map/ppermute | solution.py:422
  13.1 1.5 %attend.5.refs_0_ = bf16[512,128]{1,0:T(8,128)(2,1)S(1)} custom-call(bf16[1024,128]{1,0:T(8,128)(2,1)S(1)} %get-tuple-element.20.refs_0_, bf16[512,256]{1,0:T(8,128)(2,1)S(1)} %get-tuple-element.22.refs_2_.refs_1_, bf16[528,256]{1,0:T(8,128)(2,1)S(1)} %get-tuple-element.21.refs_2_, f32[1,1024]{1,0:T(1,128)S(1)} %get-tuple-element.23.refs_3_.refs_11_, ...), custom_call_target="tpu_custom_call" | custom-call | flops 335544320 | bytes 524288 | tf_op jit(solution)/shard_map/attend/pallas_call | solution.py:250
  14.6 1.5 %collective-permute-start.4 = (bf16[512,128]{1,0:T(8,128)(2,1)S(1)}, bf16[512,128]{1,0:T(8,128)(2,1)S(1)}, u32[]{:S(2)}, u32[]{:S(2)}) collective-permute-start(bf16[512,128]{1,0:T(8,128)(2,1)S(1)} %attend.5.refs_0_), channel_id=1, source_target_pairs={{0,2},{1,3},{2,4},{3,5},{4,6},{5,7},{6,0},{7,1},{8,10},{9,11},{10,... | collective-permute-start | bytes 393224 | tf_op jit(solution)/shard_map/ppermute | solution.py:266
  16.1 2.7 %collective-permute-start.5 = (bf16[512,128]{1,0:T(8,128)(2,1)S(1)}, bf16[512,128]{1,0:T(8,128)(2,1)S(1)}, u32[]{:S(2)}, u32[]{:S(2)}) collective-permute-start(bf16[512,128]{1,0:T(8,128)(2,1)S(1)} %attend.5.refs_0_), channel_id=1, source_target_pairs={{0,4},{1,5},{2,6},{3,7},{4,0},{5,1},{6,2},{7,3},{8,12},{9,13},{10,... | collective-permute-start | bytes 393224 | tf_op jit(solution)/shard_map/ppermute | solution.py:266
  18.8 1.0 %collective-permute-start.6 = (bf16[512,128]{1,0:T(8,128)(2,1)S(1)}, bf16[512,128]{1,0:T(8,128)(2,1)S(1)}, u32[]{:S(2)}, u32[]{:S(2)}) collective-permute-start(bf16[512,128]{1,0:T(8,128)(2,1)S(1)} %attend.5.refs_0_), channel_id=1, source_target_pairs={{0,6},{1,7},{2,0},{3,1},{4,2},{5,3},{6,4},{7,5},{8,14},{9,15},{10,... | collective-permute-start | bytes 393224 | tf_op jit(solution)/shard_map/ppermute | solution.py:266
  19.9 1.5 %attend.4.refs_4_.refs_0_ = bf16[512,128]{1,0:T(8,128)(2,1)S(1)} custom-call(bf16[1024,128]{1,0:T(8,128)(2,1)S(1)} %get-tuple-element.20.refs_0_, bf16[528,256]{1,0:T(8,128)(2,1)S(1)} %collective-permute-done.refs_1_, bf16[512,256]{1,0:T(8,128)(2,1)S(1)} %get-tuple-element.22.refs_2_.refs_1_, f32[1,1024]{1,0:T(1,128)S(1)} %get-tuple-element.23.refs_3_.refs_11_, ...), custom_call_target="tpu_custom_call" | custom-call | flops 335544320 | bytes 524288 | tf_op jit(solution)/shard_map/attend/pallas_call | solution.py:250
  21.4 2.6 %collective-permute-done.5.refs_2_ = bf16[512,128]{1,0:T(8,128)(2,1)S(1)} collective-permute-done((bf16[512,128]{1,0:T(8,128)(2,1)S(1)}, bf16[512,128]{1,0:T(8,128)(2,1)S(1)}, u32[]{:S(2)}, u32[]{:S(2)}) %collective-permute-start.5) | collective-permute-done | bytes 131104 | tf_op jit(solution)/shard_map/ppermute | solution.py:266
  24.0 15.8 %collective-permute-start.7 = (bf16[4,512,128]{2,1,0:T(8,128)(2,1)S(1)}, bf16[4,512,128]{2,1,0:T(8,128)(2,1)S(1)}, u32[]{:S(2)}, u32[]{:S(2)}) collective-permute-start(bf16[4,512,128]{2,1,0:T(8,128)(2,1)S(1)} %stack.4), channel_id=1, source_target_pairs={{0,1},{1,0},{2,3},{3,2},{4,5},{5,4},{6,7},{7,6},{8,9},{9,8},{10,11... | collective-permute-start | bytes 1572872 | tf_op jit(solution)/shard_map/ppermute | solution.py:266
  39.9 0.3 collective-permute-start.1
  40.2 2.9 %collective-permute-start.2 = (bf16[512,128]{1,0:T(8,128)(2,1)S(1)}, bf16[512,128]{1,0:T(8,128)(2,1)S(1)}, u32[]{:S(2)}, u32[]{:S(2)}) collective-permute-start(bf16[512,128]{1,0:T(8,128)(2,1)S(1)} %attend.4.refs_4_.refs_0_), channel_id=1, source_target_pairs={{0,4},{1,5},{2,6},{3,7},{4,0},{5,1},{6,2},{7,3},{8,12},{9,13},{10,... | collective-permute-start | bytes 393224 | tf_op jit(solution)/shard_map/ppermute | solution.py:266
  43.1 3.7 %next_heads.2 = (bf16[512,128]{1,0:T(8,128)(2,1)S(1)}, bf16[528,256]{1,0:T(8,128)(2,1)S(1)}, bf16[512,256]{1,0:T(8,128)(2,1)S(1)}) custom-call(bf16[512,128]{1,0:T(8,128)(2,1)S(1)} %attend.5.refs_0_, bf16[512,128]{1,0:T(8,128)(2,1)S(1)} %collective-permute-done.4.refs_1_, bf16[512,128]{1,0:T(8,128)(2,1)S(1)} %collective-permute-done.5.refs_2_, ...), custom_call_target="tpu_custom_call" | custom-call | flops 2952790016 | bytes 7864320 | tf_op jit(solution)/shard_map/next_heads/pallas_call | solution.py:357
  46.8 2.6 %collective-permute-done.2.refs_2_ = bf16[512,128]{1,0:T(8,128)(2,1)S(1)} collective-permute-done((bf16[512,128]{1,0:T(8,128)(2,1)S(1)}, bf16[512,128]{1,0:T(8,128)(2,1)S(1)}, u32[]{:S(2)}, u32[]{:S(2)}) %collective-permute-start.2) | collective-permute-done | bytes 131104 | tf_op jit(solution)/shard_map/ppermute | solution.py:266
  49.4 1.1 %collective-permute-start.8 = (bf16[4,512,128]{2,1,0:T(8,128)(2,1)S(1)}, bf16[4,512,128]{2,1,0:T(8,128)(2,1)S(1)}, u32[]{:S(2)}, u32[]{:S(2)}) collective-permute-start(bf16[4,512,128]{2,1,0:T(8,128)(2,1)S(1)} %stack.5), channel_id=1, source_target_pairs={{0,1},{1,0},{2,3},{3,2},{4,5},{5,4},{6,7},{7,6},{8,9},{9,8},{10,11... | collective-permute-start | bytes 1572872 | tf_op jit(solution)/shard_map/ppermute | solution.py:266
  50.6 1.3 %collective-permute-start.9 = (bf16[528,256]{1,0:T(8,128)(2,1)S(1)}, bf16[528,256]{1,0:T(8,128)(2,1)S(1)}, u32[]{:S(2)}, u32[]{:S(2)}) collective-permute-start(bf16[528,256]{1,0:T(8,128)(2,1)S(1)} %get-tuple-element.29.refs_4_.refs_2_), channel_id=1, source_target_pairs={{0,8},{8,16},{16,24},{24,32},{32,40},{40,48},{48,56},{56,64},{64,7... | collective-permute-start | bytes 811016 | tf_op jit(solution)/shard_map/ppermute | solution.py:437
  52.1 3.6 %next_heads.3 = (bf16[512,128]{1,0:T(8,128)(2,1)S(1)}, bf16[512,256]{1,0:T(8,128)(2,1)S(1)}, bf16[512,256]{1,0:T(8,128)(2,1)S(1)}) custom-call(bf16[512,128]{1,0:T(8,128)(2,1)S(1)} %attend.4.refs_4_.refs_0_, bf16[512,128]{1,0:T(8,128)(2,1)S(1)} %collective-permute-done.1.refs_1_, bf16[512,128]{1,0:T(8,128)(2,1)S(1)} %collective-permute-done.2.refs_2_, ...), custom_call_target="tpu_custom_call" | custom-call | flops 2952790016 | bytes 7864320 | tf_op jit(solution)/shard_map/next_heads/pallas_call | solution.py:357
  55.8 1.5 %attend.7.refs_0_ = bf16[512,128]{1,0:T(8,128)(2,1)S(1)} custom-call(bf16[512,128]{1,0:T(8,128)(2,1)S(1)} %get-tuple-element.32.refs_0_, bf16[512,256]{1,0:T(8,128)(2,1)S(1)} %get-tuple-element.31.refs_2_.refs_1_, bf16[528,256]{1,0:T(8,128)(2,1)S(1)} %get-tuple-element.29.refs_4_.refs_2_, f32[1,1024]{1,0:T(1,128)S(1)} %get-tuple-element.23.refs_3_.refs_11_, ...), custom_call_target="tpu_custom_call" | custom-call | flops 335544320 | bytes 524288 | tf_op jit(solution)/shard_map/attend/pallas_call | solution.py:250
  57.4 3.5 %collective-permute-start.14 = (bf16[512,128]{1,0:T(8,128)(2,1)S(1)}, bf16[512,128]{1,0:T(8,128)(2,1)S(1)}, u32[]{:S(2)}, u32[]{:S(2)}) collective-permute-start(bf16[512,128]{1,0:T(8,128)(2,1)S(1)} %attend.7.refs_0_), channel_id=1, source_target_pairs={{0,4},{1,5},{2,6},{3,7},{4,0},{5,1},{6,2},{7,3},{8,12},{9,13},{10,... | collective-permute-start | bytes 393224 | tf_op jit(solution)/shard_map/ppermute | solution.py:266
  61.0 1.5 %attend.6.refs_4_.refs_0_ = bf16[512,128]{1,0:T(8,128)(2,1)S(1)} custom-call(bf16[512,128]{1,0:T(8,128)(2,1)S(1)} %get-tuple-element.30.refs_0_, bf16[528,256]{1,0:T(8,128)(2,1)S(1)} %collective-permute-done.9.refs_1_, bf16[512,256]{1,0:T(8,128)(2,1)S(1)} %get-tuple-element.31.refs_2_.refs_1_, f32[1,1024]{1,0:T(1,128)S(1)} %get-tuple-element.23.refs_3_.refs_11_, ...), custom_call_target="tpu_custom_call" | custom-call | flops 335544320 | bytes 524288 | tf_op jit(solution)/shard_map/attend/pallas_call | solution.py:250
  62.5 0.8 collective-permute-done.13.refs_1_
  63.3 3.7 %collective-permute-done.14.refs_2_ = bf16[512,128]{1,0:T(8,128)(2,1)S(1)} collective-permute-done((bf16[512,128]{1,0:T(8,128)(2,1)S(1)}, bf16[512,128]{1,0:T(8,128)(2,1)S(1)}, u32[]{:S(2)}, u32[]{:S(2)}) %collective-permute-start.14) | collective-permute-done | bytes 131104 | tf_op jit(solution)/shard_map/ppermute | solution.py:266
  67.0 1.6 %collective-permute-start.16 = (bf16[4,512,128]{2,1,0:T(8,128)(2,1)S(1)}, bf16[4,512,128]{2,1,0:T(8,128)(2,1)S(1)}, u32[]{:S(2)}, u32[]{:S(2)}) collective-permute-start(bf16[4,512,128]{2,1,0:T(8,128)(2,1)S(1)} %stack.6), channel_id=1, source_target_pairs={{0,1},{1,0},{2,3},{3,2},{4,5},{5,4},{6,7},{7,6},{8,9},{9,8},{10,11... | collective-permute-start | bytes 1572872 | tf_op jit(solution)/shard_map/ppermute | solution.py:266
  68.6 3.3 %collective-permute-start.11 = (bf16[512,128]{1,0:T(8,128)(2,1)S(1)}, bf16[512,128]{1,0:T(8,128)(2,1)S(1)}, u32[]{:S(2)}, u32[]{:S(2)}) collective-permute-start(bf16[512,128]{1,0:T(8,128)(2,1)S(1)} %attend.6.refs_4_.refs_0_), channel_id=1, source_target_pairs={{0,4},{1,5},{2,6},{3,7},{4,0},{5,1},{6,2},{7,3},{8,12},{9,13},{10,... | collective-permute-start | bytes 393224 | tf_op jit(solution)/shard_map/ppermute | solution.py:266
  71.9 0.5 last.2.refs_4_.refs_7_
  72.4 2.4 %collective-permute-done.10.refs_1_ = bf16[512,128]{1,0:T(8,128)(2,1)S(1)} collective-permute-done((bf16[512,128]{1,0:T(8,128)(2,1)S(1)}, bf16[512,128]{1,0:T(8,128)(2,1)S(1)}, u32[]{:S(2)}, u32[]{:S(2)}) %collective-permute-start.10) | collective-permute-done | bytes 131104 | tf_op jit(solution)/shard_map/ppermute | solution.py:266
  74.7 3.4 %collective-permute-done.11.refs_2_ = bf16[512,128]{1,0:T(8,128)(2,1)S(1)} collective-permute-done((bf16[512,128]{1,0:T(8,128)(2,1)S(1)}, bf16[512,128]{1,0:T(8,128)(2,1)S(1)}, u32[]{:S(2)}, u32[]{:S(2)}) %collective-permute-start.11) | collective-permute-done | bytes 131104 | tf_op jit(solution)/shard_map/ppermute | solution.py:266
  78.2 1.1 %collective-permute-start.17 = (bf16[4,512,128]{2,1,0:T(8,128)(2,1)S(1)}, bf16[4,512,128]{2,1,0:T(8,128)(2,1)S(1)}, u32[]{:S(2)}, u32[]{:S(2)}) collective-permute-start(bf16[4,512,128]{2,1,0:T(8,128)(2,1)S(1)} %stack.7), channel_id=1, source_target_pairs={{0,1},{1,0},{2,3},{3,2},{4,5},{5,4},{6,7},{7,6},{8,9},{9,8},{10,11... | collective-permute-start | bytes 1572872 | tf_op jit(solution)/shard_map/ppermute | solution.py:266
  79.3 1.5 %collective-permute-done.17.refs_4_ = bf16[4,512,128]{2,1,0:T(8,128)(2,1)S(1)} collective-permute-done((bf16[4,512,128]{2,1,0:T(8,128)(2,1)S(1)}, bf16[4,512,128]{2,1,0:T(8,128)(2,1)S(1)}, u32[]{:S(2)}, u32[]{:S(2)}) %collective-permute-start.17) | collective-permute-done | bytes 524320 | tf_op jit(solution)/shard_map/ppermute | solution.py:266
  80.8 1.3 %last.3 = bf16[1024,256]{1,0:T(8,128)(2,1)} custom-call(bf16[512,128]{1,0:T(8,128)(2,1)S(1)} %attend.6.refs_4_.refs_0_, bf16[512,128]{1,0:T(8,128)(2,1)S(1)} %collective-permute-done.10.refs_1_, bf16[512,128]{1,0:T(8,128)(2,1)S(1)} %collective-permute-done.11.refs_2_, bf16[512,128]{1,0:T(8,128)(2,1)S(1)} %collective-permute-done.12.refs_3_, ...), custom_call_target="tpu_custom_call" | custom-call | flops 268435456 | bytes 1572864 | tf_op jit(solution)/shard_map/last/pallas_call | solution.py:396
  (29 shorter events, 0.5 us)
Async XLA Ops:
  0.0 19.8 %copy-start = (bf16[1024,2048]{1,0:T(8,128)(2,1)S(1)}, bf16[1024,2048]{1,0:T(8,128)(2,1)}, u32[]{:S(2)}) copy-start(bf16[1024,2048]{1,0:T(8,128)(2,1)} %refs_5_.8) | copy-start | bytes 12582916
  0.0 19.8 %copy-start.1 = (bf16[1024,2048]{1,0:T(8,128)(2,1)S(1)}, bf16[1024,2048]{1,0:T(8,128)(2,1)}, u32[]{:S(2)}) copy-start(bf16[1024,2048]{1,0:T(8,128)(2,1)} %refs_6_.9) | copy-start | bytes 12582916
  0.0 0.8 %copy-start.3 = (bf16[2,2048]{1,0:T(2,128)(2,1)S(1)}, bf16[2,2048]{1,0:T(2,128)(2,1)}, u32[]{:S(2)}) copy-start(bf16[2,2048]{1,0:T(2,128)(2,1)} %refs_1_.1) | copy-start | bytes 24580
  0.9 1.1 %copy-start.4 = (f32[2,2,257]{2,1,0:T(2,128)S(1)}, f32[2,2,257]{2,1,0:T(2,128)}, u32[]{:S(2)}) copy-start(f32[2,2,257]{2,1,0:T(2,128)} %refs_6_.6) | copy-start | bytes 12340
  2.0 1.2 %copy-start.5 = (s32[1024]{0:T(1024)S(1)}, s32[1024]{0:T(1024)}, u32[]{:S(2)}) copy-start(s32[1024]{0:T(1024)} %refs_5_.5) | copy-start | bytes 12292
  7.8 12.0 %collective-permute-start = (bf16[528,256]{1,0:T(8,128)(2,1)S(1)}, bf16[528,256]{1,0:T(8,128)(2,1)S(1)}, u32[]{:S(2)}, u32[]{:S(2)}) collective-permute-start(bf16[528,256]{1,0:T(8,128)(2,1)S(1)} %get-tuple-element.21.refs_2_), channel_id=1, source_target_pairs={{0,8},{8,16},{16,24},{24,32},{32,40},{40,48},{48,56},{56,64},{64,7... | collective-permute-start | bytes 811016 | tf_op jit(solution)/shard_map/ppermute | solution.py:422
  14.6 6.7 %collective-permute-start.4 = (bf16[512,128]{1,0:T(8,128)(2,1)S(1)}, bf16[512,128]{1,0:T(8,128)(2,1)S(1)}, u32[]{:S(2)}, u32[]{:S(2)}) collective-permute-start(bf16[512,128]{1,0:T(8,128)(2,1)S(1)} %attend.5.refs_0_), channel_id=1, source_target_pairs={{0,2},{1,3},{2,4},{3,5},{4,6},{5,7},{6,0},{7,1},{8,10},{9,11},{10,... | collective-permute-start | bytes 393224 | tf_op jit(solution)/shard_map/ppermute | solution.py:266
  16.1 7.9 %collective-permute-start.5 = (bf16[512,128]{1,0:T(8,128)(2,1)S(1)}, bf16[512,128]{1,0:T(8,128)(2,1)S(1)}, u32[]{:S(2)}, u32[]{:S(2)}) collective-permute-start(bf16[512,128]{1,0:T(8,128)(2,1)S(1)} %attend.5.refs_0_), channel_id=1, source_target_pairs={{0,4},{1,5},{2,6},{3,7},{4,0},{5,1},{6,2},{7,3},{8,12},{9,13},{10,... | collective-permute-start | bytes 393224 | tf_op jit(solution)/shard_map/ppermute | solution.py:266
  18.8 5.2 %collective-permute-start.6 = (bf16[512,128]{1,0:T(8,128)(2,1)S(1)}, bf16[512,128]{1,0:T(8,128)(2,1)S(1)}, u32[]{:S(2)}, u32[]{:S(2)}) collective-permute-start(bf16[512,128]{1,0:T(8,128)(2,1)S(1)} %attend.5.refs_0_), channel_id=1, source_target_pairs={{0,6},{1,7},{2,0},{3,1},{4,2},{5,3},{6,4},{7,5},{8,14},{9,15},{10,... | collective-permute-start | bytes 393224 | tf_op jit(solution)/shard_map/ppermute | solution.py:266
  24.0 19.1 %collective-permute-start.7 = (bf16[4,512,128]{2,1,0:T(8,128)(2,1)S(1)}, bf16[4,512,128]{2,1,0:T(8,128)(2,1)S(1)}, u32[]{:S(2)}, u32[]{:S(2)}) collective-permute-start(bf16[4,512,128]{2,1,0:T(8,128)(2,1)S(1)} %stack.4), channel_id=1, source_target_pairs={{0,1},{1,0},{2,3},{3,2},{4,5},{5,4},{6,7},{7,6},{8,9},{9,8},{10,11... | collective-permute-start | bytes 1572872 | tf_op jit(solution)/shard_map/ppermute | solution.py:266
  39.9 6.9 %collective-permute-start.1 = (bf16[512,128]{1,0:T(8,128)(2,1)S(1)}, bf16[512,128]{1,0:T(8,128)(2,1)S(1)}, u32[]{:S(2)}, u32[]{:S(2)}) collective-permute-start(bf16[512,128]{1,0:T(8,128)(2,1)S(1)} %attend.4.refs_4_.refs_0_), channel_id=1, source_target_pairs={{0,2},{1,3},{2,4},{3,5},{4,6},{5,7},{6,0},{7,1},{8,10},{9,11},{10,... | collective-permute-start | bytes 393224 | tf_op jit(solution)/shard_map/ppermute | solution.py:266
  40.2 9.2 %collective-permute-start.2 = (bf16[512,128]{1,0:T(8,128)(2,1)S(1)}, bf16[512,128]{1,0:T(8,128)(2,1)S(1)}, u32[]{:S(2)}, u32[]{:S(2)}) collective-permute-start(bf16[512,128]{1,0:T(8,128)(2,1)S(1)} %attend.4.refs_4_.refs_0_), channel_id=1, source_target_pairs={{0,4},{1,5},{2,6},{3,7},{4,0},{5,1},{6,2},{7,3},{8,12},{9,13},{10,... | collective-permute-start | bytes 393224 | tf_op jit(solution)/shard_map/ppermute | solution.py:266
  43.1 6.3 %collective-permute-start.3 = (bf16[512,128]{1,0:T(8,128)(2,1)S(1)}, bf16[512,128]{1,0:T(8,128)(2,1)S(1)}, u32[]{:S(2)}, u32[]{:S(2)}) collective-permute-start(bf16[512,128]{1,0:T(8,128)(2,1)S(1)} %attend.4.refs_4_.refs_0_), channel_id=1, source_target_pairs={{0,6},{1,7},{2,0},{3,1},{4,2},{5,3},{6,4},{7,5},{8,14},{9,15},{10,... | collective-permute-start | bytes 393224 | tf_op jit(solution)/shard_map/ppermute | solution.py:266
  49.4 11.6 %copy-start.2 = (bf16[1024,256]{1,0:T(8,128)(2,1)S(1)}, bf16[1024,256]{1,0:T(8,128)(2,1)}, u32[]{:S(2)}) copy-start(bf16[1024,256]{1,0:T(8,128)(2,1)} %refs_6_.11) | copy-start | bytes 1572868
  49.4 2.7 %collective-permute-start.8 = (bf16[4,512,128]{2,1,0:T(8,128)(2,1)S(1)}, bf16[4,512,128]{2,1,0:T(8,128)(2,1)S(1)}, u32[]{:S(2)}, u32[]{:S(2)}) collective-permute-start(bf16[4,512,128]{2,1,0:T(8,128)(2,1)S(1)} %stack.5), channel_id=1, source_target_pairs={{0,1},{1,0},{2,3},{3,2},{4,5},{5,4},{6,7},{7,6},{8,9},{9,8},{10,11... | collective-permute-start | bytes 1572872 | tf_op jit(solution)/shard_map/ppermute | solution.py:266
  50.6 10.4 %collective-permute-start.9 = (bf16[528,256]{1,0:T(8,128)(2,1)S(1)}, bf16[528,256]{1,0:T(8,128)(2,1)S(1)}, u32[]{:S(2)}, u32[]{:S(2)}) collective-permute-start(bf16[528,256]{1,0:T(8,128)(2,1)S(1)} %get-tuple-element.29.refs_4_.refs_2_), channel_id=1, source_target_pairs={{0,8},{8,16},{16,24},{24,32},{32,40},{40,48},{48,56},{56,64},{64,7... | collective-permute-start | bytes 811016 | tf_op jit(solution)/shard_map/ppermute | solution.py:437
  57.3 6.0 %collective-permute-start.13 = (bf16[512,128]{1,0:T(8,128)(2,1)S(1)}, bf16[512,128]{1,0:T(8,128)(2,1)S(1)}, u32[]{:S(2)}, u32[]{:S(2)}) collective-permute-start(bf16[512,128]{1,0:T(8,128)(2,1)S(1)} %attend.7.refs_0_), channel_id=1, source_target_pairs={{0,2},{1,3},{2,4},{3,5},{4,6},{5,7},{6,0},{7,1},{8,10},{9,11},{10,... | collective-permute-start | bytes 393224 | tf_op jit(solution)/shard_map/ppermute | solution.py:266
  57.4 9.6 %collective-permute-start.14 = (bf16[512,128]{1,0:T(8,128)(2,1)S(1)}, bf16[512,128]{1,0:T(8,128)(2,1)S(1)}, u32[]{:S(2)}, u32[]{:S(2)}) collective-permute-start(bf16[512,128]{1,0:T(8,128)(2,1)S(1)} %attend.7.refs_0_), channel_id=1, source_target_pairs={{0,4},{1,5},{2,6},{3,7},{4,0},{5,1},{6,2},{7,3},{8,12},{9,13},{10,... | collective-permute-start | bytes 393224 | tf_op jit(solution)/shard_map/ppermute | solution.py:266
  61.0 6.0 %collective-permute-start.15 = (bf16[512,128]{1,0:T(8,128)(2,1)S(1)}, bf16[512,128]{1,0:T(8,128)(2,1)S(1)}, u32[]{:S(2)}, u32[]{:S(2)}) collective-permute-start(bf16[512,128]{1,0:T(8,128)(2,1)S(1)} %attend.7.refs_0_), channel_id=1, source_target_pairs={{0,6},{1,7},{2,0},{3,1},{4,2},{5,3},{6,4},{7,5},{8,14},{9,15},{10,... | collective-permute-start | bytes 393224 | tf_op jit(solution)/shard_map/ppermute | solution.py:266
  67.0 4.8 %collective-permute-start.16 = (bf16[4,512,128]{2,1,0:T(8,128)(2,1)S(1)}, bf16[4,512,128]{2,1,0:T(8,128)(2,1)S(1)}, u32[]{:S(2)}, u32[]{:S(2)}) collective-permute-start(bf16[4,512,128]{2,1,0:T(8,128)(2,1)S(1)} %stack.6), channel_id=1, source_target_pairs={{0,1},{1,0},{2,3},{3,2},{4,5},{5,4},{6,7},{7,6},{8,9},{9,8},{10,11... | collective-permute-start | bytes 1572872 | tf_op jit(solution)/shard_map/ppermute | solution.py:266
  68.6 6.1 %collective-permute-start.10 = (bf16[512,128]{1,0:T(8,128)(2,1)S(1)}, bf16[512,128]{1,0:T(8,128)(2,1)S(1)}, u32[]{:S(2)}, u32[]{:S(2)}) collective-permute-start(bf16[512,128]{1,0:T(8,128)(2,1)S(1)} %attend.6.refs_4_.refs_0_), channel_id=1, source_target_pairs={{0,2},{1,3},{2,4},{3,5},{4,6},{5,7},{6,0},{7,1},{8,10},{9,11},{10,... | collective-permute-start | bytes 393224 | tf_op jit(solution)/shard_map/ppermute | solution.py:266
  68.6 9.5 %collective-permute-start.11 = (bf16[512,128]{1,0:T(8,128)(2,1)S(1)}, bf16[512,128]{1,0:T(8,128)(2,1)S(1)}, u32[]{:S(2)}, u32[]{:S(2)}) collective-permute-start(bf16[512,128]{1,0:T(8,128)(2,1)S(1)} %attend.6.refs_4_.refs_0_), channel_id=1, source_target_pairs={{0,4},{1,5},{2,6},{3,7},{4,0},{5,1},{6,2},{7,3},{8,12},{9,13},{10,... | collective-permute-start | bytes 393224 | tf_op jit(solution)/shard_map/ppermute | solution.py:266
  71.9 6.3 %collective-permute-start.12 = (bf16[512,128]{1,0:T(8,128)(2,1)S(1)}, bf16[512,128]{1,0:T(8,128)(2,1)S(1)}, u32[]{:S(2)}, u32[]{:S(2)}) collective-permute-start(bf16[512,128]{1,0:T(8,128)(2,1)S(1)} %attend.6.refs_4_.refs_0_), channel_id=1, source_target_pairs={{0,6},{1,7},{2,0},{3,1},{4,2},{5,3},{6,4},{7,5},{8,14},{9,15},{10,... | collective-permute-start | bytes 393224 | tf_op jit(solution)/shard_map/ppermute | solution.py:266
  78.2 2.7 %collective-permute-start.17 = (bf16[4,512,128]{2,1,0:T(8,128)(2,1)S(1)}, bf16[4,512,128]{2,1,0:T(8,128)(2,1)S(1)}, u32[]{:S(2)}, u32[]{:S(2)}) collective-permute-start(bf16[4,512,128]{2,1,0:T(8,128)(2,1)S(1)} %stack.7), channel_id=1, source_target_pairs={{0,1},{1,0},{2,3},{3,2},{4,5},{5,4},{6,7},{7,6},{8,9},{9,8},{10,11... | collective-permute-start | bytes 1572872 | tf_op jit(solution)/shard_map/ppermute | solution.py:266

commit v3 on v2

--- a/solution.py
+++ b/solution.py
@@ -116,7 +116,9 @@
     half_rows = row_count // 2
     depth, width = wq.shape[1:]
     items = rel_table.shape[0] * rel_table.shape[1]
-    hbm = pl.BlockSpec(memory_space=pl.ANY)
+    hbm = pl.BlockSpec(memory_space=pltpu.HBM)
+    args = [tokens, gains, wq, wk, wv, doc_ids, rel_table]
+    args = [pltpu.with_memory_space_constraint(array, pltpu.HBM) for array in args]
     return pl.pallas_call(
         functools.partial(heads_kernel, q_scale, block_rows),
         in_specs=[hbm] * 7,
@@ -141,7 +143,7 @@
         cost_estimate=cost(6 * row_count * depth * width, 2 * depth * (row_count + 3 * width)),
         compiler_params=pltpu.CompilerParams(vmem_limit_bytes=FIRST_VMEM_LIMIT),
         name="heads",
-    )(tokens, gains, wq, wk, wv, doc_ids, rel_table)
+    )(*args)
 
 
 def near_bias(table_ref, out_ref):
@@ -252,7 +254,7 @@
         in_specs=whole(5 + len(ahead)),
         out_specs=pl.BlockSpec(memory_space=pltpu.VMEM),
         out_shape=jax.ShapeDtypeStruct((half_rows, width), BF16),
-        cost_estimate=cost(8 * half_rows * BAND * width, 8 * half_rows * width, half_rows * BAND * 2),
+        cost_estimate=cost(400 * half_rows * BAND * width, 8 * half_rows * width, half_rows * BAND * 2),
         compiler_params=pltpu.CompilerParams(vmem_limit_bytes=VMEM_LIMIT),
         name="attend",
     )(queries, lo, hi, docs, biases, *ahead)

time: 82.4 us -> 79.5 us (0.965)
  local copies, waits for them, and re-layouts: 3.18 us -> 0.02 us
    unnamed x12 -> x6, local copies, waits for them, and re-layouts: 3.18 us -> 0.02 us
  transfers between devices with their start and end apart: 18 -> 18, of which waited for: 8 -> 8; matrix products, arithmetic and copies ran while one was open for 0% -> 0% of each run, Pallas kernels for 17% -> 18%
where the time goes in v3:
time: 79.5 us; the launch traced here: 79.3 us
  starting transfers between devices  41.6 us (52%)
  Pallas kernels  20.4 us (26%)
  waiting for transfers between devices  17.2 us (22%)
    ppermute x16, starting transfers between devices, moved(): lax.ppermute(array, 'tp', [(2 * x + core, 2 * ((x + by) % chips) + (1 - c...  35.1 us
    ppermute x16, waiting for transfers between devices, moved(): lax.ppermute(array, 'tp', [(2 * x + core, 2 * ((x + by) % chips) + (1 - c...  17.2 us
    pallas_call x2, Pallas kernels, next_heads(): pl.pallas_call(functools.partial(next_kernel, q_scale, block_rows, len(bl...  7.34 us
    ppermute x2, starting transfers between devices, shards(): far = lax.ppermute(kv_late, 'sp', onward)  6.58 us
    pallas_call x4, Pallas kernels, attention(): pl.pallas_call(functools.partial(attention_kernel, head_width, layer, fro...  6.09 us
    pallas_call x1, Pallas kernels, heads(): pl.pallas_call(functools.partial(heads_kernel, q_scale, block_rows), in_s...  5 us
    pallas_call x2, Pallas kernels, last_update(): pl.pallas_call(functools.partial(last_kernel, len(blocks)), in_specs=whol...  1.79 us
  transfers between devices with their start and end apart: 18, of which 8 were waited for; matrix products, arithmetic and copies ran while one was open for 0% of the time, Pallas kernels for 18%

profile of v3, /device:TPU:33, one launch (start us, length us, event | category | flops | bytes accessed | tf_op | source)
XLA Modules:
  0.0 79.3 jit_solution(2599362715867859206)
XLA Ops:
  0.0 5.0 %heads.1 = (bf16[1024,128]{1,0:T(8,128)(2,1)S(1)}, bf16[512,256]{1,0:T(8,128)(2,1)S(1)}, bf16[528,256]{1,0:T(8,128)(2,1)S(1)}, f32[1,1024]{1,0:T(1,128)S(1)}, f3...) custom-call(bf16[1024,2048]{1,0:T(8,128)(2,1)} %refs_5_.8, ...), custom_call_target="tpu_custom_call" | custom-call | flops 1610612736 | bytes 5767168 | tf_op jit(solution)/shard_map/heads/pallas_call | solution.py:122
  5.0 5.3 %collective-permute-start = (bf16[528,256]{1,0:T(8,128)(2,1)S(1)}, bf16[528,256]{1,0:T(8,128)(2,1)S(1)}, u32[]{:S(2)}, u32[]{:S(2)}) collective-permute-start(bf16[528,256]{1,0:T(8,128)(2,1)S(1)} %get-tuple-element.21.refs_2_), channel_id=1, source_target_pairs={{0,8},{8,16},{16,24},{24,32},{32,40},{40,48},{48,56},{56,64},{64,7... | collective-permute-start | bytes 811016 | tf_op jit(solution)/shard_map/ppermute | solution.py:424
  10.3 0.0 copy-start
  10.3 1.5 %attend.5.refs_0_ = bf16[512,128]{1,0:T(8,128)(2,1)S(1)} custom-call(bf16[1024,128]{1,0:T(8,128)(2,1)S(1)} %get-tuple-element.20.refs_0_, bf16[512,256]{1,0:T(8,128)(2,1)S(1)} %get-tuple-element.22.refs_2_.refs_1_, bf16[528,256]{1,0:T(8,128)(2,1)S(1)} %get-tuple-element.21.refs_2_, f32[1,1024]{1,0:T(1,128)S(1)} %get-tuple-element.23.refs_3_.refs_11_, ...), custom_call_target="tpu_custom_call" | custom-call | flops 16777216000 | bytes 524288 | tf_op jit(solution)/shard_map/attend/pallas_call | solution.py:252
  11.8 1.5 %collective-permute-start.4 = (bf16[512,128]{1,0:T(8,128)(2,1)S(1)}, bf16[512,128]{1,0:T(8,128)(2,1)S(1)}, u32[]{:S(2)}, u32[]{:S(2)}) collective-permute-start(bf16[512,128]{1,0:T(8,128)(2,1)S(1)} %attend.5.refs_0_), channel_id=1, source_target_pairs={{0,2},{1,3},{2,4},{3,5},{4,6},{5,7},{6,0},{7,1},{8,10},{9,11},{10,... | collective-permute-start | bytes 393224 | tf_op jit(solution)/shard_map/ppermute | solution.py:268
  13.3 2.7 %collective-permute-start.5 = (bf16[512,128]{1,0:T(8,128)(2,1)S(1)}, bf16[512,128]{1,0:T(8,128)(2,1)S(1)}, u32[]{:S(2)}, u32[]{:S(2)}) collective-permute-start(bf16[512,128]{1,0:T(8,128)(2,1)S(1)} %attend.5.refs_0_), channel_id=1, source_target_pairs={{0,4},{1,5},{2,6},{3,7},{4,0},{5,1},{6,2},{7,3},{8,12},{9,13},{10,... | collective-permute-start | bytes 393224 | tf_op jit(solution)/shard_map/ppermute | solution.py:268
  16.0 1.0 %collective-permute-start.6 = (bf16[512,128]{1,0:T(8,128)(2,1)S(1)}, bf16[512,128]{1,0:T(8,128)(2,1)S(1)}, u32[]{:S(2)}, u32[]{:S(2)}) collective-permute-start(bf16[512,128]{1,0:T(8,128)(2,1)S(1)} %attend.5.refs_0_), channel_id=1, source_target_pairs={{0,6},{1,7},{2,0},{3,1},{4,2},{5,3},{6,4},{7,5},{8,14},{9,15},{10,... | collective-permute-start | bytes 393224 | tf_op jit(solution)/shard_map/ppermute | solution.py:268
  17.1 1.5 %attend.4.refs_4_.refs_0_ = bf16[512,128]{1,0:T(8,128)(2,1)S(1)} custom-call(bf16[1024,128]{1,0:T(8,128)(2,1)S(1)} %get-tuple-element.20.refs_0_, bf16[528,256]{1,0:T(8,128)(2,1)S(1)} %collective-permute-done.refs_1_, bf16[512,256]{1,0:T(8,128)(2,1)S(1)} %get-tuple-element.22.refs_2_.refs_1_, f32[1,1024]{1,0:T(1,128)S(1)} %get-tuple-element.23.refs_3_.refs_11_, ...), custom_call_target="tpu_custom_call" | custom-call | flops 16777216000 | bytes 524288 | tf_op jit(solution)/shard_map/attend/pallas_call | solution.py:252
  18.6 2.6 %collective-permute-done.5.refs_2_ = bf16[512,128]{1,0:T(8,128)(2,1)S(1)} collective-permute-done((bf16[512,128]{1,0:T(8,128)(2,1)S(1)}, bf16[512,128]{1,0:T(8,128)(2,1)S(1)}, u32[]{:S(2)}, u32[]{:S(2)}) %collective-permute-start.5) | collective-permute-done | bytes 131104 | tf_op jit(solution)/shard_map/ppermute | solution.py:268
  21.2 15.8 %collective-permute-start.7 = (bf16[4,512,128]{2,1,0:T(8,128)(2,1)S(1)}, bf16[4,512,128]{2,1,0:T(8,128)(2,1)S(1)}, u32[]{:S(2)}, u32[]{:S(2)}) collective-permute-start(bf16[4,512,128]{2,1,0:T(8,128)(2,1)S(1)} %stack.4), channel_id=1, source_target_pairs={{0,1},{1,0},{2,3},{3,2},{4,5},{5,4},{6,7},{7,6},{8,9},{9,8},{10,11... | collective-permute-start | bytes 1572872 | tf_op jit(solution)/shard_map/ppermute | solution.py:268
  37.1 0.3 collective-permute-start.1
  37.4 2.9 %collective-permute-start.2 = (bf16[512,128]{1,0:T(8,128)(2,1)S(1)}, bf16[512,128]{1,0:T(8,128)(2,1)S(1)}, u32[]{:S(2)}, u32[]{:S(2)}) collective-permute-start(bf16[512,128]{1,0:T(8,128)(2,1)S(1)} %attend.4.refs_4_.refs_0_), channel_id=1, source_target_pairs={{0,4},{1,5},{2,6},{3,7},{4,0},{5,1},{6,2},{7,3},{8,12},{9,13},{10,... | collective-permute-start | bytes 393224 | tf_op jit(solution)/shard_map/ppermute | solution.py:268
  40.3 3.7 %next_heads.2 = (bf16[512,128]{1,0:T(8,128)(2,1)S(1)}, bf16[528,256]{1,0:T(8,128)(2,1)S(1)}, bf16[512,256]{1,0:T(8,128)(2,1)S(1)}) custom-call(bf16[512,128]{1,0:T(8,128)(2,1)S(1)} %attend.5.refs_0_, bf16[512,128]{1,0:T(8,128)(2,1)S(1)} %collective-permute-done.4.refs_1_, bf16[512,128]{1,0:T(8,128)(2,1)S(1)} %collective-permute-done.5.refs_2_, ...), custom_call_target="tpu_custom_call" | custom-call | flops 2952790016 | bytes 7864320 | tf_op jit(solution)/shard_map/next_heads/pallas_call | solution.py:359
  44.0 2.6 %collective-permute-done.2.refs_2_ = bf16[512,128]{1,0:T(8,128)(2,1)S(1)} collective-permute-done((bf16[512,128]{1,0:T(8,128)(2,1)S(1)}, bf16[512,128]{1,0:T(8,128)(2,1)S(1)}, u32[]{:S(2)}, u32[]{:S(2)}) %collective-permute-start.2) | collective-permute-done | bytes 131104 | tf_op jit(solution)/shard_map/ppermute | solution.py:268
  46.6 1.1 %collective-permute-start.8 = (bf16[4,512,128]{2,1,0:T(8,128)(2,1)S(1)}, bf16[4,512,128]{2,1,0:T(8,128)(2,1)S(1)}, u32[]{:S(2)}, u32[]{:S(2)}) collective-permute-start(bf16[4,512,128]{2,1,0:T(8,128)(2,1)S(1)} %stack.5), channel_id=1, source_target_pairs={{0,1},{1,0},{2,3},{3,2},{4,5},{5,4},{6,7},{7,6},{8,9},{9,8},{10,11... | collective-permute-start | bytes 1572872 | tf_op jit(solution)/shard_map/ppermute | solution.py:268
  47.8 1.3 %collective-permute-start.9 = (bf16[528,256]{1,0:T(8,128)(2,1)S(1)}, bf16[528,256]{1,0:T(8,128)(2,1)S(1)}, u32[]{:S(2)}, u32[]{:S(2)}) collective-permute-start(bf16[528,256]{1,0:T(8,128)(2,1)S(1)} %get-tuple-element.29.refs_4_.refs_2_), channel_id=1, source_target_pairs={{0,8},{8,16},{16,24},{24,32},{32,40},{40,48},{48,56},{56,64},{64,7... | collective-permute-start | bytes 811016 | tf_op jit(solution)/shard_map/ppermute | solution.py:439
  49.1 0.2 collective-permute-done.8.refs_4_
  49.3 3.7 %next_heads.3 = (bf16[512,128]{1,0:T(8,128)(2,1)S(1)}, bf16[512,256]{1,0:T(8,128)(2,1)S(1)}, bf16[512,256]{1,0:T(8,128)(2,1)S(1)}) custom-call(bf16[512,128]{1,0:T(8,128)(2,1)S(1)} %attend.4.refs_4_.refs_0_, bf16[512,128]{1,0:T(8,128)(2,1)S(1)} %collective-permute-done.1.refs_1_, bf16[512,128]{1,0:T(8,128)(2,1)S(1)} %collective-permute-done.2.refs_2_, ...), custom_call_target="tpu_custom_call" | custom-call | flops 2952790016 | bytes 7864320 | tf_op jit(solution)/shard_map/next_heads/pallas_call | solution.py:359
  53.0 1.5 %attend.7.refs_0_ = bf16[512,128]{1,0:T(8,128)(2,1)S(1)} custom-call(bf16[512,128]{1,0:T(8,128)(2,1)S(1)} %get-tuple-element.32.refs_0_, bf16[512,256]{1,0:T(8,128)(2,1)S(1)} %get-tuple-element.31.refs_2_.refs_1_, bf16[528,256]{1,0:T(8,128)(2,1)S(1)} %get-tuple-element.29.refs_4_.refs_2_, f32[1,1024]{1,0:T(1,128)S(1)} %get-tuple-element.23.refs_3_.refs_11_, ...), custom_call_target="tpu_custom_call" | custom-call | flops 16777216000 | bytes 524288 | tf_op jit(solution)/shard_map/attend/pallas_call | solution.py:252
  54.5 0.1 collective-permute-start.13
  54.7 3.5 %collective-permute-start.14 = (bf16[512,128]{1,0:T(8,128)(2,1)S(1)}, bf16[512,128]{1,0:T(8,128)(2,1)S(1)}, u32[]{:S(2)}, u32[]{:S(2)}) collective-permute-start(bf16[512,128]{1,0:T(8,128)(2,1)S(1)} %attend.7.refs_0_), channel_id=1, source_target_pairs={{0,4},{1,5},{2,6},{3,7},{4,0},{5,1},{6,2},{7,3},{8,12},{9,13},{10,... | collective-permute-start | bytes 393224 | tf_op jit(solution)/shard_map/ppermute | solution.py:268
  58.2 1.5 %attend.6.refs_4_.refs_0_ = bf16[512,128]{1,0:T(8,128)(2,1)S(1)} custom-call(bf16[512,128]{1,0:T(8,128)(2,1)S(1)} %get-tuple-element.30.refs_0_, bf16[528,256]{1,0:T(8,128)(2,1)S(1)} %collective-permute-done.9.refs_1_, bf16[512,256]{1,0:T(8,128)(2,1)S(1)} %get-tuple-element.31.refs_2_.refs_1_, f32[1,1024]{1,0:T(1,128)S(1)} %get-tuple-element.23.refs_3_.refs_11_, ...), custom_call_target="tpu_custom_call" | custom-call | flops 16777216000 | bytes 524288 | tf_op jit(solution)/shard_map/attend/pallas_call | solution.py:252
  59.7 0.8 collective-permute-done.13.refs_1_
  60.5 3.7 %collective-permute-done.14.refs_2_ = bf16[512,128]{1,0:T(8,128)(2,1)S(1)} collective-permute-done((bf16[512,128]{1,0:T(8,128)(2,1)S(1)}, bf16[512,128]{1,0:T(8,128)(2,1)S(1)}, u32[]{:S(2)}, u32[]{:S(2)}) %collective-permute-start.14) | collective-permute-done | bytes 131104 | tf_op jit(solution)/shard_map/ppermute | solution.py:268
  64.3 1.6 %collective-permute-start.16 = (bf16[4,512,128]{2,1,0:T(8,128)(2,1)S(1)}, bf16[4,512,128]{2,1,0:T(8,128)(2,1)S(1)}, u32[]{:S(2)}, u32[]{:S(2)}) collective-permute-start(bf16[4,512,128]{2,1,0:T(8,128)(2,1)S(1)} %stack.6), channel_id=1, source_target_pairs={{0,1},{1,0},{2,3},{3,2},{4,5},{5,4},{6,7},{7,6},{8,9},{9,8},{10,11... | collective-permute-start | bytes 1572872 | tf_op jit(solution)/shard_map/ppermute | solution.py:268
  65.8 3.3 %collective-permute-start.11 = (bf16[512,128]{1,0:T(8,128)(2,1)S(1)}, bf16[512,128]{1,0:T(8,128)(2,1)S(1)}, u32[]{:S(2)}, u32[]{:S(2)}) collective-permute-start(bf16[512,128]{1,0:T(8,128)(2,1)S(1)} %attend.6.refs_4_.refs_0_), channel_id=1, source_target_pairs={{0,4},{1,5},{2,6},{3,7},{4,0},{5,1},{6,2},{7,3},{8,12},{9,13},{10,... | collective-permute-start | bytes 393224 | tf_op jit(solution)/shard_map/ppermute | solution.py:268
  69.1 0.5 last.2.refs_4_.refs_7_
  69.6 2.4 %collective-permute-done.10.refs_1_ = bf16[512,128]{1,0:T(8,128)(2,1)S(1)} collective-permute-done((bf16[512,128]{1,0:T(8,128)(2,1)S(1)}, bf16[512,128]{1,0:T(8,128)(2,1)S(1)}, u32[]{:S(2)}, u32[]{:S(2)}) %collective-permute-start.10) | collective-permute-done | bytes 131104 | tf_op jit(solution)/shard_map/ppermute | solution.py:268
  72.0 3.4 %collective-permute-done.11.refs_2_ = bf16[512,128]{1,0:T(8,128)(2,1)S(1)} collective-permute-done((bf16[512,128]{1,0:T(8,128)(2,1)S(1)}, bf16[512,128]{1,0:T(8,128)(2,1)S(1)}, u32[]{:S(2)}, u32[]{:S(2)}) %collective-permute-start.11) | collective-permute-done | bytes 131104 | tf_op jit(solution)/shard_map/ppermute | solution.py:268
  75.4 1.1 %collective-permute-start.17 = (bf16[4,512,128]{2,1,0:T(8,128)(2,1)S(1)}, bf16[4,512,128]{2,1,0:T(8,128)(2,1)S(1)}, u32[]{:S(2)}, u32[]{:S(2)}) collective-permute-start(bf16[4,512,128]{2,1,0:T(8,128)(2,1)S(1)} %stack.7), channel_id=1, source_target_pairs={{0,1},{1,0},{2,3},{3,2},{4,5},{5,4},{6,7},{7,6},{8,9},{9,8},{10,11... | collective-permute-start | bytes 1572872 | tf_op jit(solution)/shard_map/ppermute | solution.py:268
  76.5 1.5 %collective-permute-done.17.refs_4_ = bf16[4,512,128]{2,1,0:T(8,128)(2,1)S(1)} collective-permute-done((bf16[4,512,128]{2,1,0:T(8,128)(2,1)S(1)}, bf16[4,512,128]{2,1,0:T(8,128)(2,1)S(1)}, u32[]{:S(2)}, u32[]{:S(2)}) %collective-permute-start.17) | collective-permute-done | bytes 524320 | tf_op jit(solution)/shard_map/ppermute | solution.py:268
  78.1 1.3 %last.3 = bf16[1024,256]{1,0:T(8,128)(2,1)} custom-call(bf16[512,128]{1,0:T(8,128)(2,1)S(1)} %attend.6.refs_4_.refs_0_, bf16[512,128]{1,0:T(8,128)(2,1)S(1)} %collective-permute-done.10.refs_1_, bf16[512,128]{1,0:T(8,128)(2,1)S(1)} %collective-permute-done.11.refs_2_, bf16[512,128]{1,0:T(8,128)(2,1)S(1)} %collective-permute-done.12.refs_3_, ...), custom_call_target="tpu_custom_call" | custom-call | flops 268435456 | bytes 1572864 | tf_op jit(solution)/shard_map/last/pallas_call | solution.py:398
  (23 shorter events, 0.2 us)
Async XLA Ops:
  5.0 12.0 %collective-permute-start = (bf16[528,256]{1,0:T(8,128)(2,1)S(1)}, bf16[528,256]{1,0:T(8,128)(2,1)S(1)}, u32[]{:S(2)}, u32[]{:S(2)}) collective-permute-start(bf16[528,256]{1,0:T(8,128)(2,1)S(1)} %get-tuple-element.21.refs_2_), channel_id=1, source_target_pairs={{0,8},{8,16},{16,24},{24,32},{32,40},{40,48},{48,56},{56,64},{64,7... | collective-permute-start | bytes 811016 | tf_op jit(solution)/shard_map/ppermute | solution.py:424
  10.3 6.8 %copy-start = (bf16[1024,2048]{1,0:T(8,128)(2,1)S(1)}, bf16[1024,2048]{1,0:T(8,128)(2,1)}, u32[]{:S(2)}) copy-start(bf16[1024,2048]{1,0:T(8,128)(2,1)} %refs_5_.8) | copy-start | bytes 12582916
  10.3 6.8 %copy-start.1 = (bf16[1024,2048]{1,0:T(8,128)(2,1)S(1)}, bf16[1024,2048]{1,0:T(8,128)(2,1)}, u32[]{:S(2)}) copy-start(bf16[1024,2048]{1,0:T(8,128)(2,1)} %refs_6_.9) | copy-start | bytes 12582916
  11.8 6.7 %collective-permute-start.4 = (bf16[512,128]{1,0:T(8,128)(2,1)S(1)}, bf16[512,128]{1,0:T(8,128)(2,1)S(1)}, u32[]{:S(2)}, u32[]{:S(2)}) collective-permute-start(bf16[512,128]{1,0:T(8,128)(2,1)S(1)} %attend.5.refs_0_), channel_id=1, source_target_pairs={{0,2},{1,3},{2,4},{3,5},{4,6},{5,7},{6,0},{7,1},{8,10},{9,11},{10,... | collective-permute-start | bytes 393224 | tf_op jit(solution)/shard_map/ppermute | solution.py:268
  13.3 7.9 %collective-permute-start.5 = (bf16[512,128]{1,0:T(8,128)(2,1)S(1)}, bf16[512,128]{1,0:T(8,128)(2,1)S(1)}, u32[]{:S(2)}, u32[]{:S(2)}) collective-permute-start(bf16[512,128]{1,0:T(8,128)(2,1)S(1)} %attend.5.refs_0_), channel_id=1, source_target_pairs={{0,4},{1,5},{2,6},{3,7},{4,0},{5,1},{6,2},{7,3},{8,12},{9,13},{10,... | collective-permute-start | bytes 393224 | tf_op jit(solution)/shard_map/ppermute | solution.py:268
  16.0 5.2 %collective-permute-start.6 = (bf16[512,128]{1,0:T(8,128)(2,1)S(1)}, bf16[512,128]{1,0:T(8,128)(2,1)S(1)}, u32[]{:S(2)}, u32[]{:S(2)}) collective-permute-start(bf16[512,128]{1,0:T(8,128)(2,1)S(1)} %attend.5.refs_0_), channel_id=1, source_target_pairs={{0,6},{1,7},{2,0},{3,1},{4,2},{5,3},{6,4},{7,5},{8,14},{9,15},{10,... | collective-permute-start | bytes 393224 | tf_op jit(solution)/shard_map/ppermute | solution.py:268
  21.2 19.1 %collective-permute-start.7 = (bf16[4,512,128]{2,1,0:T(8,128)(2,1)S(1)}, bf16[4,512,128]{2,1,0:T(8,128)(2,1)S(1)}, u32[]{:S(2)}, u32[]{:S(2)}) collective-permute-start(bf16[4,512,128]{2,1,0:T(8,128)(2,1)S(1)} %stack.4), channel_id=1, source_target_pairs={{0,1},{1,0},{2,3},{3,2},{4,5},{5,4},{6,7},{7,6},{8,9},{9,8},{10,11... | collective-permute-start | bytes 1572872 | tf_op jit(solution)/shard_map/ppermute | solution.py:268
  37.1 6.9 %collective-permute-start.1 = (bf16[512,128]{1,0:T(8,128)(2,1)S(1)}, bf16[512,128]{1,0:T(8,128)(2,1)S(1)}, u32[]{:S(2)}, u32[]{:S(2)}) collective-permute-start(bf16[512,128]{1,0:T(8,128)(2,1)S(1)} %attend.4.refs_4_.refs_0_), channel_id=1, source_target_pairs={{0,2},{1,3},{2,4},{3,5},{4,6},{5,7},{6,0},{7,1},{8,10},{9,11},{10,... | collective-permute-start | bytes 393224 | tf_op jit(solution)/shard_map/ppermute | solution.py:268
  37.4 9.2 %collective-permute-start.2 = (bf16[512,128]{1,0:T(8,128)(2,1)S(1)}, bf16[512,128]{1,0:T(8,128)(2,1)S(1)}, u32[]{:S(2)}, u32[]{:S(2)}) collective-permute-start(bf16[512,128]{1,0:T(8,128)(2,1)S(1)} %attend.4.refs_4_.refs_0_), channel_id=1, source_target_pairs={{0,4},{1,5},{2,6},{3,7},{4,0},{5,1},{6,2},{7,3},{8,12},{9,13},{10,... | collective-permute-start | bytes 393224 | tf_op jit(solution)/shard_map/ppermute | solution.py:268
  40.3 6.3 %collective-permute-start.3 = (bf16[512,128]{1,0:T(8,128)(2,1)S(1)}, bf16[512,128]{1,0:T(8,128)(2,1)S(1)}, u32[]{:S(2)}, u32[]{:S(2)}) collective-permute-start(bf16[512,128]{1,0:T(8,128)(2,1)S(1)} %attend.4.refs_4_.refs_0_), channel_id=1, source_target_pairs={{0,6},{1,7},{2,0},{3,1},{4,2},{5,3},{6,4},{7,5},{8,14},{9,15},{10,... | collective-permute-start | bytes 393224 | tf_op jit(solution)/shard_map/ppermute | solution.py:268
  46.6 2.7 %collective-permute-start.8 = (bf16[4,512,128]{2,1,0:T(8,128)(2,1)S(1)}, bf16[4,512,128]{2,1,0:T(8,128)(2,1)S(1)}, u32[]{:S(2)}, u32[]{:S(2)}) collective-permute-start(bf16[4,512,128]{2,1,0:T(8,128)(2,1)S(1)} %stack.5), channel_id=1, source_target_pairs={{0,1},{1,0},{2,3},{3,2},{4,5},{5,4},{6,7},{7,6},{8,9},{9,8},{10,11... | collective-permute-start | bytes 1572872 | tf_op jit(solution)/shard_map/ppermute | solution.py:268
  47.8 10.4 %collective-permute-start.9 = (bf16[528,256]{1,0:T(8,128)(2,1)S(1)}, bf16[528,256]{1,0:T(8,128)(2,1)S(1)}, u32[]{:S(2)}, u32[]{:S(2)}) collective-permute-start(bf16[528,256]{1,0:T(8,128)(2,1)S(1)} %get-tuple-element.29.refs_4_.refs_2_), channel_id=1, source_target_pairs={{0,8},{8,16},{16,24},{24,32},{32,40},{40,48},{48,56},{56,64},{64,7... | collective-permute-start | bytes 811016 | tf_op jit(solution)/shard_map/ppermute | solution.py:439
  53.0 5.2 %copy-start.2 = (bf16[1024,256]{1,0:T(8,128)(2,1)S(1)}, bf16[1024,256]{1,0:T(8,128)(2,1)}, u32[]{:S(2)}) copy-start(bf16[1024,256]{1,0:T(8,128)(2,1)} %refs_6_.11) | copy-start | bytes 1572868
  54.5 6.0 %collective-permute-start.13 = (bf16[512,128]{1,0:T(8,128)(2,1)S(1)}, bf16[512,128]{1,0:T(8,128)(2,1)S(1)}, u32[]{:S(2)}, u32[]{:S(2)}) collective-permute-start(bf16[512,128]{1,0:T(8,128)(2,1)S(1)} %attend.7.refs_0_), channel_id=1, source_target_pairs={{0,2},{1,3},{2,4},{3,5},{4,6},{5,7},{6,0},{7,1},{8,10},{9,11},{10,... | collective-permute-start | bytes 393224 | tf_op jit(solution)/shard_map/ppermute | solution.py:268
  54.7 9.6 %collective-permute-start.14 = (bf16[512,128]{1,0:T(8,128)(2,1)S(1)}, bf16[512,128]{1,0:T(8,128)(2,1)S(1)}, u32[]{:S(2)}, u32[]{:S(2)}) collective-permute-start(bf16[512,128]{1,0:T(8,128)(2,1)S(1)} %attend.7.refs_0_), channel_id=1, source_target_pairs={{0,4},{1,5},{2,6},{3,7},{4,0},{5,1},{6,2},{7,3},{8,12},{9,13},{10,... | collective-permute-start | bytes 393224 | tf_op jit(solution)/shard_map/ppermute | solution.py:268
  58.2 6.0 %collective-permute-start.15 = (bf16[512,128]{1,0:T(8,128)(2,1)S(1)}, bf16[512,128]{1,0:T(8,128)(2,1)S(1)}, u32[]{:S(2)}, u32[]{:S(2)}) collective-permute-start(bf16[512,128]{1,0:T(8,128)(2,1)S(1)} %attend.7.refs_0_), channel_id=1, source_target_pairs={{0,6},{1,7},{2,0},{3,1},{4,2},{5,3},{6,4},{7,5},{8,14},{9,15},{10,... | collective-permute-start | bytes 393224 | tf_op jit(solution)/shard_map/ppermute | solution.py:268
  64.3 4.8 %collective-permute-start.16 = (bf16[4,512,128]{2,1,0:T(8,128)(2,1)S(1)}, bf16[4,512,128]{2,1,0:T(8,128)(2,1)S(1)}, u32[]{:S(2)}, u32[]{:S(2)}) collective-permute-start(bf16[4,512,128]{2,1,0:T(8,128)(2,1)S(1)} %stack.6), channel_id=1, source_target_pairs={{0,1},{1,0},{2,3},{3,2},{4,5},{5,4},{6,7},{7,6},{8,9},{9,8},{10,11... | collective-permute-start | bytes 1572872 | tf_op jit(solution)/shard_map/ppermute | solution.py:268
  65.8 6.1 %collective-permute-start.10 = (bf16[512,128]{1,0:T(8,128)(2,1)S(1)}, bf16[512,128]{1,0:T(8,128)(2,1)S(1)}, u32[]{:S(2)}, u32[]{:S(2)}) collective-permute-start(bf16[512,128]{1,0:T(8,128)(2,1)S(1)} %attend.6.refs_4_.refs_0_), channel_id=1, source_target_pairs={{0,2},{1,3},{2,4},{3,5},{4,6},{5,7},{6,0},{7,1},{8,10},{9,11},{10,... | collective-permute-start | bytes 393224 | tf_op jit(solution)/shard_map/ppermute | solution.py:268
  65.8 9.5 %collective-permute-start.11 = (bf16[512,128]{1,0:T(8,128)(2,1)S(1)}, bf16[512,128]{1,0:T(8,128)(2,1)S(1)}, u32[]{:S(2)}, u32[]{:S(2)}) collective-permute-start(bf16[512,128]{1,0:T(8,128)(2,1)S(1)} %attend.6.refs_4_.refs_0_), channel_id=1, source_target_pairs={{0,4},{1,5},{2,6},{3,7},{4,0},{5,1},{6,2},{7,3},{8,12},{9,13},{10,... | collective-permute-start | bytes 393224 | tf_op jit(solution)/shard_map/ppermute | solution.py:268
  69.1 6.3 %collective-permute-start.12 = (bf16[512,128]{1,0:T(8,128)(2,1)S(1)}, bf16[512,128]{1,0:T(8,128)(2,1)S(1)}, u32[]{:S(2)}, u32[]{:S(2)}) collective-permute-start(bf16[512,128]{1,0:T(8,128)(2,1)S(1)} %attend.6.refs_4_.refs_0_), channel_id=1, source_target_pairs={{0,6},{1,7},{2,0},{3,1},{4,2},{5,3},{6,4},{7,5},{8,14},{9,15},{10,... | collective-permute-start | bytes 393224 | tf_op jit(solution)/shard_map/ppermute | solution.py:268
  75.4 2.7 %collective-permute-start.17 = (bf16[4,512,128]{2,1,0:T(8,128)(2,1)S(1)}, bf16[4,512,128]{2,1,0:T(8,128)(2,1)S(1)}, u32[]{:S(2)}, u32[]{:S(2)}) collective-permute-start(bf16[4,512,128]{2,1,0:T(8,128)(2,1)S(1)} %stack.7), channel_id=1, source_target_pairs={{0,1},{1,0},{2,3},{3,2},{4,5},{5,4},{6,7},{7,6},{8,9},{9,8},{10,11... | collective-permute-start | bytes 1572872 | tf_op jit(solution)/shard_map/ppermute | solution.py:268

commit v4 on v3

--- a/solution.py
+++ b/solution.py
@@ -171,7 +171,9 @@
 
 def attention_kernel(head_width, layer, from_far, *refs):
     q_ref, lo_ref, hi_ref, docs_ref, bias_ref, out_ref = (*refs[:5], refs[-1])
-    half_rows, width = out_ref.shape
+    half_rows, width = docs_ref.shape[1] // 2, out_ref.shape[1]
+    if out_ref.shape[0] > half_rows:
+        out_ref[half_rows:, :] = refs[5][...]
     first_query = 0 if from_far else q_ref.shape[0] - half_rows
     if from_far:
         docs_rows = lo_ref[-DOC_ROWS:, :].astype(F32)
@@ -246,21 +248,21 @@
         out_ref[start:stop, :] = mine.astype(BF16)
 
 
-def attention(queries, lo, hi, docs, biases, layer, head_width, from_far, ahead=()):
+def attention(queries, lo, hi, docs, biases, layer, head_width, from_far, ahead=(), below=()):
     half_rows = docs.shape[1] // 2
     width = queries.shape[1]
     return pl.pallas_call(
         functools.partial(attention_kernel, head_width, layer, from_far),
-        in_specs=whole(5 + len(ahead)),
+        in_specs=whole(5 + len(below) + len(ahead)),
         out_specs=pl.BlockSpec(memory_space=pltpu.VMEM),
-        out_shape=jax.ShapeDtypeStruct((half_rows, width), BF16),
+        out_shape=jax.ShapeDtypeStruct((half_rows * (1 + len(below)), width), BF16),
         cost_estimate=cost(400 * half_rows * BAND * width, 8 * half_rows * width, half_rows * BAND * 2),
         compiler_params=pltpu.CompilerParams(vmem_limit_bytes=VMEM_LIMIT),
         name="attend",
-    )(queries, lo, hi, docs, biases, *ahead)
-
-
-def gather(block):
+    )(queries, lo, hi, docs, biases, *below, *ahead)
+
+
+def gather(block, order=(1, 2, 3)):
     chips = lax.axis_size("tp") // 2
     pairs = [(x, core) for x in range(chips) for core in range(2)]
 
@@ -275,7 +277,7 @@
         )
 
     blocks = [block]
-    for by in range(1, chips):
+    for by in order:
         blocks.append(moved(block, by))
     return moved, blocks
 
@@ -378,32 +380,44 @@
     )(*args)
 
 
-def last_kernel(gathered_count, *refs):
-    block_refs, refs = refs[:gathered_count], refs[gathered_count:]
-    own_ref, w_ref, out_ref, slots_ref = refs[0], refs[1], refs[-2], refs[-1]
-    place(lax.axis_index("tp"), block_refs, slots_ref)
-    half_rows = own_ref.shape[0]
-    attended = rows_of(slots_ref, 0, half_rows)
-    update = jnp.dot(attended, w_ref[...], preferred_element_type=F32)
-    out_ref[:half_rows, :] = (own_ref[...].astype(F32) + update).astype(BF16)
-    if len(refs) == 5:
-        out_ref[half_rows:, :] = refs[2][...]
-
-
-def last_update(blocks, own, w_out, below=()):
-    half_rows, block_width = blocks[0].shape
+def last_kernel(near_count, *refs):
+    *block_refs, early_ref, late_ref, w_ref, out_ref, slots_ref = refs
+    members = slots_ref.shape[0]
+    slots = slots_of(lax.axis_index("tp"), members // 2)
+    near_refs, near_partners, far_ref, far_partner = (
+        block_refs[:near_count],
+        block_refs[near_count],
+        block_refs[-2],
+        block_refs[-1],
+    )
+    sources = [0, 1, members // 2 - 1]
+    for i, source in enumerate(sources):
+        slots_ref[slots[source]] = near_refs[i][...]
+        slots_ref[slots[members // 2 + source]] = near_partners[i]
+    slots_ref[slots[2]] = far_ref[...]
+    slots_ref[slots[members // 2 + 2]] = far_partner[...]
+    half_rows = early_ref.shape[0]
+    for start, own_ref in ((0, early_ref), (half_rows, late_ref)):
+        attended = rows_of(slots_ref, start, half_rows)
+        update = jnp.dot(attended, w_ref[...], preferred_element_type=F32)
+        rows = own_ref[...].astype(F32) + update
+        out_ref[start : start + half_rows, :] = rows.astype(BF16)
+
+
+def last_update(attended, early, late, w_out):
+    moved, blocks = gather(attended, (1, 3, 2))
+    near, far = blocks[:3], blocks[3]
+    near = from_partner(moved, near, near[0])
+    args = [*near, far, moved(far, 0, True), early, late, w_out]
+    rows, block_width = attended.shape
     inner, col_width = w_out.shape
-    args = [*blocks, own, w_out, *below]
-    rows = half_rows + sum(array.shape[0] for array in below)
     return pl.pallas_call(
-        functools.partial(last_kernel, len(blocks)),
+        functools.partial(last_kernel, len(near) - 1),
         in_specs=whole(len(args)),
         out_specs=pl.BlockSpec(memory_space=pltpu.VMEM),
-        scratch_shapes=[pltpu.VMEM((inner // block_width, half_rows, block_width), BF16)],
+        scratch_shapes=[pltpu.VMEM((inner // block_width, rows, block_width), BF16)],
         out_shape=jax.ShapeDtypeStruct((rows, col_width), BF16),
-        cost_estimate=cost(
-            2 * half_rows * inner * col_width, 2 * inner * (half_rows + col_width)
-        ),
+        cost_estimate=cost(2 * rows * inner * col_width, 2 * inner * (rows + col_width)),
         compiler_params=pltpu.CompilerParams(vmem_limit_bytes=VMEM_LIMIT),
         name="last",
     )(*args)
@@ -425,26 +439,25 @@
     result = None
     for layer in range(LAYERS):
         late = attention(q_late, kv_early, kv_late, docs, biases, layer, head_width, False)
+        if layer == LAYERS - 1:
+            attended = attention(
+                q_early, far, kv_early, docs, biases, layer, head_width, True,
+                (out_last,), (late,),
+            )
+            result = last_update(attended, own_early, own_late, out_last)
+            break
         moved, late = gather(late)
-        ahead = (tokens, out_first) if layer == 0 else (out_last,)
         early = attention(
-            q_early, far, kv_early, docs, biases, layer, head_width, True, ahead
+            q_early, far, kv_early, docs, biases, layer, head_width, True, (tokens, out_first)
         )
         late = from_partner(moved, late, early)
         moved, early = gather(early)
-        if layer == 0:
-            q_late, kv_late, own_late = next_heads(
-                late, tokens, out_first, *weights, docs, 1, q_scale
-            )
-            far = lax.ppermute(kv_late, "sp", onward)
-            early = from_partner(moved, early, kv_late)
-            q_early, kv_early, own_early = next_heads(
-                early, tokens, out_first, *weights, docs, 0, q_scale
-            )
-        else:
-            below = last_update(late, own_late, out_last)
-            early = from_partner(moved, early, below)
-            result = last_update(early, own_early, out_last, (below,))
+        q_late, kv_late, own_late = next_heads(late, tokens, out_first, *weights, docs, 1, q_scale)
+        far = lax.ppermute(kv_late, "sp", onward)
+        early = from_partner(moved, early, kv_late)
+        q_early, kv_early, own_early = next_heads(
+            early, tokens, out_first, *weights, docs, 0, q_scale
+        )
     return result
 
 

time: 79.5 us -> 80.1 us (level)
  waiting for transfers between devices: 17.2 us -> 19.8 us
  starting transfers between devices: 41.6 us -> 39.7 us
    ppermute x16 -> x13, waiting for transfers between devices: 17.2 us -> 19.2 us  [moved(): lax.ppermute(array, 'tp', [(2 * x + core, 2 * ((x + by) % chips) + (1 - c...]
    ppermute x16 -> x13, starting transfers between devices: 35.1 us -> 33.2 us  [moved(): lax.ppermute(array, 'tp', [(2 * x + core, 2 * ((x + by) % chips) + (1 - c...]
    pallas_call x2 -> x1, Pallas kernels: 1.79 us -> 1.64 us  [last_update(): pl.pallas_call(functools.partial(last_kernel, len(near) - 1), in_specs=wh...]
  transfers between devices with their start and end apart: 18 -> 15, of which waited for: 8 -> 7; matrix products, arithmetic and copies ran while one was open for 0% -> 0% of each run, Pallas kernels for 18% -> 15%
where the time goes in v4:
time: 80.1 us; the launch traced here: 79.9 us
  starting transfers between devices  39.7 us (50%)
  Pallas kernels  20.2 us (25%)
  waiting for transfers between devices  19.8 us (25%)
    ppermute x13, starting transfers between devices, moved(): lax.ppermute(array, 'tp', [(2 * x + core, 2 * ((x + by) % chips) + (1 - c...  33.2 us
    ppermute x13, waiting for transfers between devices, moved(): lax.ppermute(array, 'tp', [(2 * x + core, 2 * ((x + by) % chips) + (1 - c...  19.2 us
    pallas_call x2, Pallas kernels, next_heads(): pl.pallas_call(functools.partial(next_kernel, q_scale, block_rows, len(bl...  7.34 us
    ppermute x2, starting transfers between devices, shards(): far = lax.ppermute(kv_late, 'sp', onward)  6.58 us
    pallas_call x4, Pallas kernels, attention(): pl.pallas_call(functools.partial(attention_kernel, head_width, layer, fro...  6.1 us
    pallas_call x1, Pallas kernels, heads(): pl.pallas_call(functools.partial(heads_kernel, q_scale, block_rows), in_s...  5 us
    pallas_call x1, Pallas kernels, last_update(): pl.pallas_call(functools.partial(last_kernel, len(near) - 1), in_specs=wh...  1.64 us
  transfers between devices with their start and end apart: 15, of which 7 were waited for; matrix products, arithmetic and copies ran while one was open for 0% of the time, Pallas kernels for 15%

profile of v4, /device:TPU:33, one launch (start us, length us, event | category | flops | bytes accessed | tf_op | source)
XLA Modules:
  0.0 79.9 jit_solution(7696412860856175675)
XLA Ops:
  0.0 5.0 %heads.1 = (bf16[1024,128]{1,0:T(8,128)(2,1)S(1)}, bf16[512,256]{1,0:T(8,128)(2,1)S(1)}, bf16[528,256]{1,0:T(8,128)(2,1)S(1)}, f32[1,1024]{1,0:T(1,128)S(1)}, f3...) custom-call(bf16[1024,2048]{1,0:T(8,128)(2,1)} %refs_5_.7, ...), custom_call_target="tpu_custom_call" | custom-call | flops 1610612736 | bytes 5767168 | tf_op jit(solution)/shard_map/heads/pallas_call | solution.py:122
  5.0 5.3 %collective-permute-start = (bf16[528,256]{1,0:T(8,128)(2,1)S(1)}, bf16[528,256]{1,0:T(8,128)(2,1)S(1)}, u32[]{:S(2)}, u32[]{:S(2)}) collective-permute-start(bf16[528,256]{1,0:T(8,128)(2,1)S(1)} %get-tuple-element.21.refs_2_), channel_id=1, source_target_pairs={{0,8},{8,16},{16,24},{24,32},{32,40},{40,48},{48,56},{56,64},{64,7... | collective-permute-start | bytes 811016 | tf_op jit(solution)/shard_map/ppermute | solution.py:438
  10.3 0.0 copy-start
  10.3 0.0 copy-start.1
  10.3 1.5 %attend.5.refs_0_ = bf16[512,128]{1,0:T(8,128)(2,1)S(1)} custom-call(bf16[1024,128]{1,0:T(8,128)(2,1)S(1)} %get-tuple-element.20.refs_0_, bf16[512,256]{1,0:T(8,128)(2,1)S(1)} %get-tuple-element.22.refs_2_.refs_1_, bf16[528,256]{1,0:T(8,128)(2,1)S(1)} %get-tuple-element.21.refs_2_, f32[1,1024]{1,0:T(1,128)S(1)} %get-tuple-element.23.refs_3_.refs_11_, ...), custom_call_target="tpu_custom_call" | custom-call | flops 16777216000 | bytes 524288 | tf_op jit(solution)/shard_map/attend/pallas_call | solution.py:254
  11.8 1.5 %collective-permute-start.4 = (bf16[512,128]{1,0:T(8,128)(2,1)S(1)}, bf16[512,128]{1,0:T(8,128)(2,1)S(1)}, u32[]{:S(2)}, u32[]{:S(2)}) collective-permute-start(bf16[512,128]{1,0:T(8,128)(2,1)S(1)} %attend.5.refs_0_), channel_id=1, source_target_pairs={{0,2},{1,3},{2,4},{3,5},{4,6},{5,7},{6,0},{7,1},{8,10},{9,11},{10,... | collective-permute-start | bytes 393224 | tf_op jit(solution)/shard_map/ppermute | solution.py:270
  13.3 2.7 %collective-permute-start.5 = (bf16[512,128]{1,0:T(8,128)(2,1)S(1)}, bf16[512,128]{1,0:T(8,128)(2,1)S(1)}, u32[]{:S(2)}, u32[]{:S(2)}) collective-permute-start(bf16[512,128]{1,0:T(8,128)(2,1)S(1)} %attend.5.refs_0_), channel_id=1, source_target_pairs={{0,4},{1,5},{2,6},{3,7},{4,0},{5,1},{6,2},{7,3},{8,12},{9,13},{10,... | collective-permute-start | bytes 393224 | tf_op jit(solution)/shard_map/ppermute | solution.py:270
  16.0 1.0 %collective-permute-start.6 = (bf16[512,128]{1,0:T(8,128)(2,1)S(1)}, bf16[512,128]{1,0:T(8,128)(2,1)S(1)}, u32[]{:S(2)}, u32[]{:S(2)}) collective-permute-start(bf16[512,128]{1,0:T(8,128)(2,1)S(1)} %attend.5.refs_0_), channel_id=1, source_target_pairs={{0,6},{1,7},{2,0},{3,1},{4,2},{5,3},{6,4},{7,5},{8,14},{9,15},{10,... | collective-permute-start | bytes 393224 | tf_op jit(solution)/shard_map/ppermute | solution.py:270
  17.1 1.5 %attend.4.refs_4_.refs_0_ = bf16[512,128]{1,0:T(8,128)(2,1)S(1)} custom-call(bf16[1024,128]{1,0:T(8,128)(2,1)S(1)} %get-tuple-element.20.refs_0_, bf16[528,256]{1,0:T(8,128)(2,1)S(1)} %collective-permute-done.refs_1_, bf16[512,256]{1,0:T(8,128)(2,1)S(1)} %get-tuple-element.22.refs_2_.refs_1_, f32[1,1024]{1,0:T(1,128)S(1)} %get-tuple-element.23.refs_3_.refs_11_, ...), custom_call_target="tpu_custom_call" | custom-call | flops 16777216000 | bytes 524288 | tf_op jit(solution)/shard_map/attend/pallas_call | solution.py:254
  18.6 2.6 %collective-permute-done.5.refs_2_ = bf16[512,128]{1,0:T(8,128)(2,1)S(1)} collective-permute-done((bf16[512,128]{1,0:T(8,128)(2,1)S(1)}, bf16[512,128]{1,0:T(8,128)(2,1)S(1)}, u32[]{:S(2)}, u32[]{:S(2)}) %collective-permute-start.5) | collective-permute-done | bytes 131104 | tf_op jit(solution)/shard_map/ppermute | solution.py:270
  21.2 15.8 %collective-permute-start.7 = (bf16[4,512,128]{2,1,0:T(8,128)(2,1)S(1)}, bf16[4,512,128]{2,1,0:T(8,128)(2,1)S(1)}, u32[]{:S(2)}, u32[]{:S(2)}) collective-permute-start(bf16[4,512,128]{2,1,0:T(8,128)(2,1)S(1)} %stack.3), channel_id=1, source_target_pairs={{0,1},{1,0},{2,3},{3,2},{4,5},{5,4},{6,7},{7,6},{8,9},{9,8},{10,11... | collective-permute-start | bytes 1572872 | tf_op jit(solution)/shard_map/ppermute | solution.py:270
  37.1 0.3 collective-permute-start.1
  37.4 2.9 %collective-permute-start.2 = (bf16[512,128]{1,0:T(8,128)(2,1)S(1)}, bf16[512,128]{1,0:T(8,128)(2,1)S(1)}, u32[]{:S(2)}, u32[]{:S(2)}) collective-permute-start(bf16[512,128]{1,0:T(8,128)(2,1)S(1)} %attend.4.refs_4_.refs_0_), channel_id=1, source_target_pairs={{0,4},{1,5},{2,6},{3,7},{4,0},{5,1},{6,2},{7,3},{8,12},{9,13},{10,... | collective-permute-start | bytes 393224 | tf_op jit(solution)/shard_map/ppermute | solution.py:270
  40.3 3.7 %next_heads.2 = (bf16[512,128]{1,0:T(8,128)(2,1)S(1)}, bf16[528,256]{1,0:T(8,128)(2,1)S(1)}, bf16[512,256]{1,0:T(8,128)(2,1)S(1)}) custom-call(bf16[512,128]{1,0:T(8,128)(2,1)S(1)} %attend.5.refs_0_, bf16[512,128]{1,0:T(8,128)(2,1)S(1)} %collective-permute-done.4.refs_1_, bf16[512,128]{1,0:T(8,128)(2,1)S(1)} %collective-permute-done.5.refs_2_, ...), custom_call_target="tpu_custom_call" | custom-call | flops 2952790016 | bytes 7864320 | tf_op jit(solution)/shard_map/next_heads/pallas_call | solution.py:361
  44.0 2.6 %collective-permute-done.2.refs_2_ = bf16[512,128]{1,0:T(8,128)(2,1)S(1)} collective-permute-done((bf16[512,128]{1,0:T(8,128)(2,1)S(1)}, bf16[512,128]{1,0:T(8,128)(2,1)S(1)}, u32[]{:S(2)}, u32[]{:S(2)}) %collective-permute-start.2) | collective-permute-done | bytes 131104 | tf_op jit(solution)/shard_map/ppermute | solution.py:270
  46.6 1.1 %collective-permute-start.8 = (bf16[4,512,128]{2,1,0:T(8,128)(2,1)S(1)}, bf16[4,512,128]{2,1,0:T(8,128)(2,1)S(1)}, u32[]{:S(2)}, u32[]{:S(2)}) collective-permute-start(bf16[4,512,128]{2,1,0:T(8,128)(2,1)S(1)} %stack.4), channel_id=1, source_target_pairs={{0,1},{1,0},{2,3},{3,2},{4,5},{5,4},{6,7},{7,6},{8,9},{9,8},{10,11... | collective-permute-start | bytes 1572872 | tf_op jit(solution)/shard_map/ppermute | solution.py:270
  47.8 1.3 %collective-permute-start.9 = (bf16[528,256]{1,0:T(8,128)(2,1)S(1)}, bf16[528,256]{1,0:T(8,128)(2,1)S(1)}, u32[]{:S(2)}, u32[]{:S(2)}) collective-permute-start(bf16[528,256]{1,0:T(8,128)(2,1)S(1)} %get-tuple-element.29.refs_4_.refs_2_), channel_id=1, source_target_pairs={{0,8},{8,16},{16,24},{24,32},{32,40},{40,48},{48,56},{56,64},{64,7... | collective-permute-start | bytes 811016 | tf_op jit(solution)/shard_map/ppermute | solution.py:456
  49.1 0.2 collective-permute-done.8.refs_4_
  49.3 3.7 %next_heads.3 = (bf16[512,128]{1,0:T(8,128)(2,1)S(1)}, bf16[512,256]{1,0:T(8,128)(2,1)S(1)}, bf16[512,256]{1,0:T(8,128)(2,1)S(1)}) custom-call(bf16[512,128]{1,0:T(8,128)(2,1)S(1)} %attend.4.refs_4_.refs_0_, bf16[512,128]{1,0:T(8,128)(2,1)S(1)} %collective-permute-done.1.refs_1_, bf16[512,128]{1,0:T(8,128)(2,1)S(1)} %collective-permute-done.2.refs_2_, ...), custom_call_target="tpu_custom_call" | custom-call | flops 2952790016 | bytes 7864320 | tf_op jit(solution)/shard_map/next_heads/pallas_call | solution.py:361
  53.0 1.5 %attend.6.refs_5_ = bf16[512,128]{1,0:T(8,128)(2,1)S(1)} custom-call(bf16[512,128]{1,0:T(8,128)(2,1)S(1)} %get-tuple-element.32.refs_0_, bf16[512,256]{1,0:T(8,128)(2,1)S(1)} %get-tuple-element.31.refs_1_.refs_2_, bf16[528,256]{1,0:T(8,128)(2,1)S(1)} %get-tuple-element.29.refs_4_.refs_2_, f32[1,1024]{1,0:T(1,128)S(1)} %get-tuple-element.23.refs_3_.refs_11_, ...), custom_call_target="tpu_custom_call" | custom-call | flops 16777216000 | bytes 524288 | tf_op jit(solution)/shard_map/attend/pallas_call | solution.py:254
  54.5 0.6 collective-permute-done.9.refs_1_
  55.1 1.5 %attend.7.refs_0_.refs_3_ = bf16[1024,128]{1,0:T(8,128)(2,1)S(1)} custom-call(bf16[512,128]{1,0:T(8,128)(2,1)S(1)} %get-tuple-element.30.refs_0_, bf16[528,256]{1,0:T(8,128)(2,1)S(1)} %collective-permute-done.9.refs_1_, bf16[512,256]{1,0:T(8,128)(2,1)S(1)} %get-tuple-element.31.refs_1_.refs_2_, f32[1,1024]{1,0:T(1,128)S(1)} %get-tuple-element.23.refs_3_.refs_11_, ...), custom_call_target="tpu_custom_call" | custom-call | flops 16777216000 | bytes 524288 | tf_op jit(solution)/shard_map/attend/pallas_call | solution.py:254
  56.7 0.1 collective-permute-start.10
  56.8 2.6 %collective-permute-start.11 = (bf16[1024,128]{1,0:T(8,128)(2,1)S(1)}, bf16[1024,128]{1,0:T(8,128)(2,1)S(1)}, u32[]{:S(2)}, u32[]{:S(2)}) collective-permute-start(bf16[1024,128]{1,0:T(8,128)(2,1)S(1)} %attend.7.refs_0_.refs_3_), channel_id=1, source_target_pairs={{0,6},{1,7},{2,0},{3,1},{4,2},{5,3},{6,4},{7,5},{8,14},{9,15},{10,... | collective-permute-start | bytes 786440 | tf_op jit(solution)/shard_map/ppermute | solution.py:270
  59.4 5.8 %collective-permute-done.10.refs_1_ = bf16[1024,128]{1,0:T(8,128)(2,1)S(1)} collective-permute-done((bf16[1024,128]{1,0:T(8,128)(2,1)S(1)}, bf16[1024,128]{1,0:T(8,128)(2,1)S(1)}, u32[]{:S(2)}, u32[]{:S(2)}) %collective-permute-start.10) | collective-permute-done | bytes 262176 | tf_op jit(solution)/shard_map/ppermute | solution.py:270
  65.2 0.1 stack.5
  65.3 1.6 %collective-permute-start.12 = (bf16[3,1024,128]{2,1,0:T(8,128)(2,1)S(1)}, bf16[3,1024,128]{2,1,0:T(8,128)(2,1)S(1)}, u32[]{:S(2)}, u32[]{:S(2)}) collective-permute-start(bf16[3,1024,128]{2,1,0:T(8,128)(2,1)S(1)} %stack.5), channel_id=1, source_target_pairs={{0,1},{1,0},{2,3},{3,2},{4,5},{5,4},{6,7},{7,6},{8,9},{9,8},{10,11... | collective-permute-start | bytes 2359304 | tf_op jit(solution)/shard_map/ppermute | solution.py:270
  66.9 2.3 %collective-permute-start.13 = (bf16[1024,128]{1,0:T(8,128)(2,1)S(1)}, bf16[1024,128]{1,0:T(8,128)(2,1)S(1)}, u32[]{:S(2)}, u32[]{:S(2)}) collective-permute-start(bf16[1024,128]{1,0:T(8,128)(2,1)S(1)} %attend.7.refs_0_.refs_3_), channel_id=1, source_target_pairs={{0,4},{1,5},{2,6},{3,7},{4,0},{5,1},{6,2},{7,3},{8,12},{9,13},{10,... | collective-permute-start | bytes 786440 | tf_op jit(solution)/shard_map/ppermute | solution.py:270
  69.2 6.9 %collective-permute-done.13.refs_4_ = bf16[1024,128]{1,0:T(8,128)(2,1)S(1)} collective-permute-done((bf16[1024,128]{1,0:T(8,128)(2,1)S(1)}, bf16[1024,128]{1,0:T(8,128)(2,1)S(1)}, u32[]{:S(2)}, u32[]{:S(2)}) %collective-permute-start.13) | collective-permute-done | bytes 262176 | tf_op jit(solution)/shard_map/ppermute | solution.py:270
  76.1 1.0 %collective-permute-start.14 = (bf16[1024,128]{1,0:T(8,128)(2,1)S(1)}, bf16[1024,128]{1,0:T(8,128)(2,1)S(1)}, u32[]{:S(2)}, u32[]{:S(2)}) collective-permute-start(bf16[1024,128]{1,0:T(8,128)(2,1)S(1)} %collective-permute-done.13.refs_4_), channel_id=1, source_target_pairs={{0,1},{1,0},{2,3},{3,2},{4,5},{5,4},{6,7},{7,6},{8,9},{9,8},{10,11... | collective-permute-start | bytes 786440 | tf_op jit(solution)/shard_map/ppermute | solution.py:270
  77.1 1.2 %collective-permute-done.14.refs_5_ = bf16[1024,128]{1,0:T(8,128)(2,1)S(1)} collective-permute-done((bf16[1024,128]{1,0:T(8,128)(2,1)S(1)}, bf16[1024,128]{1,0:T(8,128)(2,1)S(1)}, u32[]{:S(2)}, u32[]{:S(2)}) %collective-permute-start.14) | collective-permute-done | bytes 262176 | tf_op jit(solution)/shard_map/ppermute | solution.py:270
  78.3 1.6 %last.1 = bf16[1024,256]{1,0:T(8,128)(2,1)} custom-call(bf16[1024,128]{1,0:T(8,128)(2,1)S(1)} %attend.7.refs_0_.refs_3_, bf16[1024,128]{1,0:T(8,128)(2,1)S(1)} %collective-permute-done.10.refs_1_, bf16[1024,128]{1,0:T(8,128)(2,1)S(1)} %collective-permute-done.11.refs_2_, bf16[3,1024,128]{2,1,0:T(8,128)(2,1)S(1)} %collective-permute-done.12.refs_3_, ...), custom_call_target="tpu_custom_call" | custom-call | flops 536870912 | bytes 2621440 | tf_op jit(solution)/shard_map/last/pallas_call | solution.py:414
  (15 shorter events, 0.1 us)
Async XLA Ops:
  5.0 12.0 %collective-permute-start = (bf16[528,256]{1,0:T(8,128)(2,1)S(1)}, bf16[528,256]{1,0:T(8,128)(2,1)S(1)}, u32[]{:S(2)}, u32[]{:S(2)}) collective-permute-start(bf16[528,256]{1,0:T(8,128)(2,1)S(1)} %get-tuple-element.21.refs_2_), channel_id=1, source_target_pairs={{0,8},{8,16},{16,24},{24,32},{32,40},{40,48},{48,56},{56,64},{64,7... | collective-permute-start | bytes 811016 | tf_op jit(solution)/shard_map/ppermute | solution.py:438
  10.3 6.8 %copy-start = (bf16[1024,2048]{1,0:T(8,128)(2,1)S(1)}, bf16[1024,2048]{1,0:T(8,128)(2,1)}, u32[]{:S(2)}) copy-start(bf16[1024,2048]{1,0:T(8,128)(2,1)} %refs_5_.7) | copy-start | bytes 12582916
  10.3 6.8 %copy-start.1 = (bf16[1024,2048]{1,0:T(8,128)(2,1)S(1)}, bf16[1024,2048]{1,0:T(8,128)(2,1)}, u32[]{:S(2)}) copy-start(bf16[1024,2048]{1,0:T(8,128)(2,1)} %refs_6_.8) | copy-start | bytes 12582916
  11.8 6.7 %collective-permute-start.4 = (bf16[512,128]{1,0:T(8,128)(2,1)S(1)}, bf16[512,128]{1,0:T(8,128)(2,1)S(1)}, u32[]{:S(2)}, u32[]{:S(2)}) collective-permute-start(bf16[512,128]{1,0:T(8,128)(2,1)S(1)} %attend.5.refs_0_), channel_id=1, source_target_pairs={{0,2},{1,3},{2,4},{3,5},{4,6},{5,7},{6,0},{7,1},{8,10},{9,11},{10,... | collective-permute-start | bytes 393224 | tf_op jit(solution)/shard_map/ppermute | solution.py:270
  13.3 7.9 %collective-permute-start.5 = (bf16[512,128]{1,0:T(8,128)(2,1)S(1)}, bf16[512,128]{1,0:T(8,128)(2,1)S(1)}, u32[]{:S(2)}, u32[]{:S(2)}) collective-permute-start(bf16[512,128]{1,0:T(8,128)(2,1)S(1)} %attend.5.refs_0_), channel_id=1, source_target_pairs={{0,4},{1,5},{2,6},{3,7},{4,0},{5,1},{6,2},{7,3},{8,12},{9,13},{10,... | collective-permute-start | bytes 393224 | tf_op jit(solution)/shard_map/ppermute | solution.py:270
  16.0 5.2 %collective-permute-start.6 = (bf16[512,128]{1,0:T(8,128)(2,1)S(1)}, bf16[512,128]{1,0:T(8,128)(2,1)S(1)}, u32[]{:S(2)}, u32[]{:S(2)}) collective-permute-start(bf16[512,128]{1,0:T(8,128)(2,1)S(1)} %attend.5.refs_0_), channel_id=1, source_target_pairs={{0,6},{1,7},{2,0},{3,1},{4,2},{5,3},{6,4},{7,5},{8,14},{9,15},{10,... | collective-permute-start | bytes 393224 | tf_op jit(solution)/shard_map/ppermute | solution.py:270
  21.2 19.1 %collective-permute-start.7 = (bf16[4,512,128]{2,1,0:T(8,128)(2,1)S(1)}, bf16[4,512,128]{2,1,0:T(8,128)(2,1)S(1)}, u32[]{:S(2)}, u32[]{:S(2)}) collective-permute-start(bf16[4,512,128]{2,1,0:T(8,128)(2,1)S(1)} %stack.3), channel_id=1, source_target_pairs={{0,1},{1,0},{2,3},{3,2},{4,5},{5,4},{6,7},{7,6},{8,9},{9,8},{10,11... | collective-permute-start | bytes 1572872 | tf_op jit(solution)/shard_map/ppermute | solution.py:270
  37.1 6.9 %collective-permute-start.1 = (bf16[512,128]{1,0:T(8,128)(2,1)S(1)}, bf16[512,128]{1,0:T(8,128)(2,1)S(1)}, u32[]{:S(2)}, u32[]{:S(2)}) collective-permute-start(bf16[512,128]{1,0:T(8,128)(2,1)S(1)} %attend.4.refs_4_.refs_0_), channel_id=1, source_target_pairs={{0,2},{1,3},{2,4},{3,5},{4,6},{5,7},{6,0},{7,1},{8,10},{9,11},{10,... | collective-permute-start | bytes 393224 | tf_op jit(solution)/shard_map/ppermute | solution.py:270
  37.4 9.2 %collective-permute-start.2 = (bf16[512,128]{1,0:T(8,128)(2,1)S(1)}, bf16[512,128]{1,0:T(8,128)(2,1)S(1)}, u32[]{:S(2)}, u32[]{:S(2)}) collective-permute-start(bf16[512,128]{1,0:T(8,128)(2,1)S(1)} %attend.4.refs_4_.refs_0_), channel_id=1, source_target_pairs={{0,4},{1,5},{2,6},{3,7},{4,0},{5,1},{6,2},{7,3},{8,12},{9,13},{10,... | collective-permute-start | bytes 393224 | tf_op jit(solution)/shard_map/ppermute | solution.py:270
  40.3 6.3 %collective-permute-start.3 = (bf16[512,128]{1,0:T(8,128)(2,1)S(1)}, bf16[512,128]{1,0:T(8,128)(2,1)S(1)}, u32[]{:S(2)}, u32[]{:S(2)}) collective-permute-start(bf16[512,128]{1,0:T(8,128)(2,1)S(1)} %attend.4.refs_4_.refs_0_), channel_id=1, source_target_pairs={{0,6},{1,7},{2,0},{3,1},{4,2},{5,3},{6,4},{7,5},{8,14},{9,15},{10,... | collective-permute-start | bytes 393224 | tf_op jit(solution)/shard_map/ppermute | solution.py:270
  46.6 2.7 %collective-permute-start.8 = (bf16[4,512,128]{2,1,0:T(8,128)(2,1)S(1)}, bf16[4,512,128]{2,1,0:T(8,128)(2,1)S(1)}, u32[]{:S(2)}, u32[]{:S(2)}) collective-permute-start(bf16[4,512,128]{2,1,0:T(8,128)(2,1)S(1)} %stack.4), channel_id=1, source_target_pairs={{0,1},{1,0},{2,3},{3,2},{4,5},{5,4},{6,7},{7,6},{8,9},{9,8},{10,11... | collective-permute-start | bytes 1572872 | tf_op jit(solution)/shard_map/ppermute | solution.py:270
  47.8 7.4 %collective-permute-start.9 = (bf16[528,256]{1,0:T(8,128)(2,1)S(1)}, bf16[528,256]{1,0:T(8,128)(2,1)S(1)}, u32[]{:S(2)}, u32[]{:S(2)}) collective-permute-start(bf16[528,256]{1,0:T(8,128)(2,1)S(1)} %get-tuple-element.29.refs_4_.refs_2_), channel_id=1, source_target_pairs={{0,8},{8,16},{16,24},{24,32},{32,40},{40,48},{48,56},{56,64},{64,7... | collective-permute-start | bytes 811016 | tf_op jit(solution)/shard_map/ppermute | solution.py:456
  53.0 2.2 %copy-start.2 = (bf16[1024,256]{1,0:T(8,128)(2,1)S(1)}, bf16[1024,256]{1,0:T(8,128)(2,1)}, u32[]{:S(2)}) copy-start(bf16[1024,256]{1,0:T(8,128)(2,1)} %refs_8_.1) | copy-start | bytes 1572868
  56.7 8.6 %collective-permute-start.10 = (bf16[1024,128]{1,0:T(8,128)(2,1)S(1)}, bf16[1024,128]{1,0:T(8,128)(2,1)S(1)}, u32[]{:S(2)}, u32[]{:S(2)}) collective-permute-start(bf16[1024,128]{1,0:T(8,128)(2,1)S(1)} %attend.7.refs_0_.refs_3_), channel_id=1, source_target_pairs={{0,2},{1,3},{2,4},{3,5},{4,6},{5,7},{6,0},{7,1},{8,10},{9,11},{10,... | collective-permute-start | bytes 786440 | tf_op jit(solution)/shard_map/ppermute | solution.py:270
  56.8 8.4 %collective-permute-start.11 = (bf16[1024,128]{1,0:T(8,128)(2,1)S(1)}, bf16[1024,128]{1,0:T(8,128)(2,1)S(1)}, u32[]{:S(2)}, u32[]{:S(2)}) collective-permute-start(bf16[1024,128]{1,0:T(8,128)(2,1)S(1)} %attend.7.refs_0_.refs_3_), channel_id=1, source_target_pairs={{0,6},{1,7},{2,0},{3,1},{4,2},{5,3},{6,4},{7,5},{8,14},{9,15},{10,... | collective-permute-start | bytes 786440 | tf_op jit(solution)/shard_map/ppermute | solution.py:270
  65.3 13.0 %collective-permute-start.12 = (bf16[3,1024,128]{2,1,0:T(8,128)(2,1)S(1)}, bf16[3,1024,128]{2,1,0:T(8,128)(2,1)S(1)}, u32[]{:S(2)}, u32[]{:S(2)}) collective-permute-start(bf16[3,1024,128]{2,1,0:T(8,128)(2,1)S(1)} %stack.5), channel_id=1, source_target_pairs={{0,1},{1,0},{2,3},{3,2},{4,5},{5,4},{6,7},{7,6},{8,9},{9,8},{10,11... | collective-permute-start | bytes 2359304 | tf_op jit(solution)/shard_map/ppermute | solution.py:270
  66.9 9.2 %collective-permute-start.13 = (bf16[1024,128]{1,0:T(8,128)(2,1)S(1)}, bf16[1024,128]{1,0:T(8,128)(2,1)S(1)}, u32[]{:S(2)}, u32[]{:S(2)}) collective-permute-start(bf16[1024,128]{1,0:T(8,128)(2,1)S(1)} %attend.7.refs_0_.refs_3_), channel_id=1, source_target_pairs={{0,4},{1,5},{2,6},{3,7},{4,0},{5,1},{6,2},{7,3},{8,12},{9,13},{10,... | collective-permute-start | bytes 786440 | tf_op jit(solution)/shard_map/ppermute | solution.py:270
  76.1 2.2 %collective-permute-start.14 = (bf16[1024,128]{1,0:T(8,128)(2,1)S(1)}, bf16[1024,128]{1,0:T(8,128)(2,1)S(1)}, u32[]{:S(2)}, u32[]{:S(2)}) collective-permute-start(bf16[1024,128]{1,0:T(8,128)(2,1)S(1)} %collective-permute-done.13.refs_4_), channel_id=1, source_target_pairs={{0,1},{1,0},{2,3},{3,2},{4,5},{5,4},{6,7},{7,6},{8,9},{9,8},{10,11... | collective-permute-start | bytes 786440 | tf_op jit(solution)/shard_map/ppermute | solution.py:270
